TPU v7x, 512 devices: a 8x2x16 block of a 8x8x16 slice. The times are simulated.
512 devices in a mesh: grp: 2 (over y), dp: 8 (over x), kv: 16 (over z), tp: 2 (over core).
Axes of the slice: x: 8, y: 2, z: 16, core: 2. Of those that a mesh axis runs over, the one named last changes fastest.
The devices are a block of a 8x8x16 slice.
Arguments:
- inputs: bfloat16 [512, 4096], P(('grp', 'dp'), 'kv'), parts along dimension 0, may hold values from -6 to 6
- gain_in: float32 [4096], P('kv'), may hold values from 0.1 to 1.9
- w_gate: bfloat16 [4096, 2048], P('kv', 'tp'), may hold values from -0.09375 to 0.09375
- w_input: bfloat16 [4096, 2048], P('kv', 'tp'), may hold values from -0.09375 to 0.09375
- w_bproj: bfloat16 [4096, 1024], P('kv', 'tp'), may hold values from -0.09375 to 0.09375
- w_cproj: bfloat16 [4096, 1024], P('kv', 'tp'), may hold values from -0.09375 to 0.09375
- w_step: bfloat16 [4096, 32], P('kv', 'tp'), may hold values from -0.09375 to 0.09375
- conv_input: float32 [4, 2048], P(None, 'tp'), may hold values from -3 to 3
- conv_bproj: float32 [4, 1024], P(None, 'tp'), may hold values from -3 to 3
- conv_cproj: float32 [4, 1024], P(None, 'tp'), may hold values from -3 to 3
- tail_input: bfloat16 [512, 3, 2048], P(('grp', 'dp', 'kv'), None, 'tp'), parts along dimension 0, may hold values from -6 to 6
- tail_bproj: bfloat16 [512, 3, 1024], P(('grp', 'dp', 'kv'), None, 'tp'), parts along dimension 0, may hold values from -6 to 6
- tail_cproj: bfloat16 [512, 3, 1024], P(('grp', 'dp', 'kv'), None, 'tp'), parts along dimension 0, may hold values from -6 to 6
- step_bias: float32 [32], P('tp'), may hold values from -3 to 0
- decay_log: float32 [32], P('tp'), may hold values from -2 to 2
- block_input: bfloat16 [512, 128, 2048], P(('grp', 'dp', 'kv'), None, 'tp'), parts along dimension 0, may hold values from -6 to 6
- block_bproj: bfloat16 [512, 128, 1024], P(('grp', 'dp', 'kv'), None, 'tp'), parts along dimension 0, may hold values from -0.59765625 to 0.59765625
- block_step: float32 [512, 128, 32], P(('grp', 'dp', 'kv'), None, 'tp'), parts along dimension 0, may hold values from 0.005 to 0.2
- lengths: int32 [512], P(('grp', 'dp', 'kv')), parts along dimension 0, may hold values from 1 to 127, 8192 in all
- state: float32 [512, 32, 64, 128], P(('grp', 'dp', 'kv'), 'tp'), parts along dimension 0, may hold values from -0.6 to 0.6
- gain_mix: float32 [2048], P('tp'), may hold values from 0.1 to 1.9
- w_out: bfloat16 [2048, 4096], P('tp', 'kv'), may hold values from -0.125 to 0.125
- gain_mlp: float32 [4096], P(('kv', 'tp')), may hold values from 0.1 to 1.9
- w_up: bfloat16 [4096, 16384], P(('kv', 'tp'), 'dp'), may hold values from -0.09375 to 0.09375
- w_down: bfloat16 [16384, 4096], P('dp', ('kv', 'tp')), may hold values from -0.046875 to 0.046875
Outputs:
- layer_out: bfloat16 [512, 4096], P(('grp', 'dp'), ('kv', 'tp')), parts along dimension 0
There are 2 independent parts, one for each index of `grp`. A program takes and returns all parts, laid end to end along the dimension named above; an argument that names none is the same for every part. Nothing has to cross between parts.
Inputs may be any that keep to these rules, and one draw needn't show every extreme that they name: `lengths`: the number of live positions before the new token in each sequence's current block; the largest equals 127 in every draw.
All inputs are finite; a program needn't handle non-finite values.
Results may differ from a plain program's by a relative error of at most 0.012.
Values may be sent and summed in bfloat16 or wider, within the bound.
No kernel may reach another device: no remote copies, remote signals or barrier semaphores. Data moves between devices by JAX's collectives and lax.ppermute only.
A program may use at most 64 MiB of HBM per device.

v0:
```python
import math

import jax
import jax.numpy as jnp
from jax import lax
from jax.sharding import PartitionSpec as P

D = 4096
HEAD_DIM = 64
D_STATE = 128
TAPS = 4
SSM_WIDTH = 2048


EPS = 1e-06


def in_blocks(shard, dim, size):
    before, after = (shard.shape[:dim], shard.shape[dim + 1 :])
    return jnp.moveaxis(shard.reshape(*before, size, -1, *after), dim, 0)


def sent_and_summed(shard, axis, dim):
    size = lax.axis_size(axis)
    tiles = lax.all_to_all(in_blocks(shard, dim, size), axis, 0, 0, tiled=True)
    return jnp.sum(tiles, axis=0)


def sent_together(arrays, axis, dim, along):
    widths = [math.prod(a.shape[along:]) for a in arrays]
    both = jnp.concatenate(
        [a.reshape(*a.shape[:along], w) for a, w in zip(arrays, widths)], axis=along
    )
    whole = sent_and_summed(both, axis, dim)
    tiles = jnp.split(whole, [sum(widths[:k]) for k in range(1, len(widths))], axis=along)
    return tuple((b.reshape(*whole.shape[:along], *a.shape[along:]) for a, b in zip(arrays, tiles)))


def gathered_total(shard, axis):
    return lax.all_gather(shard, axis).sum(0)


def from_everyone(shard, axis):
    size = lax.axis_size(axis)
    return lax.all_to_all(
        jnp.broadcast_to(shard[None], (size, *shard.shape)), axis, 0, 0, tiled=True
    )


def joined_along(tiles, dim):
    dims = list(tiles.shape[1:])
    dims[dim] *= tiles.shape[0]
    return jnp.moveaxis(tiles, 0, dim).reshape(dims)


def gather_directly(shard, axis, dim):
    tiles = from_everyone(shard, axis)
    return joined_along(tiles, dim)


def in_one_piece(arrays, axis, dim, along):
    ends, at = ([], 0)
    for a in arrays[:-1]:
        at += a.shape[along]
        ends.append(at)
    both = jnp.concatenate(arrays, axis=along)
    return tuple(jnp.split(lax.all_gather(both, axis, axis=dim, tiled=True), ends, axis=along))


def of_everyone(shard, axis):
    everything = from_everyone(shard, axis)
    return jnp.sum(everything, axis=0)


def summed_on_arrival(shard, axis, dim):
    tiles = in_blocks(shard, dim, lax.axis_size(axis))
    arrived = lax.all_to_all(tiles, axis, split_axis=0, concat_axis=0, tiled=True)
    return arrived.astype(jnp.float32).sum(axis=0)


def stacked_from(shard, axes, order):
    tiles = shard[None]
    for k in order:
        tiles = lax.all_gather(tiles, axes[k], axis=0, tiled=True)
    current = [lax.axis_size(axes[k]) for k in reversed(order)]
    tiles = tiles.reshape(*current, *shard.shape)
    turned = sorted(range(len(order)), key=lambda place: order[len(order) - 1 - place])
    return tiles.transpose(*turned, *range(len(order), tiles.ndim)).reshape(-1, *shard.shape)


def gathered_by_axis(shard, axes, order, dim):
    return joined_along(stacked_from(shard, axes, order), dim)


def convolve(history, weights, newest):
    summed = weights[TAPS - 1] * newest
    for offset in range(TAPS - 1):
        summed = summed + weights[offset] * history[:, offset].astype(jnp.float32)
    return jax.nn.silu(summed)


def per_device(
    inputs,
    gain_in,
    w_gate,
    w_input,
    w_bproj,
    w_cproj,
    w_step,
    conv_input,
    conv_bproj,
    conv_cproj,
    tail_input,
    tail_bproj,
    tail_cproj,
    step_bias,
    decay_log,
    block_input,
    block_bproj,
    block_step,
    lengths,
    state,
    gain_mix,
    w_out,
    gain_mlp,
    w_up,
    w_down,
):
    stream = inputs.astype(jnp.float32)
    squares = jnp.sum(stream * stream, axis=1)
    scaled = (stream * gain_in).astype(jnp.bfloat16)
    matrices = (w_gate, w_input, w_bproj, w_cproj, w_step)
    pieces = [jnp.dot(scaled, weight, preferred_element_type=jnp.float32) for weight in matrices]
    projected, totals = sent_together((jnp.concatenate(pieces, axis=1), squares), "kv", 0, 1)
    inverse = lax.rsqrt(totals / D + EPS)[:, None]
    bounds = [0]
    for weight in matrices:
        bounds.append(bounds[-1] + weight.shape[1])
    gate_pre, value_pre, b_pre, c_pre, step_pre = [
        projected[:, bounds[member] : bounds[member + 1]] * inverse for member in range(5)
    ]
    seq_count = lengths.shape[0]
    head_count = step_bias.shape[0]
    group_count = w_bproj.shape[1] // D_STATE
    block_len = block_step.shape[1]
    per_group = head_count // group_count
    current = convolve(tail_input, conv_input, value_pre)
    b_now = convolve(tail_bproj, conv_bproj, b_pre)
    c_now = convolve(tail_cproj, conv_cproj, c_pre)
    step_size = jax.nn.softplus(step_pre + step_bias)
    decay_rate = -jnp.exp(decay_log)
    positions = lax.broadcasted_iota(jnp.int32, (1, block_len), 1)
    live_rows = (positions < lengths[:, None]).astype(jnp.float32)
    masked = block_step * live_rows[:, :, None]
    later_steps = jnp.sum(masked, axis=1, keepdims=True) - jnp.cumsum(masked, axis=1)
    decays = jnp.exp(decay_rate * (step_size[:, None, :] + later_steps)) * live_rows[:, :, None]
    c_query = c_now.astype(jnp.bfloat16).reshape(seq_count, group_count, D_STATE)
    keys = block_bproj.reshape(seq_count, block_len, group_count, D_STATE)
    scores = jnp.einsum("bsgn,bgn->bsg", keys, c_query, preferred_element_type=jnp.float32)
    scores = jnp.repeat(scores, per_group, axis=2)
    weights = (decays * scores * block_step).astype(jnp.bfloat16)
    values = block_input.reshape(seq_count, block_len, head_count, HEAD_DIM)
    inner_sum = jnp.einsum("bsh,bshp->bhp", weights, values, preferred_element_type=jnp.float32)
    c_full = c_now.reshape(seq_count, group_count, D_STATE)
    b_full = b_now.reshape(seq_count, group_count, D_STATE)
    own_score = jnp.repeat(jnp.sum(c_full * b_full, axis=2), per_group, axis=1)
    own_term = (step_size * own_score)[:, :, None] * current.reshape(
        seq_count, head_count, HEAD_DIM
    )
    carried = jnp.exp(decay_rate * (step_size + jnp.sum(masked, axis=1)))
    c_heads = jnp.repeat(c_full, per_group, axis=1)
    readout = jnp.einsum("bhpn,bhn->bhp", state, c_heads, precision=lax.Precision.HIGHEST)
    mixed = (inner_sum + own_term + carried[:, :, None] * readout).reshape(
        seq_count, -1
    ) * jax.nn.silu(gate_pre)
    local_sq = jnp.sum(mixed * mixed, axis=1)
    total_sq = gathered_total(local_sq, "tp")
    normed = (mixed * lax.rsqrt(total_sq / SSM_WIDTH + EPS)[:, None] * gain_mix).astype(
        jnp.bfloat16
    )
    products = jnp.dot(gather_directly(normed, "kv", 0), w_out, preferred_element_type=jnp.float32)
    mixed_in = sent_and_summed(products, "tp", 1)
    column_count = mixed_in.shape[1]
    residual = lax.dynamic_slice_in_dim(
        stream, lax.axis_index("tp") * column_count, column_count, 1
    )
    hidden = (residual + mixed_in).astype(jnp.bfloat16)
    lifted = (hidden.astype(jnp.float32) * gain_mlp).astype(jnp.bfloat16)
    all_lifted, all_hidden = in_one_piece((lifted, hidden), "dp", 0, 1)
    whole_rows = all_hidden.astype(jnp.float32)
    row_sq = jnp.sum(whole_rows * whole_rows, axis=1)
    partial_value = jnp.dot(all_lifted, w_up, preferred_element_type=jnp.float32)
    sq_sum = of_everyone(row_sq, ("kv", "tp"))
    shares = summed_on_arrival(partial_value.astype(jnp.bfloat16), ("kv", "tp"), 1)
    unit_share = jnp.square(jax.nn.relu(shares * lax.rsqrt(sq_sum / D + EPS)[:, None])).astype(
        jnp.bfloat16
    )
    hidden_units = gathered_by_axis(unit_share, ("kv", "tp"), (0, 1), 1)
    lowered = sent_and_summed(
        jnp.dot(hidden_units, w_down, preferred_element_type=jnp.float32), "dp", 0
    )
    return (hidden.astype(jnp.float32) + lowered).astype(jnp.bfloat16)


def solution(mesh):
    return jax.shard_map(
        per_device,
        mesh=mesh,
        in_specs=(
            P(("grp", "dp"), "kv"),
            P("kv"),
            P("kv", "tp"),
            P("kv", "tp"),
            P("kv", "tp"),
            P("kv", "tp"),
            P("kv", "tp"),
            P(None, "tp"),
            P(None, "tp"),
            P(None, "tp"),
            P(("grp", "dp", "kv"), None, "tp"),
            P(("grp", "dp", "kv"), None, "tp"),
            P(("grp", "dp", "kv"), None, "tp"),
            P("tp"),
            P("tp"),
            P(("grp", "dp", "kv"), None, "tp"),
            P(("grp", "dp", "kv"), None, "tp"),
            P(("grp", "dp", "kv"), None, "tp"),
            P(("grp", "dp", "kv")),
            P(("grp", "dp", "kv"), "tp", None, None),
            P("tp"),
            P("tp", "kv"),
            P(("kv", "tp")),
            P(("kv", "tp"), "dp"),
            P("dp", ("kv", "tp")),
        ),
        out_specs=P(("grp", "dp"), ("kv", "tp")),
        check_vma=False,
    )
```

profile of v0, /device:TPU:65, one launch (start us, length us, event | category | flops | bytes accessed | tf_op | source)
XLA Modules:
  0.0 298.7 jit_solution(5687502616347760678)
XLA Ops:
  6.6 0.9 multiply_reduce_fusion.1
  7.5 0.1 concatenate.27
  7.6 0.9 fusion.14
  8.5 1.1 fusion.16
  9.7 1.2 fusion.15
  10.9 1.3 fusion.18
  12.3 0.9 fusion.17
  13.4 1.2 concatenate.25
  14.6 44.4 %all-to-all-start = ((f32[16,2,3089]{2,1,0:T(2,128)}), f32[16,2,3089]{2,1,0:T(2,128)S(1)}, u32[]{:S(2)}, u32[]{:S(2)}) async-start(f32[16,2,3089]{2,1,0:T(2,128)} %concatenate.25), calls=%async_computation | async-start | bytes 819200 | tf_op jit(solution)/shard_map/all_to_all | solution.py:25
  59.1 0.2 copy.88
  59.3 1.0 copy.74
  60.3 1.3 dynamic-slice
  62.3 0.1 fusion.33
  62.4 0.2 reduce_window_sum.11
  62.7 15.6 %all-to-all-done = f32[16,2,3089]{2,1,0:T(2,128)S(1)} async-done(((f32[16,2,3089]{2,1,0:T(2,128)}), f32[16,2,3089]{2,1,0:T(2,128)S(1)}, u32[]{:S(2)}, u32[]{:S(2)}) %all-to-all-start) | async-done | bytes 395424 | tf_op jit(solution)/shard_map/all_to_all | solution.py:25
  78.3 0.1 reduce_sum.106
  78.5 0.2 fusion.30
  79.2 0.2 fusion.38
  79.6 0.1 fusion.2
  79.9 1.7 fusion.40
  81.6 1.4 fusion.39
  83.2 0.2 multiply_reduce_fusion.2
  83.4 0.2 dynamic-update-slice
  83.7 8.0 %all-reduce = f32[4]{0:T(128)S(1)} all-reduce(f32[4]{0:T(128)S(1)} %dynamic-update-slice), channel_id=2, replica_groups=mesh['grp'=2,'dp'=8,'kv'=16,'tp'=2] {'tp'}, use_global_device_ids=true, to_apply=%add | all-reduce | flops 4 | bytes 32
  91.8 0.7 broadcast_in_dim.13
  92.5 6.0 %all-to-all-start.1 = ((bf16[16,2,1024]{2,1,0:T(2,128)(2,1)}), bf16[16,2,1024]{2,1,0:T(2,128)(2,1)S(1)}, u32[]{:S(2)}, u32[]{:S(2)}) async-start(bf16[16,2,1024]{2,1,0:T(2,128)(2,1)} %broadcast_in_dim.13), calls=%async_computation.1 | async-start | bytes 131072 | tf_op jit(solution)/shard_map/all_to_all | solution.py:45
  98.5 0.2 copy.89
  98.7 11.2 %all-to-all-done.1 = bf16[16,2,1024]{2,1,0:T(2,128)(2,1)S(1)} async-done(((bf16[16,2,1024]{2,1,0:T(2,128)(2,1)}), bf16[16,2,1024]{2,1,0:T(2,128)(2,1)S(1)}, u32[]{:S(2)}, u32[]{:S(2)}) %all-to-all-start.1) | async-done | bytes 65568 | tf_op jit(solution)/shard_map/all_to_all | solution.py:45
  110.0 0.2 convolution_bitcast_fusion
  110.2 5.5 %all_to_all.31 = f32[2,32,128]{2,1,0:T(8,128)S(1)} all-to-all(f32[2,32,128]{2,1,0:T(8,128)S(1)} %convolution_bitcast_fusion), channel_id=1, replica_groups=mesh['grp'=2,'dp'=8,'kv'=16,'tp'=2] {'tp'}, dimensions={0} | all-to-all | bytes 65536 | tf_op jit(solution)/shard_map/all_to_all | solution.py:25
  115.7 20.2 %all_gather.17 = bf16[256,256]{1,0:T(8,128)(2,1)S(1)} all-gather(bf16[32,256]{1,0:T(8,128)(2,1)S(1)} %pad_maximum_fusion), channel_id=1, replica_groups=mesh['grp'=2,'dp'=8,'kv'=16,'tp'=2] {'dp'}, dimensions={0}, use_global_device_ids=true | all-gather | bytes 147456 | tf_op jit(solution)/shard_map/all_gather | solution.py:67
  135.9 0.1 multiply_reduce_fusion
  136.0 0.6 broadcast_in_dim.14
  136.6 10.4 %all-to-all-start.4 = ((f32[32,1,256]{2,1,0:T(1,128)}), f32[32,1,256]{2,1,0:T(1,128)S(1)}, u32[]{:S(2)}, u32[]{:S(2)}) async-start(f32[32,1,256]{2,1,0:T(1,128)} %broadcast_in_dim.14), calls=%async_computation.4 | async-start | bytes 65536 | tf_op jit(solution)/shard_map/all_to_all | solution.py:45
  147.1 0.4 convolution_convert_fusion
  147.5 1.3 copy.76
  148.8 10.4 %all-to-all-done.4 = f32[32,1,256]{2,1,0:T(1,128)S(1)} async-done(((f32[32,1,256]{2,1,0:T(1,128)}), f32[32,1,256]{2,1,0:T(1,128)S(1)}, u32[]{:S(2)}, u32[]{:S(2)}) %all-to-all-start.4) | async-done | bytes 32800 | tf_op jit(solution)/shard_map/all_to_all | solution.py:45
  159.2 4.8 %all-to-all-start.3 = ((bf16[32,256,64]{1,2,0:T(8,128)(2,1)}), bf16[32,256,64]{1,2,0:T(8,128)(2,1)S(1)}, u32[]{:S(2)}, u32[]{:S(2)}) async-start(bf16[32,256,64]{1,2,0:T(8,128)(2,1)} %bitcast.41), calls=%async_computation.3 | async-start | bytes 2097152 | tf_op jit(solution)/shard_map/all_to_all | solution.py:77
  164.2 55.5 %all-to-all-done.3 = bf16[32,256,64]{1,2,0:T(8,128)(2,1)S(1)} async-done(((bf16[32,256,64]{1,2,0:T(8,128)(2,1)}), bf16[32,256,64]{1,2,0:T(8,128)(2,1)S(1)}, u32[]{:S(2)}, u32[]{:S(2)}) %all-to-all-start.3) | async-done | bytes 1048608 | tf_op jit(solution)/shard_map/all_to_all | solution.py:77
  219.7 0.2 convert_reduce_fusion
  219.8 24.8 %all_gather.18 = bf16[16,256,64]{1,2,0:T(8,128)(2,1)} all-gather(bf16[1,256,64]{1,2,0:T(8,128)(2,1)S(1)} %fusion.6), channel_id=1, replica_groups=mesh['grp'=2,'dp'=8,'kv'=16,'tp'=2] {'kv'}, dimensions={0}, use_global_device_ids=true | all-gather | bytes 557056 | tf_op jit(solution)/shard_map/all_gather | solution.py:84
  244.7 23.7 %all-gather.3.cloned.1.call-done = bf16[32,256,64]{1,2,0:T(8,128)(2,1)} async-done(((bf16[16,256,64]{1,2,0:T(8,128)(2,1)}), bf16[32,256,64]{1,2,0:T(8,128)(2,1)}) %all-gather.3.cloned.1.call-update) | async-done | bytes 1048592 | tf_op jit(solution)/shard_map/all_gather | solution.py:84
  268.5 2.4 copy.78
  270.8 3.9 %copy.79 = bf16[256,32,64]{2,1,0:T(8,128)(2,1)S(1)} copy(bf16[256,32,64]{0,2,1:T(8,128)(2,1)} %bitcast.101) | data formatting | bytes 2097152 | tf_op jit(solution)/shard_map/transpose | solution.py:53
  274.7 2.4 dot_general.51
  277.2 1.8 fusion
  279.0 12.3 %all_to_all.32 = f32[8,32,128]{2,1,0:T(8,128)S(1)} all-to-all(f32[8,32,128]{2,1,0:T(8,128)S(1)} %fusion), channel_id=1, replica_groups=mesh['grp'=2,'dp'=8,'kv'=16,'tp'=2] {'dp'}, dimensions={0} | all-to-all | bytes 262144 | tf_op jit(solution)/shard_map/all_to_all | solution.py:25
  291.3 0.6 fusion.8
  (81 shorter events, 2.0 us)
Async XLA Ops:
  6.5 73.3 %copy-start = (f32[2,16,64,128]{3,2,1,0:T(8,128)S(1)}, f32[2,16,64,128]{3,2,1,0:T(8,128)}, u32[]{:S(2)}) copy-start(f32[2,16,64,128]{3,2,1,0:T(8,128)} %param.44) | copy-start | bytes 3145732
  6.6 5.8 %copy-start.3 = (bf16[256,1024]{1,0:T(8,128)(2,1)S(1)}, bf16[256,1024]{1,0:T(8,128)(2,1)}, u32[]{:S(2)}) copy-start(bf16[256,1024]{1,0:T(8,128)(2,1)} %param.28) | copy-start | bytes 1572868
  9.6 49.4 %copy-start.7 = (f32[2,128,16]{1,2,0:T(8,128)S(1)}, f32[2,128,16]{1,2,0:T(8,128)}, u32[]{:S(2)}) copy-start(f32[2,128,16]{1,2,0:T(8,128)} %param.42) | copy-start | bytes 49156
  9.7 49.4 %copy-start.6 = (bf16[2,128,512]{2,1,0:T(8,128)(2,1)S(1)}, bf16[2,128,512]{2,1,0:T(8,128)(2,1)}, u32[]{:S(2)}) copy-start(bf16[2,128,512]{2,1,0:T(8,128)(2,1)} %param.41) | copy-start | bytes 786436
  10.9 48.4 %copy-start.4 = (bf16[2,128,1024]{2,1,0:T(8,128)(2,1)S(1)}, bf16[2,128,1024]{2,1,0:T(8,128)(2,1)}, u32[]{:S(2)}) copy-start(bf16[2,128,1024]{2,1,0:T(8,128)(2,1)} %param.40) | copy-start | bytes 1572868
  12.3 49.9 %copy-start.17 = (s32[2]{0:T(128)S(1)}, s32[2]{0:T(128)}, u32[]{:S(2)}) copy-start(s32[2]{0:T(128)} %param.43) | copy-start | bytes 28
  13.3 49.3 %copy-start.18 = (f32[16]{0:T(128)S(1)}, f32[16]{0:T(128)}, u32[]{:S(2)}) copy-start(f32[16]{0:T(128)} %param.39) | copy-start | bytes 196
  13.3 49.3 %copy-start.10 = (f32[4,512]{1,0:T(4,128)S(1)}, f32[4,512]{1,0:T(4,128)}, u32[]{:S(2)}) copy-start(f32[4,512]{1,0:T(4,128)} %param.33) | copy-start | bytes 24580
  13.3 49.3 %copy-start.11 = (f32[4,512]{1,0:T(4,128)S(1)}, f32[4,512]{1,0:T(4,128)}, u32[]{:S(2)}) copy-start(f32[4,512]{1,0:T(4,128)} %param.34) | copy-start | bytes 24580
  13.3 49.3 %copy-start.8 = (f32[4,1024]{1,0:T(4,128)S(1)}, f32[4,1024]{1,0:T(4,128)}, u32[]{:S(2)}) copy-start(f32[4,1024]{1,0:T(4,128)} %param.32) | copy-start | bytes 49156
  13.4 65.2 %copy-start.12 = (bf16[2,3,512]{2,0,1:T(2,128)(2,1)S(1)}, bf16[2,3,512]{2,0,1:T(2,128)(2,1)}, u32[]{:S(2)}) copy-start(bf16[2,3,512]{2,0,1:T(2,128)(2,1)} %param.37) | copy-start | bytes 18436
  13.4 65.2 %copy-start.13 = (bf16[2,3,512]{2,0,1:T(2,128)(2,1)S(1)}, bf16[2,3,512]{2,0,1:T(2,128)(2,1)}, u32[]{:S(2)}) copy-start(bf16[2,3,512]{2,0,1:T(2,128)(2,1)} %param.36) | copy-start | bytes 18436
  13.4 65.6 %copy-start.9 = (bf16[2,3,1024]{2,0,1:T(2,128)(2,1)S(1)}, bf16[2,3,1024]{2,0,1:T(2,128)(2,1)}, u32[]{:S(2)}) copy-start(bf16[2,3,1024]{2,0,1:T(2,128)(2,1)} %param.35) | copy-start | bytes 36868
  14.6 64.9 %copy-start.16 = (f32[16]{0:T(128)S(1)}, f32[16]{0:T(128)}, u32[]{:S(2)}) copy-start(f32[16]{0:T(128)} %param.38) | copy-start | bytes 196
  14.6 63.7 %all-to-all-start = ((f32[16,2,3089]{2,1,0:T(2,128)}), f32[16,2,3089]{2,1,0:T(2,128)S(1)}, u32[]{:S(2)}, u32[]{:S(2)}) async-start(f32[16,2,3089]{2,1,0:T(2,128)} %concatenate.25), calls=%async_computation | async-start | bytes 819200 | tf_op jit(solution)/shard_map/all_to_all | solution.py:25
  60.3 31.5 %copy-start.14 = (f32[1024]{0:T(1024)S(1)}, f32[1024]{0:T(1024)}, u32[]{:S(2)}) copy-start(f32[1024]{0:T(1024)} %param.45) | copy-start | bytes 12292
  62.3 36.2 %copy-start.1 = (bf16[32,256]{1,0:T(8,128)(2,1)S(1)}, bf16[32,256]{1,0:T(8,128)(2,1)}, u32[]{:S(2)}) copy-start(bf16[32,256]{1,0:T(8,128)(2,1)} %param.25) | copy-start | bytes 49156
  62.4 36.1 %copy-start.5 = (bf16[1024,256]{1,0:T(8,128)(2,1)S(1)}, bf16[1024,256]{1,0:T(8,128)(2,1)}, u32[]{:S(2)}) copy-start(bf16[1024,256]{1,0:T(8,128)(2,1)} %param.46) | copy-start | bytes 1572868
  79.8 35.9 %copy-start.15 = (f32[128]{0:T(128)S(1)}, f32[128]{0:T(128)}, u32[]{:S(2)}) copy-start(f32[128]{0:T(128)} %param.47) | copy-start | bytes 1540
  79.9 67.2 %copy-start.2 = (bf16[128,2048]{1,0:T(8,128)(2,1)S(1)}, bf16[128,2048]{1,0:T(8,128)(2,1)}, u32[]{:S(2)}) copy-start(bf16[128,2048]{1,0:T(8,128)(2,1)} %param.48) | copy-start | bytes 1572868
  92.5 17.4 %all-to-all-start.1 = ((bf16[16,2,1024]{2,1,0:T(2,128)(2,1)}), bf16[16,2,1024]{2,1,0:T(2,128)(2,1)S(1)}, u32[]{:S(2)}, u32[]{:S(2)}) async-start(bf16[16,2,1024]{2,1,0:T(2,128)(2,1)} %broadcast_in_dim.13), calls=%async_computation.1 | async-start | bytes 131072 | tf_op jit(solution)/shard_map/all_to_all | solution.py:45
  136.6 22.6 %all-to-all-start.4 = ((f32[32,1,256]{2,1,0:T(1,128)}), f32[32,1,256]{2,1,0:T(1,128)S(1)}, u32[]{:S(2)}, u32[]{:S(2)}) async-start(f32[32,1,256]{2,1,0:T(1,128)} %broadcast_in_dim.14), calls=%async_computation.4 | async-start | bytes 65536 | tf_op jit(solution)/shard_map/all_to_all | solution.py:45
  159.2 60.5 %all-to-all-start.3 = ((bf16[32,256,64]{1,2,0:T(8,128)(2,1)}), bf16[32,256,64]{1,2,0:T(8,128)(2,1)S(1)}, u32[]{:S(2)}, u32[]{:S(2)}) async-start(bf16[32,256,64]{1,2,0:T(8,128)(2,1)} %bitcast.41), calls=%async_computation.3 | async-start | bytes 2097152 | tf_op jit(solution)/shard_map/all_to_all | solution.py:77
  164.1 104.4 %all-gather.3.cloned.1.call-start = ((), (), s32[]{:S(2)}) async-start(), calls=%async_computation.6 | async-start | bytes 1572864 | tf_op jit(solution)/shard_map/all_gather | solution.py:84
Sparse Core Ops, SparseCore 0:
  244.8 23.5 all-gather.2
where the time goes:
time: 300 us; the launch traced here: 299 us
  waiting for transfers between devices  117 us (39%)
  blocking collectives  70.7 us (24%)
  starting transfers between devices  65.6 us (22%)
  local copies, waits for them, and re-layouts  16.7 us (6%)
  between operations  14.5 us (5%)
  matrix products  11.2 us (4%)
  other arithmetic  3.49 us (1%)
    all_to_all x1, waiting for transfers between devices, summed_on_arrival(): lax.all_to_all(tiles, axis, split_axis=0, concat_axis=0, tiled=True)  55.5 us
    all_to_all x1, starting transfers between devices, sent_and_summed(): tiles = lax.all_to_all(in_blocks(shard, dim, size), axis, 0, 0, tiled=True)  44.4 us
    all_gather x1, blocking collectives, stacked_from(): tiles = lax.all_gather(tiles, axes[k], axis=0, tiled=True)  24.8 us
    all_gather x1, waiting for transfers between devices, stacked_from(): tiles = lax.all_gather(tiles, axes[k], axis=0, tiled=True)  23.7 us
    all_to_all x2, waiting for transfers between devices, from_everyone(): lax.all_to_all(jnp.broadcast_to(shard[None], (size, *shard.shape)), axis,...  21.6 us
    all_gather x1, blocking collectives, in_one_piece(): lax.all_gather(both, axis, axis=dim, tiled=True)  20.2 us
    all_to_all x2, blocking collectives, sent_and_summed(): tiles = lax.all_to_all(in_blocks(shard, dim, size), axis, 0, 0, tiled=True)  17.7 us
    all_to_all x2, starting transfers between devices, from_everyone(): lax.all_to_all(jnp.broadcast_to(shard[None], (size, *shard.shape)), axis,...  16.4 us
  transfers between devices with their start and end apart: 5, of which 5 were waited for; matrix products, arithmetic and copies ran while one was open for 2% of the time, Pallas kernels for 0%

commit v1 on v0

v1 whole, which is shorter than its diff:
```python
import jax
import jax.numpy as jnp
from jax import lax
from jax.sharding import PartitionSpec as P

D = 4096
HEAD_DIM = 64
D_STATE = 128
TAPS = 4
SSM_WIDTH = 2048
LANES = 128

EPS = 1e-06
BF16 = jnp.bfloat16
F32 = jnp.float32


def two_words(x):
    high = lax.reduce_precision(x, 8, 7)
    return high.astype(BF16), (x - high).astype(BF16)


def to_everyone(shard, axes):
    size = lax.axis_size(axes)
    return lax.all_to_all(
        jnp.broadcast_to(shard[None], (size, *shard.shape)), axes, 0, 0, tiled=True
    )


def from_partner(x):
    size = lax.axis_size("tp")
    return lax.ppermute(x, "tp", [(i, (i + 1) % size) for i in range(size)])


def exchanged(weight, dim, core):
    half = weight.shape[dim] // 2
    mine = lax.dynamic_slice_in_dim(weight, core * half, half, dim)
    other = lax.dynamic_slice_in_dim(weight, (1 - core) * half, half, dim)
    return mine, from_partner(other)


def in_core_order(mine, other, core, dim):
    return jnp.where(
        core == 0,
        jnp.concatenate([mine, other], axis=dim),
        jnp.concatenate([other, mine], axis=dim),
    )


def convolve(history, weights, newest):
    summed = weights[TAPS - 1] * newest
    for offset in range(TAPS - 1):
        summed = summed + weights[offset] * history[:, offset].astype(F32)
    return jax.nn.silu(summed)


def per_device(
    inputs,
    gain_in,
    w_gate,
    w_input,
    w_bproj,
    w_cproj,
    w_step,
    conv_input,
    conv_bproj,
    conv_cproj,
    tail_input,
    tail_bproj,
    tail_cproj,
    step_bias,
    decay_log,
    block_input,
    block_bproj,
    block_step,
    lengths,
    state,
    gain_mix,
    w_out,
    gain_mlp,
    w_up,
    w_down,
):
    core = lax.axis_index("tp")
    n_kv, n_dp, n_tp = lax.axis_size("kv"), lax.axis_size("dp"), lax.axis_size("tp")
    stream = inputs.astype(F32)
    rows = inputs.shape[0]
    squares = jnp.sum(stream * stream, axis=1)
    scaled = (stream * gain_in).astype(BF16)
    matrices = (w_gate, w_input, w_bproj, w_cproj)
    pieces = [jnp.dot(scaled, weight, preferred_element_type=F32).astype(BF16) for weight in matrices]
    pieces += two_words(jnp.dot(scaled, w_step, preferred_element_type=F32))
    pieces += two_words(squares[:, None])
    bounds = [0]
    for piece in pieces:
        bounds.append(bounds[-1] + piece.shape[1])
    spare = -bounds[-1] % LANES
    pieces.append(jnp.zeros((rows, spare), BF16))
    sent = jnp.concatenate(pieces, axis=1).reshape(n_kv, rows // n_kv, -1)
    arrived = lax.all_to_all(sent, "kv", 0, 0, tiled=True)
    projected = jnp.sum(arrived.astype(F32), axis=0)

    out_mine, out_other = exchanged(w_out, 1, core)
    up_mine, up_other = exchanged(w_up, 1, core)
    down_mine, down_other = exchanged(w_down, 0, core)
    gain_other = from_partner(gain_mlp)
    out_weight = jnp.concatenate([out_mine, out_other], axis=0)
    up_weight = jnp.concatenate([up_mine, up_other], axis=0)
    down_weight = in_core_order(down_mine, down_other, core, 1)
    up_gain = jnp.concatenate([gain_mlp, gain_other])

    parts = [projected[:, a:b] for a, b in zip(bounds[:-1], bounds[1:])]
    inverse = lax.rsqrt((parts[6] + parts[7]) / D + EPS)
    gate_pre, value_pre, b_pre, c_pre = [parts[k] * inverse for k in range(4)]
    step_pre = (parts[4] + parts[5]) * inverse
    seq_count = lengths.shape[0]
    head_count = step_bias.shape[0]
    group_count = w_bproj.shape[1] // D_STATE
    block_len = block_step.shape[1]
    per_group = head_count // group_count
    current = convolve(tail_input, conv_input, value_pre)
    b_now = convolve(tail_bproj, conv_bproj, b_pre)
    c_now = convolve(tail_cproj, conv_cproj, c_pre)
    step_size = jax.nn.softplus(step_pre + step_bias)
    decay_rate = -jnp.exp(decay_log)
    positions = lax.broadcasted_iota(jnp.int32, (1, block_len), 1)
    live_rows = (positions < lengths[:, None]).astype(F32)
    masked = block_step * live_rows[:, :, None]
    later_steps = jnp.sum(masked, axis=1, keepdims=True) - jnp.cumsum(masked, axis=1)
    decays = jnp.exp(decay_rate * (step_size[:, None, :] + later_steps)) * live_rows[:, :, None]
    c_query = c_now.astype(BF16).reshape(seq_count, group_count, D_STATE)
    keys = block_bproj.reshape(seq_count, block_len, group_count, D_STATE)
    scores = jnp.einsum("bsgn,bgn->bsg", keys, c_query, preferred_element_type=F32)
    scores = jnp.repeat(scores, per_group, axis=2)
    weights = (decays * scores * block_step).astype(BF16)
    values = block_input.reshape(seq_count, block_len, head_count, HEAD_DIM)
    inner_sum = jnp.einsum("bsh,bshp->bhp", weights, values, preferred_element_type=F32)
    c_full = c_now.reshape(seq_count, group_count, D_STATE)
    b_full = b_now.reshape(seq_count, group_count, D_STATE)
    own_score = jnp.repeat(jnp.sum(c_full * b_full, axis=2), per_group, axis=1)
    own_term = (step_size * own_score)[:, :, None] * current.reshape(
        seq_count, head_count, HEAD_DIM
    )
    carried = jnp.exp(decay_rate * (step_size + jnp.sum(masked, axis=1)))
    c_heads = jnp.repeat(c_full, per_group, axis=1)
    readout = jnp.einsum("bhpn,bhn->bhp", state, c_heads, precision=lax.Precision.HIGHEST)
    mixed = (inner_sum + own_term + carried[:, :, None] * readout).reshape(
        seq_count, -1
    ) * jax.nn.silu(gate_pre)

    width = mixed.shape[1]
    local_sq = two_words(jnp.sum(mixed * mixed, axis=1, keepdims=True))
    row = jnp.concatenate(
        [(mixed * gain_mix).astype(BF16), *local_sq, jnp.zeros((seq_count, LANES - 2), BF16)], axis=1
    )
    whole = to_everyone(row, ("kv", "tp")).reshape(n_kv, n_tp, seq_count, -1)
    whole = jnp.moveaxis(whole, 1, 0).reshape(n_tp, rows, -1)
    total_sq = jnp.sum(whole[:, :, width : width + 2].astype(F32), axis=(0, 2))
    halves = whole[:, :, :width]
    channels = jnp.concatenate(
        [
            lax.dynamic_index_in_dim(halves, core, 0, keepdims=False),
            lax.dynamic_index_in_dim(halves, 1 - core, 0, keepdims=False),
        ],
        axis=1,
    )
    mixed_in = jnp.dot(channels, out_weight, preferred_element_type=F32)
    mixed_in = mixed_in * lax.rsqrt(total_sq / SSM_WIDTH + EPS)[:, None]
    column_count = mixed_in.shape[1]
    residual = lax.dynamic_slice_in_dim(stream, core * column_count, column_count, 1)
    hidden = (residual + mixed_in).astype(BF16)

    all_hidden = to_everyone(hidden, ("dp", "tp")).reshape(n_dp, n_tp, rows, -1)
    all_hidden = jnp.moveaxis(all_hidden, 1, 0).reshape(n_tp, n_dp * rows, -1)
    all_hidden = jnp.concatenate(
        [
            lax.dynamic_index_in_dim(all_hidden, core, 0, keepdims=False),
            lax.dynamic_index_in_dim(all_hidden, 1 - core, 0, keepdims=False),
        ],
        axis=1,
    ).astype(F32)
    row_sq = jnp.sum(all_hidden * all_hidden, axis=1)
    lifted = (all_hidden * up_gain).astype(BF16)
    raised = lax.dot_general(
        up_weight, lifted, (((0,), (1,)), ((), ())), preferred_element_type=F32
    ).astype(BF16)
    seqs = raised.shape[1]
    extra = jnp.concatenate(
        [*[w[None] for w in two_words(row_sq)], jnp.zeros((6, seqs), BF16)], axis=0
    )
    sent = jnp.concatenate(
        [
            raised.reshape(n_kv, -1, seqs),
            jnp.broadcast_to(extra[None], (n_kv, *extra.shape)),
        ],
        axis=1,
    )
    arrived = lax.all_to_all(sent, "kv", 0, 0, tiled=True)
    shares = jnp.sum(arrived.astype(F32), axis=0)
    unit_count = shares.shape[0] - 8
    sq_sum = shares[unit_count] + shares[unit_count + 1]
    units = jnp.square(
        jax.nn.relu(shares[:unit_count] * lax.rsqrt(sq_sum / D + EPS)[None, :])
    ).astype(BF16)
    hidden_units = lax.all_gather(units, "kv", axis=0, tiled=True)
    lowered = lax.dot_general(
        hidden_units, down_weight, (((0,), (0,)), ((), ())), preferred_element_type=F32
    ).astype(BF16)
    lowered = lowered.reshape(n_dp, rows, n_tp, -1)
    lowered = jnp.moveaxis(lowered, 2, 1).reshape(n_dp * n_tp, rows, -1)
    lowered = lax.all_to_all(lowered, ("dp", "tp"), 0, 0, tiled=True)
    return (hidden.astype(F32) + jnp.sum(lowered.astype(F32), axis=0)).astype(BF16)


def solution(mesh):
    return jax.shard_map(
        per_device,
        mesh=mesh,
        in_specs=(
            P(("grp", "dp"), "kv"),
            P("kv"),
            P("kv", "tp"),
            P("kv", "tp"),
            P("kv", "tp"),
            P("kv", "tp"),
            P("kv", "tp"),
            P(None, "tp"),
            P(None, "tp"),
            P(None, "tp"),
            P(("grp", "dp", "kv"), None, "tp"),
            P(("grp", "dp", "kv"), None, "tp"),
            P(("grp", "dp", "kv"), None, "tp"),
            P("tp"),
            P("tp"),
            P(("grp", "dp", "kv"), None, "tp"),
            P(("grp", "dp", "kv"), None, "tp"),
            P(("grp", "dp", "kv"), None, "tp"),
            P(("grp", "dp", "kv")),
            P(("grp", "dp", "kv"), "tp", None, None),
            P("tp"),
            P("tp", "kv"),
            P(("kv", "tp")),
            P(("kv", "tp"), "dp"),
            P("dp", ("kv", "tp")),
        ),
        out_specs=P(("grp", "dp"), ("kv", "tp")),
        check_vma=False,
    )
```

time: 300 us -> 201 us (0.67)
  waiting for transfers between devices: 117 us -> 55.3 us
  blocking collectives: 70.7 us -> 49.5 us
  between operations: 14.5 us -> 0.67 us
  local copies, waits for them, and re-layouts: 16.7 us -> 5.53 us
  starting transfers between devices: 65.6 us -> 76.7 us
  matrix products: 11.2 us -> 7.82 us
    all_to_all x4, waiting for transfers between devices: 92.7 us -> 55.3 us  [the longest x2 37.3 us: per_device(): arrived = lax.all_to_all(sent, 'kv', 0, 0, tiled=True)]
    all_gather x1 -> x0, waiting for transfers between devices: 23.7 us -> none  [stacked_from(): tiles = lax.all_gather(tiles, axes[k], axis=0, tiled=True)]
    all_gather x2 -> x1, blocking collectives: 45 us -> 27.8 us  [per_device(): hidden_units = lax.all_gather(units, 'kv', axis=0, tiled=True)]
    ppermute x0 -> x4, starting transfers between devices: none -> 8.98 us  [from_partner(): return lax.ppermute(x, 'tp', [(i, (i + 1) % size) for i in range(size)])]
    unnamed x1 -> x0, blocking collectives: 7.96 us -> none
    transpose x2, local copies, waits for them, and re-layouts: 6.27 us -> 0.12 us  [the longest x1 0.11 us: per_device(): whole = jnp.moveaxis(whole, 1, 0).reshape(n_tp, rows, -1)]
    all_to_all x2 -> x1, blocking collectives: 17.7 us -> 21.7 us  [per_device(): lowered = lax.all_to_all(lowered, ('dp', 'tp'), 0, 0, tiled=True)]
    dot_general x10, matrix products: 9.45 us -> 6.09 us  [the longest x4 3.73 us: per_device(): jnp.dot(scaled, weight, preferred_element_type=F32).astype(BF16)]
  transfers between devices with their start and end apart: 5 -> 8, of which waited for: 5 -> 4; matrix products, arithmetic and copies ran while one was open for 2% -> 1% of each run, Pallas kernels for 0% -> 0%
where the time goes in v1:
time: 201 us; the launch traced here: 200 us
  starting transfers between devices  76.7 us (38%)
  waiting for transfers between devices  55.3 us (28%)
  blocking collectives  49.5 us (25%)
  matrix products  7.82 us (4%)
  local copies, waits for them, and re-layouts  5.53 us (3%)
  other arithmetic  4.62 us (2%)
    all_to_all x2, starting transfers between devices, per_device(): arrived = lax.all_to_all(sent, 'kv', 0, 0, tiled=True)  48.2 us
    all_to_all x2, waiting for transfers between devices, per_device(): arrived = lax.all_to_all(sent, 'kv', 0, 0, tiled=True)  37.3 us
    all_gather x1, blocking collectives, per_device(): hidden_units = lax.all_gather(units, 'kv', axis=0, tiled=True)  27.8 us
    all_to_all x1, blocking collectives, per_device(): lowered = lax.all_to_all(lowered, ('dp', 'tp'), 0, 0, tiled=True)  21.7 us
    all_to_all x2, starting transfers between devices, to_everyone(): lax.all_to_all(jnp.broadcast_to(shard[None], (size, *shard.shape)), axes,...  19.5 us
    all_to_all x2, waiting for transfers between devices, to_everyone(): lax.all_to_all(jnp.broadcast_to(shard[None], (size, *shard.shape)), axes,...  17.9 us
    ppermute x4, starting transfers between devices, from_partner(): return lax.ppermute(x, 'tp', [(i, (i + 1) % size) for i in range(size)])  8.98 us
  transfers between devices with their start and end apart: 8, of which 4 were waited for; matrix products, arithmetic and copies ran while one was open for 1% of the time, Pallas kernels for 0%

profile of v1, /device:TPU:65, one launch (start us, length us, event | category | flops | bytes accessed | tf_op | source)
XLA Modules:
  0.0 200.1 jit_solution(6419792693657834448)
XLA Ops:
  0.0 0.9 multiply_reduce_fusion
  1.1 0.1 copy.63
  1.3 0.1 copy.62
  1.4 0.9 fusion.26
  2.4 1.1 convolution_convert_fusion.5
  3.6 1.1 convolution_convert_fusion.4
  4.8 1.3 convolution_convert_fusion.3
  6.1 0.2 convolution_convert_fusion.2
  6.4 1.1 concatenate.52
  7.5 44.2 %all-to-all-start = ((bf16[16,2,3200]{2,1,0:T(2,128)(2,1)}), bf16[16,2,3200]{2,1,0:T(2,128)(2,1)S(1)}, u32[]{:S(2)}, u32[]{:S(2)}) async-start(bf16[16,2,3200]{2,1,0:T(2,128)(2,1)} %concatenate.52), calls=%async_computation | async-start | bytes 409600 | tf_op jit(solution)/shard_map/all_to_all | solution.py:100
  51.8 0.1 copy.64
  52.0 0.1 fusion.55
  52.1 0.2 copy.80
  52.3 0.3 copy.67
  52.6 0.2 reduce_window_sum.11
  52.9 11.0 %all-to-all-done = bf16[16,2,3200]{2,1,0:T(2,128)(2,1)S(1)} async-done(((bf16[16,2,3200]{2,1,0:T(2,128)(2,1)}), bf16[16,2,3200]{2,1,0:T(2,128)(2,1)S(1)}, u32[]{:S(2)}, u32[]{:S(2)}) %all-to-all-start) | async-done | bytes 204832 | tf_op jit(solution)/shard_map/all_to_all | solution.py:100
  63.9 0.2 convert_reduce_fusion.1
  64.1 0.2 fusion.49
  64.9 0.2 fusion.60
  65.1 0.1 copy.65
  65.3 0.1 fusion.21
  65.5 1.7 fusion.62
  67.3 0.4 fusion.61
  67.8 0.2 multiply_reduce_fusion.1
  68.2 0.1 concatenate.53
  68.3 0.8 broadcast_in_dim.23
  69.0 10.6 %all-to-all-start.1 = ((bf16[32,2,1152]{2,1,0:T(2,128)(2,1)}), bf16[32,2,1152]{2,1,0:T(2,128)(2,1)S(1)}, u32[]{:S(2)}, u32[]{:S(2)}) async-start(bf16[32,2,1152]{2,1,0:T(2,128)(2,1)} %broadcast_in_dim.23), calls=%async_computation.1 | async-start | bytes 294912 | tf_op jit(solution)/shard_map/all_to_all | solution.py:25
  79.7 2.6 %collective-permute-start = (bf16[1024,128]{1,0:T(8,128)(2,1)S(1)}, bf16[1024,128]{1,0:T(8,128)(2,1)S(1)}, u32[]{:S(2)}, u32[]{:S(2)}) collective-permute-start(bf16[1024,128]{1,0:T(8,128)(2,1)S(1)} %get-tuple-element.18), channel_id=1, source_target_pairs={{0,1},{1,0},{2,3},{3,2},{4,5},{5,4},{6,7},{7,6},{8,9},{9,8},{10,11... | collective-permute-start | bytes 786440 | tf_op jit(solution)/shard_map/ppermute | solution.py:32
  82.3 13.6 %all-to-all-done.1 = bf16[32,2,1152]{2,1,0:T(2,128)(2,1)S(1)} async-done(((bf16[32,2,1152]{2,1,0:T(2,128)(2,1)}), bf16[32,2,1152]{2,1,0:T(2,128)(2,1)S(1)}, u32[]{:S(2)}, u32[]{:S(2)}) %all-to-all-start.1) | async-done | bytes 147488 | tf_op jit(solution)/shard_map/all_to_all | solution.py:25
  95.9 0.1 copy.70
  96.0 0.3 convert_reduce_fusion.3
  96.5 0.3 constant_dynamic-slice_fusion.7
  96.8 0.2 fusion.1
  97.1 0.7 broadcast_in_dim.24
  97.7 8.9 %all-to-all-start.2 = ((bf16[16,32,128]{2,1,0:T(8,128)(2,1)}), bf16[16,32,128]{2,1,0:T(8,128)(2,1)S(1)}, u32[]{:S(2)}, u32[]{:S(2)}) async-start(bf16[16,32,128]{2,1,0:T(8,128)(2,1)} %broadcast_in_dim.24), calls=%async_computation.2 | async-start | bytes 262144 | tf_op jit(solution)/shard_map/all_to_all | solution.py:25
  106.6 2.2 %collective-permute-start.2 = (f32[128]{0:T(128)S(1)}, f32[128]{0:T(128)S(1)}, u32[]{:S(2)}, u32[]{:S(2)}) collective-permute-start(f32[128]{0:T(128)S(1)} %copy-done.18), channel_id=1, source_target_pairs={{0,1},{1,0},{2,3},{3,2},{4,5},{5,4},{6,7},{7,6},{8,9},{9,8},{10,11... | collective-permute-start | bytes 1544 | tf_op jit(solution)/shard_map/ppermute | solution.py:32
  109.0 2.1 %collective-permute-start.1 = (bf16[128,1024]{1,0:T(8,128)(2,1)S(1)}, bf16[128,1024]{1,0:T(8,128)(2,1)S(1)}, u32[]{:S(2)}, u32[]{:S(2)}) collective-permute-start(bf16[128,1024]{1,0:T(8,128)(2,1)S(1)} %get-tuple-element.16), channel_id=1, source_target_pairs={{0,1},{1,0},{2,3},{3,2},{4,5},{5,4},{6,7},{7,6},{8,9},{9,8},{10,11... | collective-permute-start | bytes 786440 | tf_op jit(solution)/shard_map/ppermute | solution.py:32
  111.2 4.3 %all-to-all-done.2 = bf16[16,32,128]{2,1,0:T(8,128)(2,1)S(1)} async-done(((bf16[16,32,128]{2,1,0:T(8,128)(2,1)}), bf16[16,32,128]{2,1,0:T(8,128)(2,1)S(1)}, u32[]{:S(2)}, u32[]{:S(2)}) %all-to-all-start.2) | async-done | bytes 131104 | tf_op jit(solution)/shard_map/all_to_all | solution.py:25
  115.6 0.1 fusion.15
  115.8 0.4 convolution_convert_fusion
  116.2 0.9 pad_maximum_fusion
  117.0 4.0 %all-to-all-start.3 = ((bf16[16,72,256]{2,1,0:T(8,128)(2,1)}), bf16[16,72,256]{2,1,0:T(8,128)(2,1)S(1)}, u32[]{:S(2)}, u32[]{:S(2)}) async-start(bf16[16,72,256]{2,1,0:T(8,128)(2,1)} %pad_maximum_fusion), calls=%async_computation.3 | async-start | bytes 1179648 | tf_op jit(solution)/shard_map/all_to_all | solution.py:198
  121.1 2.0 collective-permute-start.3
  123.1 26.3 %all-to-all-done.3 = bf16[16,72,256]{2,1,0:T(8,128)(2,1)S(1)} async-done(((bf16[16,72,256]{2,1,0:T(8,128)(2,1)}), bf16[16,72,256]{2,1,0:T(8,128)(2,1)S(1)}, u32[]{:S(2)}, u32[]{:S(2)}) %all-to-all-start.3) | async-done | bytes 589856 | tf_op jit(solution)/shard_map/all_to_all | solution.py:198
  149.5 27.8 %all_gather.3 = bf16[1024,256]{1,0:T(8,128)(2,1)S(1)} all-gather(bf16[64,256]{1,0:T(8,128)(2,1)S(1)} %fusion.24), channel_id=1, replica_groups=mesh['grp'=2,'dp'=8,'kv'=16,'tp'=2] {'kv'}, dimensions={0}, use_global_device_ids=true | all-gather | bytes 557056 | tf_op jit(solution)/shard_map/all_gather | solution.py:205
  177.3 0.4 convolution_convert_fusion.1
  177.7 21.7 %all_to_all.25 = bf16[16,32,128]{2,1,0:T(8,128)(2,1)S(1)} all-to-all(bf16[16,32,128]{2,1,0:T(8,128)(2,1)S(1)} %bitcast.105), channel_id=1, replica_groups=mesh['grp'=2,'dp'=8,'kv'=16,'tp'=2] {'dp','tp'}, dimensions={0} | all-to-all | bytes 262144 | tf_op jit(solution)/shard_map/all_to_all | solution.py:211
  199.5 0.6 add_convert_fusion
  (102 shorter events, 2.4 us)
Async XLA Ops:
  0.0 65.5 %copy-start = (f32[2,16,64,128]{3,2,1,0:T(8,128)S(1)}, f32[2,16,64,128]{3,2,1,0:T(8,128)}, u32[]{:S(2)}) copy-start(f32[2,16,64,128]{3,2,1,0:T(8,128)} %param.44) | copy-start | bytes 3145732
  0.0 6.1 %copy-start.1 = (bf16[32,256]{1,0:T(8,128)(2,1)S(1)}, bf16[32,256]{1,0:T(8,128)(2,1)}, u32[]{:S(2)}) copy-start(bf16[32,256]{1,0:T(8,128)(2,1)} %param.25) | copy-start | bytes 49156
  0.0 6.1 %copy-start.8 = (f32[256]{0:T(256)S(1)}, f32[256]{0:T(256)}, u32[]{:S(2)}) copy-start(f32[256]{0:T(256)} %param.26) | copy-start | bytes 3076
  0.0 6.1 %copy-start.5 = (bf16[256,1024]{1,0:T(8,128)(2,1)S(1)}, bf16[256,1024]{1,0:T(8,128)(2,1)}, u32[]{:S(2)}) copy-start(bf16[256,1024]{1,0:T(8,128)(2,1)} %param.28) | copy-start | bytes 1572868
  4.7 47.0 %copy-start.19 = (s32[2]{0:T(128)S(1)}, s32[2]{0:T(128)}, u32[]{:S(2)}) copy-start(s32[2]{0:T(128)} %param.43) | copy-start | bytes 28
  4.8 47.1 %copy-start.9 = (f32[2,128,16]{1,2,0:T(8,128)S(1)}, f32[2,128,16]{1,2,0:T(8,128)}, u32[]{:S(2)}) copy-start(f32[2,128,16]{1,2,0:T(8,128)} %param.42) | copy-start | bytes 49156
  6.0 46.0 %copy-start.20 = (f32[16]{0:T(128)S(1)}, f32[16]{0:T(128)}, u32[]{:S(2)}) copy-start(f32[16]{0:T(128)} %param.39) | copy-start | bytes 196
  6.1 46.0 %copy-start.7 = (bf16[2,128,512]{2,1,0:T(8,128)(2,1)S(1)}, bf16[2,128,512]{2,1,0:T(8,128)(2,1)}, u32[]{:S(2)}) copy-start(bf16[2,128,512]{2,1,0:T(8,128)(2,1)} %param.41) | copy-start | bytes 786436
  6.3 46.0 %copy-start.6 = (bf16[2,128,1024]{2,1,0:T(8,128)(2,1)S(1)}, bf16[2,128,1024]{2,1,0:T(8,128)(2,1)}, u32[]{:S(2)}) copy-start(bf16[2,128,1024]{2,1,0:T(8,128)(2,1)} %param.40) | copy-start | bytes 1572868
  7.5 56.4 %all-to-all-start = ((bf16[16,2,3200]{2,1,0:T(2,128)(2,1)}), bf16[16,2,3200]{2,1,0:T(2,128)(2,1)S(1)}, u32[]{:S(2)}, u32[]{:S(2)}) async-start(bf16[16,2,3200]{2,1,0:T(2,128)(2,1)} %concatenate.52), calls=%async_computation | async-start | bytes 409600 | tf_op jit(solution)/shard_map/all_to_all | solution.py:100
  51.9 0.9 copy-start.12
  51.9 0.9 copy-start.13
  52.0 0.9 copy-start.10
  52.1 12.2 %copy-start.14 = (bf16[2,3,512]{2,0,1:T(2,128)(2,1)S(1)}, bf16[2,3,512]{2,0,1:T(2,128)(2,1)}, u32[]{:S(2)}) copy-start(bf16[2,3,512]{2,0,1:T(2,128)(2,1)} %param.37) | copy-start | bytes 18436
  52.1 12.2 %copy-start.15 = (bf16[2,3,512]{2,0,1:T(2,128)(2,1)S(1)}, bf16[2,3,512]{2,0,1:T(2,128)(2,1)}, u32[]{:S(2)}) copy-start(bf16[2,3,512]{2,0,1:T(2,128)(2,1)} %param.36) | copy-start | bytes 18436
  52.1 12.6 %copy-start.11 = (bf16[2,3,1024]{2,0,1:T(2,128)(2,1)S(1)}, bf16[2,3,1024]{2,0,1:T(2,128)(2,1)}, u32[]{:S(2)}) copy-start(bf16[2,3,1024]{2,0,1:T(2,128)(2,1)} %param.35) | copy-start | bytes 36868
  52.3 12.8 %copy-start.17 = (f32[16]{0:T(128)S(1)}, f32[16]{0:T(128)}, u32[]{:S(2)}) copy-start(f32[16]{0:T(128)} %param.38) | copy-start | bytes 196
  65.4 2.7 %copy-start.16 = (f32[1024]{0:T(1024)S(1)}, f32[1024]{0:T(1024)}, u32[]{:S(2)}) copy-start(f32[1024]{0:T(1024)} %param.45) | copy-start | bytes 12292
  65.5 14.1 %copy-start.2 = (bf16[1024,256]{1,0:T(8,128)(2,1)S(1)}, bf16[1024,256]{1,0:T(8,128)(2,1)}, u32[]{:S(2)}) copy-start(bf16[1024,256]{1,0:T(8,128)(2,1)} %param.46) | copy-start | bytes 1572868
  69.0 26.9 %all-to-all-start.1 = ((bf16[32,2,1152]{2,1,0:T(2,128)(2,1)}), bf16[32,2,1152]{2,1,0:T(2,128)(2,1)S(1)}, u32[]{:S(2)}, u32[]{:S(2)}) async-start(bf16[32,2,1152]{2,1,0:T(2,128)(2,1)} %broadcast_in_dim.23), calls=%async_computation.1 | async-start | bytes 294912 | tf_op jit(solution)/shard_map/all_to_all | solution.py:25
  79.7 17.2 %collective-permute-start = (bf16[1024,128]{1,0:T(8,128)(2,1)S(1)}, bf16[1024,128]{1,0:T(8,128)(2,1)S(1)}, u32[]{:S(2)}, u32[]{:S(2)}) collective-permute-start(bf16[1024,128]{1,0:T(8,128)(2,1)S(1)} %get-tuple-element.18), channel_id=1, source_target_pairs={{0,1},{1,0},{2,3},{3,2},{4,5},{5,4},{6,7},{7,6},{8,9},{9,8},{10,11... | collective-permute-start | bytes 786440 | tf_op jit(solution)/shard_map/ppermute | solution.py:32
  96.7 9.9 %copy-start.18 = (f32[128]{0:T(128)S(1)}, f32[128]{0:T(128)}, u32[]{:S(2)}) copy-start(f32[128]{0:T(128)} %param.47) | copy-start | bytes 1540
  96.8 12.1 %copy-start.3 = (bf16[128,2048]{1,0:T(8,128)(2,1)S(1)}, bf16[128,2048]{1,0:T(8,128)(2,1)}, u32[]{:S(2)}) copy-start(bf16[128,2048]{1,0:T(8,128)(2,1)} %param.48) | copy-start | bytes 1572868
  97.7 17.8 %all-to-all-start.2 = ((bf16[16,32,128]{2,1,0:T(8,128)(2,1)}), bf16[16,32,128]{2,1,0:T(8,128)(2,1)S(1)}, u32[]{:S(2)}, u32[]{:S(2)}) async-start(bf16[16,32,128]{2,1,0:T(8,128)(2,1)} %broadcast_in_dim.24), calls=%async_computation.2 | async-start | bytes 262144 | tf_op jit(solution)/shard_map/all_to_all | solution.py:25
  106.6 4.6 %collective-permute-start.2 = (f32[128]{0:T(128)S(1)}, f32[128]{0:T(128)S(1)}, u32[]{:S(2)}, u32[]{:S(2)}) collective-permute-start(f32[128]{0:T(128)S(1)} %copy-done.18), channel_id=1, source_target_pairs={{0,1},{1,0},{2,3},{3,2},{4,5},{5,4},{6,7},{7,6},{8,9},{9,8},{10,11... | collective-permute-start | bytes 1544 | tf_op jit(solution)/shard_map/ppermute | solution.py:32
  109.0 6.8 %collective-permute-start.1 = (bf16[128,1024]{1,0:T(8,128)(2,1)S(1)}, bf16[128,1024]{1,0:T(8,128)(2,1)S(1)}, u32[]{:S(2)}, u32[]{:S(2)}) collective-permute-start(bf16[128,1024]{1,0:T(8,128)(2,1)S(1)} %get-tuple-element.16), channel_id=1, source_target_pairs={{0,1},{1,0},{2,3},{3,2},{4,5},{5,4},{6,7},{7,6},{8,9},{9,8},{10,11... | collective-permute-start | bytes 786440 | tf_op jit(solution)/shard_map/ppermute | solution.py:32
  116.1 4.9 %copy-start.4 = (bf16[2048,128]{1,0:T(8,128)(2,1)S(1)}, bf16[2048,128]{1,0:T(8,128)(2,1)}, u32[]{:S(2)}) copy-start(bf16[2048,128]{1,0:T(8,128)(2,1)} %param.49) | copy-start | bytes 1572868
  117.0 32.4 %all-to-all-start.3 = ((bf16[16,72,256]{2,1,0:T(8,128)(2,1)}), bf16[16,72,256]{2,1,0:T(8,128)(2,1)S(1)}, u32[]{:S(2)}, u32[]{:S(2)}) async-start(bf16[16,72,256]{2,1,0:T(8,128)(2,1)} %pad_maximum_fusion), calls=%async_computation.3 | async-start | bytes 1179648 | tf_op jit(solution)/shard_map/all_to_all | solution.py:198
  121.1 56.2 %collective-permute-start.3 = (bf16[1024,128]{1,0:T(8,128)(2,1)S(1)}, bf16[1024,128]{1,0:T(8,128)(2,1)S(1)}, u32[]{:S(2)}, u32[]{:S(2)}) collective-permute-start(bf16[1024,128]{1,0:T(8,128)(2,1)S(1)} %get-tuple-element.14), channel_id=1, source_target_pairs={{0,1},{1,0},{2,3},{3,2},{4,5},{5,4},{6,7},{7,6},{8,9},{9,8},{10,11... | collective-permute-start | bytes 786440 | tf_op jit(solution)/shard_map/ppermute | solution.py:32

commit v2 on v1

v2 whole, which is shorter than its diff:
```python
import jax
import jax.numpy as jnp
from jax import lax
from jax.sharding import Mesh
from jax.sharding import PartitionSpec as P

D = 4096
HEAD_DIM = 64
D_STATE = 128
TAPS = 4
SSM_WIDTH = 2048
LANES = 128
KV = ("kh", "kl")

EPS = 1e-06
BF16 = jnp.bfloat16
F32 = jnp.float32


def two_words(x):
    high = lax.reduce_precision(x, 8, 7)
    return high.astype(BF16), (x - high).astype(BF16)


def three_words(x):
    high = lax.reduce_precision(x, 8, 7)
    rest = x - high
    middle = lax.reduce_precision(rest, 8, 7)
    return high.astype(BF16), middle.astype(BF16), (rest - middle).astype(BF16)


def to_everyone(shard, axes):
    size = lax.axis_size(axes)
    return lax.all_to_all(
        jnp.broadcast_to(shard[None], (size, *shard.shape)), axes, 0, 0, tiled=True
    )


def from_partner(x, axis):
    size = lax.axis_size(axis)
    return lax.ppermute(x, axis, [(i, (i + 1) % size) for i in range(size)])


def exchanged(blocks, here, axes):
    team = blocks.shape[0]
    own = lax.dynamic_index_in_dim(blocks, here, 0, keepdims=True)
    out = jnp.zeros_like(blocks)
    out = lax.dynamic_update_slice_in_dim(out, own, here, 0)
    for mask in range(1, team):
        perm = [(i, i ^ mask) for i in range(team)]
        sent = lax.dynamic_index_in_dim(blocks, here ^ mask, 0, keepdims=True)
        got = lax.ppermute(sent, axes, perm)
        out = lax.dynamic_update_slice_in_dim(out, got, here ^ mask, 0)
    return out


def convolve(history, weights, newest):
    summed = weights[TAPS - 1] * newest
    for offset in range(TAPS - 1):
        summed = summed + weights[offset] * history[:, offset].astype(F32)
    return jax.nn.silu(summed)


def per_device(
    inputs,
    gain_in,
    w_gate,
    w_input,
    w_bproj,
    w_cproj,
    w_step,
    conv_input,
    conv_bproj,
    conv_cproj,
    tail_input,
    tail_bproj,
    tail_cproj,
    step_bias,
    decay_log,
    block_input,
    block_bproj,
    block_step,
    lengths,
    state,
    gain_mix,
    w_out,
    gain_mlp,
    w_up,
    w_down,
):
    core = lax.axis_index("tp")
    team = ("kl", "tp")
    member = lax.axis_index(team)
    n_team = lax.axis_size(team)
    n_kv, n_dp, n_tp = lax.axis_size(KV), lax.axis_size("dp"), lax.axis_size("tp")
    n_far = lax.axis_size("kh")
    stream = inputs.astype(F32)
    rows = inputs.shape[0]
    squares = jnp.sum(stream * stream, axis=1)
    scaled = (stream * gain_in).astype(BF16)
    matrices = (w_gate, w_input, w_bproj, w_cproj)
    pieces = [jnp.dot(scaled, weight, preferred_element_type=F32).astype(BF16) for weight in matrices]
    pieces += two_words(jnp.dot(scaled, w_step, preferred_element_type=F32))
    pieces += two_words(squares[:, None])
    bounds = [0]
    for piece in pieces:
        bounds.append(bounds[-1] + piece.shape[1])
    spare = -bounds[-1] % LANES
    pieces.append(jnp.zeros((rows, spare), BF16))
    sent = jnp.concatenate(pieces, axis=1).reshape(n_kv, rows // n_kv, -1)
    arrived = lax.all_to_all(sent, KV, 0, 0, tiled=True)

    out_blocks = jnp.moveaxis(w_out.reshape(w_out.shape[0], n_tp, -1), 1, 0)
    out_weight = exchanged(out_blocks, core, ("tp",)).reshape(-1, out_blocks.shape[2])
    up_blocks = jnp.moveaxis(w_up.reshape(w_up.shape[0], n_team, -1), 1, 0)
    depth, width = up_blocks.shape[1:]
    gain_words = jnp.stack(three_words(gain_mlp))
    gain_words = jnp.pad(gain_words, ((0, 5), (0, width - gain_words.shape[1])))
    up_blocks = jnp.concatenate(
        [up_blocks, jnp.broadcast_to(gain_words[None], (n_team, *gain_words.shape))], axis=1
    )
    up_blocks = exchanged(up_blocks, member, team)
    arrived, up_blocks = lax.optimization_barrier((arrived, up_blocks))
    projected = jnp.sum(arrived.astype(F32), axis=0)
    up_gain = jnp.sum(up_blocks[:, depth : depth + 3, : gain_mlp.shape[0]].astype(F32), axis=1)
    up_gain = up_gain.reshape(-1)
    up_weight = up_blocks[:, :depth].reshape(-1, width)
    down_blocks = w_down.reshape(n_team, -1, w_down.shape[1])
    down_weight = exchanged(down_blocks, member, team)

    parts = [projected[:, a:b] for a, b in zip(bounds[:-1], bounds[1:])]
    inverse = lax.rsqrt((parts[6] + parts[7]) / D + EPS)
    gate_pre, value_pre, b_pre, c_pre = [parts[k] * inverse for k in range(4)]
    step_pre = (parts[4] + parts[5]) * inverse
    seq_count = lengths.shape[0]
    head_count = step_bias.shape[0]
    group_count = w_bproj.shape[1] // D_STATE
    block_len = block_step.shape[1]
    per_group = head_count // group_count
    current = convolve(tail_input, conv_input, value_pre)
    b_now = convolve(tail_bproj, conv_bproj, b_pre)
    c_now = convolve(tail_cproj, conv_cproj, c_pre)
    step_size = jax.nn.softplus(step_pre + step_bias)
    decay_rate = -jnp.exp(decay_log)
    positions = lax.broadcasted_iota(jnp.int32, (1, block_len), 1)
    live_rows = (positions < lengths[:, None]).astype(F32)
    masked = block_step * live_rows[:, :, None]
    later_steps = jnp.sum(masked, axis=1, keepdims=True) - jnp.cumsum(masked, axis=1)
    decays = jnp.exp(decay_rate * (step_size[:, None, :] + later_steps)) * live_rows[:, :, None]
    c_query = c_now.astype(BF16).reshape(seq_count, group_count, D_STATE)
    keys = block_bproj.reshape(seq_count, block_len, group_count, D_STATE)
    scores = jnp.einsum("bsgn,bgn->bsg", keys, c_query, preferred_element_type=F32)
    scores = jnp.repeat(scores, per_group, axis=2)
    weights = (decays * scores * block_step).astype(BF16)
    values = block_input.reshape(seq_count, block_len, head_count, HEAD_DIM)
    inner_sum = jnp.einsum("bsh,bshp->bhp", weights, values, preferred_element_type=F32)
    c_full = c_now.reshape(seq_count, group_count, D_STATE)
    b_full = b_now.reshape(seq_count, group_count, D_STATE)
    own_score = jnp.repeat(jnp.sum(c_full * b_full, axis=2), per_group, axis=1)
    own_term = (step_size * own_score)[:, :, None] * current.reshape(
        seq_count, head_count, HEAD_DIM
    )
    carried = jnp.exp(decay_rate * (step_size + jnp.sum(masked, axis=1)))
    c_heads = jnp.repeat(c_full, per_group, axis=1)
    readout = jnp.einsum("bhpn,bhn->bhp", state, c_heads, precision=lax.Precision.HIGHEST)
    mixed = (inner_sum + own_term + carried[:, :, None] * readout).reshape(
        seq_count, -1
    ) * jax.nn.silu(gate_pre)

    width = mixed.shape[1]
    local_sq = two_words(jnp.sum(mixed * mixed, axis=1, keepdims=True))
    row = jnp.concatenate(
        [(mixed * gain_mix).astype(BF16), *local_sq, jnp.zeros((seq_count, LANES - 2), BF16)], axis=1
    )
    whole = to_everyone(row, KV + ("tp",)).reshape(n_kv, n_tp, seq_count, -1)
    whole = jnp.moveaxis(whole, 1, 0).reshape(n_tp, rows, -1)
    total_sq = jnp.sum(whole[:, :, width : width + 2].astype(F32), axis=(0, 2))
    channels = jnp.concatenate([whole[k, :, :width] for k in range(n_tp)], axis=1)
    mixed_in = jnp.dot(channels, out_weight, preferred_element_type=F32)
    mixed_in = mixed_in * lax.rsqrt(total_sq / SSM_WIDTH + EPS)[:, None]
    column_count = mixed_in.shape[1]
    residual = lax.dynamic_slice_in_dim(stream, core * column_count, column_count, 1)
    hidden = (residual + mixed_in).astype(BF16)

    all_hidden = to_everyone(hidden, ("dp",) + team).reshape(n_dp, n_team, rows, -1)
    all_hidden = jnp.moveaxis(all_hidden, 1, 2).reshape(n_dp * rows, -1).astype(F32)
    row_sq = jnp.sum(all_hidden * all_hidden, axis=1)
    lifted = (all_hidden * up_gain).astype(BF16)
    raised = lax.dot_general(
        up_weight, lifted, (((0,), (1,)), ((), ())), preferred_element_type=F32
    ).astype(BF16)
    seqs = raised.shape[1]
    extra = jnp.concatenate(
        [*[w[None] for w in two_words(row_sq)], jnp.zeros((6, seqs), BF16)], axis=0
    )
    sent = jnp.concatenate(
        [
            raised.reshape(n_far, -1, seqs),
            jnp.broadcast_to(extra[None], (n_far, *extra.shape)),
        ],
        axis=1,
    )
    arrived = lax.all_to_all(sent, "kh", 0, 0, tiled=True)
    arrived, down_weight = lax.optimization_barrier((arrived, down_weight))
    shares = jnp.sum(arrived.astype(F32), axis=0)
    unit_count = shares.shape[0] - 8
    sq_sum = shares[unit_count] + shares[unit_count + 1]
    units = jnp.square(
        jax.nn.relu(shares[:unit_count] * lax.rsqrt(sq_sum / D + EPS)[None, :])
    ).astype(BF16)
    hidden_units = to_everyone(units, "kh").reshape(-1, seqs)
    lowered = lax.dot_general(
        hidden_units, down_weight, (((0,), (1,)), ((), ())), preferred_element_type=F32
    ).astype(BF16)
    lowered = lowered.reshape(n_dp, rows, n_team, -1)
    lowered = jnp.moveaxis(lowered, 2, 1).reshape(n_dp * n_team, rows, -1)
    lowered = lax.all_to_all(lowered, ("dp",) + team, 0, 0, tiled=True)
    return (hidden.astype(F32) + jnp.sum(lowered.astype(F32), axis=0)).astype(BF16)


def solution(mesh):
    sizes = [mesh.shape[name] for name in ("grp", "dp", "kv", "tp")]
    pairs = mesh.devices.reshape(sizes[0], sizes[1], sizes[2] // 2, 2, sizes[3])
    mesh = Mesh(pairs, ("grp", "dp", "kh", "kl", "tp"))
    return jax.shard_map(
        per_device,
        mesh=mesh,
        in_specs=(
            P(("grp", "dp"), KV),
            P(KV),
            P(KV, "tp"),
            P(KV, "tp"),
            P(KV, "tp"),
            P(KV, "tp"),
            P(KV, "tp"),
            P(None, "tp"),
            P(None, "tp"),
            P(None, "tp"),
            P(("grp", "dp", *KV), None, "tp"),
            P(("grp", "dp", *KV), None, "tp"),
            P(("grp", "dp", *KV), None, "tp"),
            P("tp"),
            P("tp"),
            P(("grp", "dp", *KV), None, "tp"),
            P(("grp", "dp", *KV), None, "tp"),
            P(("grp", "dp", *KV), None, "tp"),
            P(("grp", "dp", *KV)),
            P(("grp", "dp", *KV), "tp", None, None),
            P("tp"),
            P("tp", KV),
            P((*KV, "tp")),
            P((*KV, "tp"), "dp"),
            P("dp", (*KV, "tp")),
        ),
        out_specs=P(("grp", "dp"), (*KV, "tp")),
        check_vma=False,
    )
```

time: 201 us -> 201 us (level)
  waiting for transfers between devices: 55.3 us -> 40.5 us
  local copies, waits for them, and re-layouts: 5.53 us -> 17.6 us
  starting transfers between devices: 76.7 us -> 87 us
  blocking collectives: 49.5 us -> 45.4 us
  matrix products: 7.82 us -> 3.97 us
    ppermute x4 -> x7, starting transfers between devices: 8.98 us -> 60.7 us  [exchanged(): got = lax.ppermute(sent, axes, perm)]
    all_to_all x2, starting transfers between devices: 48.2 us -> 7.85 us  [the longest x1 4.1 us: per_device(): arrived = lax.all_to_all(sent, KV, 0, 0, tiled=True)]
    all_to_all x2, waiting for transfers between devices: 37.3 us -> 5.15 us  [the longest x1 5.14 us: per_device(): arrived = lax.all_to_all(sent, KV, 0, 0, tiled=True)]
    all_gather x1 -> x0, blocking collectives: 27.8 us -> none  [per_device(): hidden_units = lax.all_gather(units, 'kv', axis=0, tiled=True)]
    all_to_all x1 -> x2, blocking collectives: 21.7 us -> 45.4 us  [the longest x1 29.6 us: to_everyone(): lax.all_to_all(jnp.broadcast_to(shard[None], (size, *shard.shape)), axes,...]
    ppermute x4 -> x7, waiting for transfers between devices: 0.01 us -> 12.7 us  [exchanged(): got = lax.ppermute(sent, axes, perm)]
    unnamed x45 -> x56, local copies, waits for them, and re-layouts: 0.54 us -> 8.43 us
    all_to_all x2, waiting for transfers between devices: 17.9 us -> 22.7 us  [to_everyone(): lax.all_to_all(jnp.broadcast_to(shard[None], (size, *shard.shape)), axes,...]
  transfers between devices with their start and end apart: 8 -> 11, of which waited for: 4 -> 6; matrix products, arithmetic and copies ran while one was open for 1% -> 4% of each run, Pallas kernels for 0% -> 0%
where the time goes in v2:
time: 201 us; the launch traced here: 200 us
  starting transfers between devices  87 us (43%)
  blocking collectives  45.4 us (23%)
  waiting for transfers between devices  40.5 us (20%)
  local copies, waits for them, and re-layouts  17.6 us (9%)
  other arithmetic  4.74 us (2%)
  matrix products  3.97 us (2%)
    ppermute x7, starting transfers between devices, exchanged(): got = lax.ppermute(sent, axes, perm)  60.7 us
    all_to_all x1, blocking collectives, to_everyone(): lax.all_to_all(jnp.broadcast_to(shard[None], (size, *shard.shape)), axes,...  29.6 us
    all_to_all x2, waiting for transfers between devices, to_everyone(): lax.all_to_all(jnp.broadcast_to(shard[None], (size, *shard.shape)), axes,...  22.7 us
    all_to_all x2, starting transfers between devices, to_everyone(): lax.all_to_all(jnp.broadcast_to(shard[None], (size, *shard.shape)), axes,...  18.4 us
    all_to_all x1, blocking collectives, per_device(): lowered = lax.all_to_all(lowered, ('dp',) + team, 0, 0, tiled=True)  15.8 us
    ppermute x7, waiting for transfers between devices, exchanged(): got = lax.ppermute(sent, axes, perm)  12.7 us
    unnamed x56, local copies, waits for them, and re-layouts  8.43 us
    all_to_all x1, waiting for transfers between devices, per_device(): arrived = lax.all_to_all(sent, KV, 0, 0, tiled=True)  5.14 us
  transfers between devices with their start and end apart: 11, of which 6 were waited for; matrix products, arithmetic and copies ran while one was open for 4% of the time, Pallas kernels for 0%

profile of v2, /device:TPU:65, one launch (start us, length us, event | category | flops | bytes accessed | tf_op | source)
XLA Modules:
  0.0 199.9 jit_solution(3379960278825358231)
XLA Ops:
  0.0 0.7 copy-done.22
  0.9 1.3 copy.99
  2.4 1.0 fusion.4
  3.4 43.5 %collective-permute-start = (bf16[1,136,512]{1,2,0:T(8,128)(2,1)}, bf16[1,136,512]{1,2,0:T(8,128)(2,1)}, u32[]{:S(2)}, u32[]{:S(2)}) collective-permute-start(bf16[1,136,512]{1,2,0:T(8,128)(2,1)} %get-tuple-element.23), channel_id=1, source_target_pairs={{0,1},{1,0},{2,3},{3,2},{4,5},{5,4},{6,7},{7,6},{8,9},{9,8},{10,11... | collective-permute-start | bytes 417800 | tf_op jit(solution)/shard_map/ppermute | solution.py:52
  46.9 2.0 collective-permute-start.1
  48.9 3.6 %collective-permute-start.2 = (bf16[1,136,512]{1,2,0:T(8,128)(2,1)S(1)}, bf16[1,136,512]{1,2,0:T(8,128)(2,1)}, u32[]{:S(2)}, u32[]{:S(2)}) collective-permute-start(bf16[1,136,512]{1,2,0:T(8,128)(2,1)S(1)} %get-tuple-element.21), channel_id=1, source_target_pairs={{0,3},{1,2},{2,1},{3,0},{4,7},{5,6},{6,5},{7,4},{8,11},{9,10},{10,... | collective-permute-start | bytes 417800 | tf_op jit(solution)/shard_map/ppermute | solution.py:52
  53.3 0.2 convolution_convert_fusion.3
  53.6 0.2 convolution_convert_fusion.2
  53.8 0.7 copy-done.8
  54.9 1.1 concatenate.37
  56.1 4.1 %all-to-all-start = ((bf16[16,2,3200]{2,1,0:T(2,128)(2,1)}), bf16[16,2,3200]{2,1,0:T(2,128)(2,1)S(1)}, u32[]{:S(2)}, u32[]{:S(2)}) async-start(bf16[16,2,3200]{2,1,0:T(2,128)(2,1)} %concatenate.37), calls=%async_computation | async-start | bytes 409600 | tf_op jit(solution)/shard_map/all_to_all | solution.py:111
  60.2 0.7 copy-done.15
  60.9 0.7 copy-done.12
  61.7 0.6 copy-done.23
  62.5 0.5 copy-done.24
  63.5 1.0 copy.108
  64.8 1.1 copy.102
  65.9 1.1 copy.103
  66.9 1.1 copy.104
  68.1 5.1 %all-to-all-done = bf16[16,2,3200]{2,1,0:T(2,128)(2,1)S(1)} async-done(((bf16[16,2,3200]{2,1,0:T(2,128)(2,1)}), bf16[16,2,3200]{2,1,0:T(2,128)(2,1)S(1)}, u32[]{:S(2)}, u32[]{:S(2)}) %all-to-all-start) | async-done | bytes 204832 | tf_op jit(solution)/shard_map/all_to_all | solution.py:111
  73.6 0.5 copy-done.14
  74.3 0.7 copy-done.19
  76.1 0.4 fusion.57
  76.5 1.7 fusion.58
  78.4 0.2 multiply_reduce_fusion.1
  78.9 0.7 broadcast_in_dim.35
  79.6 9.5 %all-to-all-start.1 = ((bf16[32,2,1152]{2,1,0:T(2,128)(2,1)}), bf16[32,2,1152]{2,1,0:T(2,128)(2,1)S(1)}, u32[]{:S(2)}, u32[]{:S(2)}) async-start(bf16[32,2,1152]{2,1,0:T(2,128)(2,1)} %broadcast_in_dim.35), calls=%async_computation.1 | async-start | bytes 294912 | tf_op jit(solution)/shard_map/all_to_all | solution.py:34
  89.1 0.2 copy.112
  89.6 2.6 %collective-permute-start.3 = (bf16[1,1024,128]{2,1,0:T(8,128)(2,1)S(1)}, bf16[1,1024,128]{2,1,0:T(8,128)(2,1)S(1)}, u32[]{:S(2)}, u32[]{:S(2)}) collective-permute-start(bf16[1,1024,128]{2,1,0:T(8,128)(2,1)S(1)} %bitcast.135), channel_id=1, source_target_pairs={{0,1},{1,0},{2,3},{3,2},{4,5},{5,4},{6,7},{7,6},{8,9},{9,8},{10,11... | collective-permute-start | bytes 786440 | tf_op jit(solution)/shard_map/ppermute | solution.py:52
  92.5 0.8 collective-permute-done.3
  93.4 12.0 %all-to-all-done.1 = bf16[32,2,1152]{2,1,0:T(2,128)(2,1)S(1)} async-done(((bf16[32,2,1152]{2,1,0:T(2,128)(2,1)}), bf16[32,2,1152]{2,1,0:T(2,128)(2,1)S(1)}, u32[]{:S(2)}, u32[]{:S(2)}) %all-to-all-start.1) | async-done | bytes 147488 | tf_op jit(solution)/shard_map/all_to_all | solution.py:34
  105.8 0.3 convert_reduce_fusion.3
  106.1 0.2 fusion.1
  106.4 0.7 broadcast_in_dim.37
  107.1 8.9 %all-to-all-start.2 = ((bf16[32,32,128]{2,1,0:T(8,128)(2,1)}), bf16[32,32,128]{2,1,0:T(8,128)(2,1)S(1)}, u32[]{:S(2)}, u32[]{:S(2)}) async-start(bf16[32,32,128]{2,1,0:T(8,128)(2,1)} %broadcast_in_dim.37), calls=%async_computation.2 | async-start | bytes 524288 | tf_op jit(solution)/shard_map/all_to_all | solution.py:34
  116.1 10.6 %all-to-all-done.2 = bf16[32,32,128]{2,1,0:T(8,128)(2,1)S(1)} async-done(((bf16[32,32,128]{2,1,0:T(8,128)(2,1)}), bf16[32,32,128]{2,1,0:T(8,128)(2,1)S(1)}, u32[]{:S(2)}, u32[]{:S(2)}) %all-to-all-start.2) | async-done | bytes 262176 | tf_op jit(solution)/shard_map/all_to_all | solution.py:34
  127.2 0.3 convolution_convert_fusion.1
  127.6 0.7 pad_maximum_fusion
  128.4 3.8 %all-to-all-start.3 = ((bf16[8,72,256]{2,1,0:T(8,128)(2,1)}), bf16[8,72,256]{2,1,0:T(8,128)(2,1)S(1)}, u32[]{:S(2)}, u32[]{:S(2)}) async-start(bf16[8,72,256]{2,1,0:T(8,128)(2,1)} %pad_maximum_fusion), calls=%async_computation.3 | async-start | bytes 589824 | tf_op jit(solution)/shard_map/all_to_all | solution.py:203
  132.3 3.5 %collective-permute-start.4 = (bf16[1,512,128]{2,1,0:T(8,128)(2,1)S(1)}, bf16[1,512,128]{2,1,0:T(8,128)(2,1)S(1)}, u32[]{:S(2)}, u32[]{:S(2)}) collective-permute-start(bf16[1,512,128]{2,1,0:T(8,128)(2,1)S(1)} %get-tuple-element.27), channel_id=1, source_target_pairs={{0,1},{1,0},{2,3},{3,2},{4,5},{5,4},{6,7},{7,6},{8,9},{9,8},{10,11... | collective-permute-start | bytes 393224 | tf_op jit(solution)/shard_map/ppermute | solution.py:52
  135.9 3.1 %collective-permute-start.5 = (bf16[1,512,128]{2,1,0:T(8,128)(2,1)S(1)}, bf16[1,512,128]{2,1,0:T(8,128)(2,1)S(1)}, u32[]{:S(2)}, u32[]{:S(2)}) collective-permute-start(bf16[1,512,128]{2,1,0:T(8,128)(2,1)S(1)} %get-tuple-element.26), channel_id=1, source_target_pairs={{0,2},{1,3},{2,0},{3,1},{4,6},{5,7},{6,4},{7,5},{8,10},{9,11},{10,... | collective-permute-start | bytes 393224 | tf_op jit(solution)/shard_map/ppermute | solution.py:52
  139.0 2.4 %collective-permute-start.6 = (bf16[1,512,128]{2,1,0:T(8,128)(2,1)S(1)}, bf16[1,512,128]{2,1,0:T(8,128)(2,1)S(1)}, u32[]{:S(2)}, u32[]{:S(2)}) collective-permute-start(bf16[1,512,128]{2,1,0:T(8,128)(2,1)S(1)} %get-tuple-element.25), channel_id=1, source_target_pairs={{0,3},{1,2},{2,1},{3,0},{4,7},{5,6},{6,5},{7,4},{8,11},{9,10},{10,... | collective-permute-start | bytes 393224 | tf_op jit(solution)/shard_map/ppermute | solution.py:52
  141.4 7.8 %collective-permute-done.5 = bf16[1,512,128]{2,1,0:T(8,128)(2,1)S(1)} collective-permute-done((bf16[1,512,128]{2,1,0:T(8,128)(2,1)S(1)}, bf16[1,512,128]{2,1,0:T(8,128)(2,1)S(1)}, u32[]{:S(2)}, u32[]{:S(2)}) %collective-permute-start.5) | collective-permute-done | bytes 131104 | tf_op jit(solution)/shard_map/ppermute | solution.py:52
  149.3 4.0 %collective-permute-done.6 = bf16[1,512,128]{2,1,0:T(8,128)(2,1)S(1)} collective-permute-done((bf16[1,512,128]{2,1,0:T(8,128)(2,1)S(1)}, bf16[1,512,128]{2,1,0:T(8,128)(2,1)S(1)}, u32[]{:S(2)}, u32[]{:S(2)}) %collective-permute-start.6) | collective-permute-done | bytes 131104 | tf_op jit(solution)/shard_map/ppermute | solution.py:52
  153.4 29.6 %all_to_all.30 = bf16[8,64,256]{2,1,0:T(8,128)(2,1)S(1)} all-to-all(bf16[8,64,256]{2,1,0:T(8,128)(2,1)S(1)} %broadcast_in_dim.41), channel_id=1, replica_groups=mesh['grp'=2,'dp'=8,'kh'=8,'kl'=2,'tp'=2] {'kh'}, dimensions={0} | all-to-all | bytes 524288 | tf_op jit(solution)/shard_map/all_to_all | solution.py:34
  183.1 0.3 convolution_convert_fusion
  183.4 15.8 %all_to_all.31 = bf16[32,32,128]{2,1,0:T(8,128)(2,1)S(1)} all-to-all(bf16[32,32,128]{2,1,0:T(8,128)(2,1)S(1)} %bitcast.128), channel_id=1, replica_groups=mesh['grp'=2,'dp'=8,'kh'=8,'kl'=2,'tp'=2] {'dp','kl','tp'}, dimensions={0} | all-to-all | bytes 524288 | tf_op jit(solution)/shard_map/all_to_all | solution.py:217
  199.3 0.6 add_convert_fusion
  (142 shorter events, 6.6 us)
Async XLA Ops:
  0.0 76.5 %copy-start = (f32[2,16,64,128]{3,2,1,0:T(8,128)S(1)}, f32[2,16,64,128]{3,2,1,0:T(8,128)}, u32[]{:S(2)}) copy-start(f32[2,16,64,128]{3,2,1,0:T(8,128)} %param.44) | copy-start | bytes 3145732
  0.0 0.7 copy-start.22
  2.4 50.1 %copy-start.1 = (bf16[32,256]{1,0:T(8,128)(2,1)S(1)}, bf16[32,256]{1,0:T(8,128)(2,1)}, u32[]{:S(2)}) copy-start(bf16[32,256]{1,0:T(8,128)(2,1)} %param.25) | copy-start | bytes 49156
  2.4 50.6 %copy-start.11 = (f32[256]{0:T(256)S(1)}, f32[256]{0:T(256)}, u32[]{:S(2)}) copy-start(f32[256]{0:T(256)} %param.26) | copy-start | bytes 3076
  2.4 50.6 %copy-start.17 = (bf16[256,16]{0,1:T(8,128)(2,1)S(1)}, bf16[256,16]{0,1:T(8,128)(2,1)}, u32[]{:S(2)}) copy-start(bf16[256,16]{0,1:T(8,128)(2,1)} %param.31) | copy-start | bytes 24580
  2.4 50.9 %copy-start.2 = (bf16[256,1024]{1,0:T(8,128)(2,1)S(1)}, bf16[256,1024]{1,0:T(8,128)(2,1)}, u32[]{:S(2)}) copy-start(bf16[256,1024]{1,0:T(8,128)(2,1)} %param.27) | copy-start | bytes 1572868
  3.4 50.1 %copy-start.3 = (bf16[256,1024]{1,0:T(8,128)(2,1)S(1)}, bf16[256,1024]{1,0:T(8,128)(2,1)}, u32[]{:S(2)}) copy-start(bf16[256,1024]{1,0:T(8,128)(2,1)} %param.28) | copy-start | bytes 1572868
  3.4 61.4 %collective-permute-start = (bf16[1,136,512]{1,2,0:T(8,128)(2,1)}, bf16[1,136,512]{1,2,0:T(8,128)(2,1)}, u32[]{:S(2)}, u32[]{:S(2)}) collective-permute-start(bf16[1,136,512]{1,2,0:T(8,128)(2,1)} %get-tuple-element.23), channel_id=1, source_target_pairs={{0,1},{1,0},{2,3},{3,2},{4,5},{5,4},{6,7},{7,6},{8,9},{9,8},{10,11... | collective-permute-start | bytes 417800 | tf_op jit(solution)/shard_map/ppermute | solution.py:52
  46.9 19.0 %collective-permute-start.1 = (bf16[1,136,512]{1,2,0:T(8,128)(2,1)}, bf16[1,136,512]{1,2,0:T(8,128)(2,1)}, u32[]{:S(2)}, u32[]{:S(2)}) collective-permute-start(bf16[1,136,512]{1,2,0:T(8,128)(2,1)} %get-tuple-element.24), channel_id=1, source_target_pairs={{0,2},{1,3},{2,0},{3,1},{4,6},{5,7},{6,4},{7,5},{8,10},{9,11},{10,... | collective-permute-start | bytes 417800 | tf_op jit(solution)/shard_map/ppermute | solution.py:52
  48.9 18.1 %collective-permute-start.2 = (bf16[1,136,512]{1,2,0:T(8,128)(2,1)S(1)}, bf16[1,136,512]{1,2,0:T(8,128)(2,1)}, u32[]{:S(2)}, u32[]{:S(2)}) collective-permute-start(bf16[1,136,512]{1,2,0:T(8,128)(2,1)S(1)} %get-tuple-element.21), channel_id=1, source_target_pairs={{0,3},{1,2},{2,1},{3,0},{4,7},{5,6},{6,5},{7,4},{8,11},{9,10},{10,... | collective-permute-start | bytes 417800 | tf_op jit(solution)/shard_map/ppermute | solution.py:52
  53.5 1.0 copy-start.8
  53.8 1.0 copy-start.9
  56.1 4.1 %copy-start.13 = (f32[4,1024]{1,0:T(4,128)S(1)}, f32[4,1024]{1,0:T(4,128)}, u32[]{:S(2)}) copy-start(f32[4,1024]{1,0:T(4,128)} %param.32) | copy-start | bytes 49156
  56.1 17.2 %all-to-all-start = ((bf16[16,2,3200]{2,1,0:T(2,128)(2,1)}), bf16[16,2,3200]{2,1,0:T(2,128)(2,1)S(1)}, u32[]{:S(2)}, u32[]{:S(2)}) async-start(bf16[16,2,3200]{2,1,0:T(2,128)(2,1)} %concatenate.37), calls=%async_computation | async-start | bytes 409600 | tf_op jit(solution)/shard_map/all_to_all | solution.py:111
  60.2 0.7 copy-start.15
  60.9 0.7 copy-start.12
  61.6 0.7 copy-start.23
  61.6 0.8 copy-start.16
  62.3 0.7 copy-start.24
  62.3 1.0 copy-start.10
  62.4 1.1 copy-start.4
  73.4 0.7 copy-start.14
  74.2 1.5 copy-start.21
  74.3 0.7 copy-start.19
  74.3 0.7 copy-start.18
  75.1 1.0 copy-start.7
  76.5 2.2 %copy-start.20 = (f32[1024]{0:T(1024)S(1)}, f32[1024]{0:T(1024)}, u32[]{:S(2)}) copy-start(f32[1024]{0:T(1024)} %param.45) | copy-start | bytes 12292
  78.3 10.8 %copy-start.5 = (bf16[1024,256]{1,0:T(8,128)(2,1)S(1)}, bf16[1024,256]{1,0:T(8,128)(2,1)}, u32[]{:S(2)}) copy-start(bf16[1024,256]{1,0:T(8,128)(2,1)} %param.46) | copy-start | bytes 1572868
  79.6 25.8 %all-to-all-start.1 = ((bf16[32,2,1152]{2,1,0:T(2,128)(2,1)}), bf16[32,2,1152]{2,1,0:T(2,128)(2,1)S(1)}, u32[]{:S(2)}, u32[]{:S(2)}) async-start(bf16[32,2,1152]{2,1,0:T(2,128)(2,1)} %broadcast_in_dim.35), calls=%async_computation.1 | async-start | bytes 294912 | tf_op jit(solution)/shard_map/all_to_all | solution.py:34
  89.6 3.8 %collective-permute-start.3 = (bf16[1,1024,128]{2,1,0:T(8,128)(2,1)S(1)}, bf16[1,1024,128]{2,1,0:T(8,128)(2,1)S(1)}, u32[]{:S(2)}, u32[]{:S(2)}) collective-permute-start(bf16[1,1024,128]{2,1,0:T(8,128)(2,1)S(1)} %bitcast.135), channel_id=1, source_target_pairs={{0,1},{1,0},{2,3},{3,2},{4,5},{5,4},{6,7},{7,6},{8,9},{9,8},{10,11... | collective-permute-start | bytes 786440 | tf_op jit(solution)/shard_map/ppermute | solution.py:52
  107.1 19.7 %all-to-all-start.2 = ((bf16[32,32,128]{2,1,0:T(8,128)(2,1)}), bf16[32,32,128]{2,1,0:T(8,128)(2,1)S(1)}, u32[]{:S(2)}, u32[]{:S(2)}) async-start(bf16[32,32,128]{2,1,0:T(8,128)(2,1)} %broadcast_in_dim.37), calls=%async_computation.2 | async-start | bytes 524288 | tf_op jit(solution)/shard_map/all_to_all | solution.py:34
  128.4 3.8 %copy-start.6 = (bf16[2048,128]{1,0:T(8,128)(2,1)S(1)}, bf16[2048,128]{1,0:T(8,128)(2,1)}, u32[]{:S(2)}) copy-start(bf16[2048,128]{1,0:T(8,128)(2,1)} %param.49) | copy-start | bytes 1572868
  128.4 24.9 %all-to-all-start.3 = ((bf16[8,72,256]{2,1,0:T(8,128)(2,1)}), bf16[8,72,256]{2,1,0:T(8,128)(2,1)S(1)}, u32[]{:S(2)}, u32[]{:S(2)}) async-start(bf16[8,72,256]{2,1,0:T(8,128)(2,1)} %pad_maximum_fusion), calls=%async_computation.3 | async-start | bytes 589824 | tf_op jit(solution)/shard_map/all_to_all | solution.py:203
  132.3 9.1 %collective-permute-start.4 = (bf16[1,512,128]{2,1,0:T(8,128)(2,1)S(1)}, bf16[1,512,128]{2,1,0:T(8,128)(2,1)S(1)}, u32[]{:S(2)}, u32[]{:S(2)}) collective-permute-start(bf16[1,512,128]{2,1,0:T(8,128)(2,1)S(1)} %get-tuple-element.27), channel_id=1, source_target_pairs={{0,1},{1,0},{2,3},{3,2},{4,5},{5,4},{6,7},{7,6},{8,9},{9,8},{10,11... | collective-permute-start | bytes 393224 | tf_op jit(solution)/shard_map/ppermute | solution.py:52
  135.9 13.4 %collective-permute-start.5 = (bf16[1,512,128]{2,1,0:T(8,128)(2,1)S(1)}, bf16[1,512,128]{2,1,0:T(8,128)(2,1)S(1)}, u32[]{:S(2)}, u32[]{:S(2)}) collective-permute-start(bf16[1,512,128]{2,1,0:T(8,128)(2,1)S(1)} %get-tuple-element.26), channel_id=1, source_target_pairs={{0,2},{1,3},{2,0},{3,1},{4,6},{5,7},{6,4},{7,5},{8,10},{9,11},{10,... | collective-permute-start | bytes 393224 | tf_op jit(solution)/shard_map/ppermute | solution.py:52
  139.0 14.3 %collective-permute-start.6 = (bf16[1,512,128]{2,1,0:T(8,128)(2,1)S(1)}, bf16[1,512,128]{2,1,0:T(8,128)(2,1)S(1)}, u32[]{:S(2)}, u32[]{:S(2)}) collective-permute-start(bf16[1,512,128]{2,1,0:T(8,128)(2,1)S(1)} %get-tuple-element.25), channel_id=1, source_target_pairs={{0,3},{1,2},{2,1},{3,0},{4,7},{5,6},{6,5},{7,4},{8,11},{9,10},{10,... | collective-permute-start | bytes 393224 | tf_op jit(solution)/shard_map/ppermute | solution.py:52

commit v3 on v2

--- a/solution.py
+++ b/solution.py
@@ -1,6 +1,7 @@
 import jax
 import jax.numpy as jnp
 from jax import lax
+from jax.experimental import pallas as pl
 from jax.sharding import Mesh
 from jax.sharding import PartitionSpec as P
 
@@ -34,11 +35,6 @@
     return lax.all_to_all(
         jnp.broadcast_to(shard[None], (size, *shard.shape)), axes, 0, 0, tiled=True
     )
-
-
-def from_partner(x, axis):
-    size = lax.axis_size(axis)
-    return lax.ppermute(x, axis, [(i, (i + 1) % size) for i in range(size)])
 
 
 def exchanged(blocks, here, axes):
@@ -54,6 +50,46 @@
     return out
 
 
+def project_body(x_ref, gain_ref, gate_ref, input_ref, b_ref, c_ref, step_ref, out_ref):
+    stream = x_ref[...].astype(F32)
+    scaled = (stream * gain_ref[...]).astype(BF16)
+    dests, each = out_ref.shape[:2]
+    at = 0
+
+    def put(block):
+        for k in range(dests):
+            out_ref[k, :, at : at + block.shape[1]] = block[k * each : (k + 1) * each].astype(BF16)
+
+    step = lax.dot_general(
+        scaled, step_ref[...], (((1,), (1,)), ((), ())), preferred_element_type=F32
+    )
+    step_high = step.astype(BF16)
+    step_low = (step - step_high.astype(F32)).astype(BF16)
+    heads = step.shape[1]
+    row = lax.broadcasted_iota(jnp.int32, (heads, LANES), 0)
+    lane = lax.broadcasted_iota(jnp.int32, (heads, LANES), 1)
+    tail = jnp.dot(step_high, (lane == row).astype(BF16), preferred_element_type=F32)
+    tail += jnp.dot(step_low, (lane == row + heads).astype(BF16), preferred_element_type=F32)
+    squares = jnp.sum(stream * stream, axis=1, keepdims=True)
+    high = squares.astype(BF16).astype(F32)
+    lane = lax.broadcasted_iota(jnp.int32, tail.shape, 1)
+    tail += jnp.where(lane == 2 * heads, high, 0.0)
+    tail += jnp.where(lane == 2 * heads + 1, squares - high, 0.0)
+    for ref in (gate_ref, input_ref, b_ref, c_ref):
+        put(jnp.dot(scaled, ref[...], preferred_element_type=F32))
+        at += ref.shape[1]
+    put(tail)
+
+
+def project(inputs, gain_in, matrices, w_step, dests):
+    rows = inputs.shape[0]
+    width = sum(w.shape[1] for w in matrices) + LANES
+    return pl.pallas_call(
+        project_body,
+        out_shape=jax.ShapeDtypeStruct((dests, rows // dests, width), BF16),
+    )(inputs, gain_in[None], *matrices, w_step.T)
+
+
 def convolve(history, weights, newest):
     summed = weights[TAPS - 1] * newest
     for offset in range(TAPS - 1):
@@ -61,7 +97,7 @@
     return jax.nn.silu(summed)
 
 
-def per_device(
+def layer(
     inputs,
     gain_in,
     w_gate,
@@ -96,18 +132,12 @@
     n_far = lax.axis_size("kh")
     stream = inputs.astype(F32)
     rows = inputs.shape[0]
-    squares = jnp.sum(stream * stream, axis=1)
-    scaled = (stream * gain_in).astype(BF16)
     matrices = (w_gate, w_input, w_bproj, w_cproj)
-    pieces = [jnp.dot(scaled, weight, preferred_element_type=F32).astype(BF16) for weight in matrices]
-    pieces += two_words(jnp.dot(scaled, w_step, preferred_element_type=F32))
-    pieces += two_words(squares[:, None])
+    heads = w_step.shape[1]
+    sent = project(inputs, gain_in, matrices, w_step, n_kv)
     bounds = [0]
-    for piece in pieces:
-        bounds.append(bounds[-1] + piece.shape[1])
-    spare = -bounds[-1] % LANES
-    pieces.append(jnp.zeros((rows, spare), BF16))
-    sent = jnp.concatenate(pieces, axis=1).reshape(n_kv, rows // n_kv, -1)
+    for width in [w.shape[1] for w in matrices] + [heads, heads, 1, 1]:
+        bounds.append(bounds[-1] + width)
     arrived = lax.all_to_all(sent, KV, 0, 0, tiled=True)
 
     out_blocks = jnp.moveaxis(w_out.reshape(w_out.shape[0], n_tp, -1), 1, 0)
@@ -223,7 +253,7 @@
     pairs = mesh.devices.reshape(sizes[0], sizes[1], sizes[2] // 2, 2, sizes[3])
     mesh = Mesh(pairs, ("grp", "dp", "kh", "kl", "tp"))
     return jax.shard_map(
-        per_device,
+        layer,
         mesh=mesh,
         in_specs=(
             P(("grp", "dp"), KV),

time: 201 us -> 201 us (level)
  Pallas kernels: 0 us -> 2.56 us
  local copies, waits for them, and re-layouts: 17.6 us -> 15.3 us
    ppermute x7, waiting for transfers between devices: 12.7 us -> 16.4 us  [exchanged(): got = lax.ppermute(sent, axes, perm)]
    all_to_all x2, waiting for transfers between devices: 5.15 us -> 2.33 us  [the longest x1 2.33 us: layer(): arrived = lax.all_to_all(sent, KV, 0, 0, tiled=True)]
    pallas_call x0 -> x1, Pallas kernels: none -> 2.56 us  [project(): pl.pallas_call(project_body, out_shape=jax.ShapeDtypeStruct((dests, rows...]
    unnamed x56 -> x42, local copies, waits for them, and re-layouts: 8.43 us -> 7.97 us
  transfers between devices with their start and end apart: 11 -> 11, of which waited for: 6 -> 7; matrix products, arithmetic and copies ran while one was open for 4% -> 3% of each run, Pallas kernels for 0% -> 1%
where the time goes in v3:
time: 201 us; the launch traced here: 200 us
  starting transfers between devices  86.7 us (43%)
  blocking collectives  45.4 us (23%)
  waiting for transfers between devices  41.4 us (21%)
  local copies, waits for them, and re-layouts  15.3 us (8%)
  other arithmetic  4.59 us (2%)
  matrix products  3.18 us (2%)
  Pallas kernels  2.56 us (1%)
    ppermute x7, starting transfers between devices, exchanged(): got = lax.ppermute(sent, axes, perm)  60.6 us
    all_to_all x1, blocking collectives, to_everyone(): lax.all_to_all(jnp.broadcast_to(shard[None], (size, *shard.shape)), axes,...  29.6 us
    all_to_all x2, waiting for transfers between devices, to_everyone(): lax.all_to_all(jnp.broadcast_to(shard[None], (size, *shard.shape)), axes,...  22.7 us
    all_to_all x2, starting transfers between devices, to_everyone(): lax.all_to_all(jnp.broadcast_to(shard[None], (size, *shard.shape)), axes,...  18.3 us
    ppermute x7, waiting for transfers between devices, exchanged(): got = lax.ppermute(sent, axes, perm)  16.4 us
    all_to_all x1, blocking collectives, layer(): lowered = lax.all_to_all(lowered, ('dp',) + team, 0, 0, tiled=True)  15.8 us
    unnamed x42, local copies, waits for them, and re-layouts  7.97 us
    all_to_all x1, starting transfers between devices, layer(): arrived = lax.all_to_all(sent, KV, 0, 0, tiled=True)  4.1 us
  transfers between devices with their start and end apart: 11, of which 7 were waited for; matrix products, arithmetic and copies ran while one was open for 3% of the time, Pallas kernels for 1%

profile of v3, /device:TPU:65, one launch (start us, length us, event | category | flops | bytes accessed | tf_op | source)
XLA Modules:
  0.0 199.7 jit_solution(14775872750310021214)
XLA Ops:
  0.0 0.7 copy-done.15
  0.9 1.3 copy.58
  2.4 1.0 fusion.4
  3.3 43.4 %collective-permute-start = (bf16[1,136,512]{1,2,0:T(8,128)(2,1)}, bf16[1,136,512]{1,2,0:T(8,128)(2,1)}, u32[]{:S(2)}, u32[]{:S(2)}) collective-permute-start(bf16[1,136,512]{1,2,0:T(8,128)(2,1)} %get-tuple-element.23), channel_id=1, source_target_pairs={{0,1},{1,0},{2,3},{3,2},{4,5},{5,4},{6,7},{7,6},{8,9},{9,8},{10,11... | collective-permute-start | bytes 417800 | tf_op jit(solution)/shard_map/ppermute | solution.py:48
  46.7 2.0 collective-permute-start.1
  48.7 3.6 %collective-permute-start.2 = (bf16[1,136,512]{1,2,0:T(8,128)(2,1)}, bf16[1,136,512]{1,2,0:T(8,128)(2,1)}, u32[]{:S(2)}, u32[]{:S(2)}) collective-permute-start(bf16[1,136,512]{1,2,0:T(8,128)(2,1)} %get-tuple-element.21), channel_id=1, source_target_pairs={{0,3},{1,2},{2,1},{3,0},{4,7},{5,6},{6,5},{7,4},{8,11},{9,10},{10,... | collective-permute-start | bytes 417800 | tf_op jit(solution)/shard_map/ppermute | solution.py:48
  52.2 2.6 %shard_map.235 = bf16[16,2,3200]{2,1,0:T(2,128)(2,1)} custom-call(bf16[32,256]{1,0:T(8,128)(2,1)} %x_ref.1, f32[1,256]{1,0:T(1,128)} %bitcast.152, bf16[256,1024]{1,0:T(8,128)(2,1)} %gate_ref.1, bf16[256,1024]{1,0:T(8,128)(2,1)} %input_ref.1, bf16[256,512]{1,0:T(8,128)(2,1)} %b_ref.1, bf16[256,512]{1,0:T(8,128)(2,1)} %c_ref.1, bf16[16,256]{1,0:T(8,128)(2,1)} %bitcast.142), custom_call_target="tpu_custom_call" | custom-call | tf_op jit(solution)/shard_map/pallas_call | solution.py:87
  54.8 4.1 %all-to-all-start = ((bf16[16,2,3200]{2,1,0:T(2,128)(2,1)}), bf16[16,2,3200]{2,1,0:T(2,128)(2,1)S(1)}, u32[]{:S(2)}, u32[]{:S(2)}) async-start(bf16[16,2,3200]{2,1,0:T(2,128)(2,1)} %shard_map.235), calls=%async_computation | async-start | bytes 409600 | tf_op jit(solution)/shard_map/all_to_all | solution.py:141
  59.0 0.7 copy-done.9
  59.6 0.7 copy-done.6
  60.4 0.6 copy-done.16
  61.2 0.5 copy-done.17
  62.3 0.3 copy.67
  62.8 1.1 copy.61
  63.9 1.1 copy.62
  65.0 3.7 %collective-permute-done.2 = bf16[1,136,512]{1,2,0:T(8,128)(2,1)} collective-permute-done((bf16[1,136,512]{1,2,0:T(8,128)(2,1)}, bf16[1,136,512]{1,2,0:T(8,128)(2,1)}, u32[]{:S(2)}, u32[]{:S(2)}) %collective-permute-start.2) | collective-permute-done | bytes 139296 | tf_op jit(solution)/shard_map/ppermute | solution.py:48
  68.6 1.1 copy.63
  69.8 2.3 %all-to-all-done = bf16[16,2,3200]{2,1,0:T(2,128)(2,1)S(1)} async-done(((bf16[16,2,3200]{2,1,0:T(2,128)(2,1)}), bf16[16,2,3200]{2,1,0:T(2,128)(2,1)S(1)}, u32[]{:S(2)}, u32[]{:S(2)}) %all-to-all-start) | async-done | bytes 204832 | tf_op jit(solution)/shard_map/all_to_all | solution.py:141
  72.5 0.5 copy-done.8
  73.2 0.7 copy-done.12
  74.6 0.6 copy-done.14
  75.4 0.4 fusion.54
  75.8 1.7 fusion.55
  77.7 0.2 multiply_reduce_fusion
  78.2 0.7 broadcast_in_dim.35
  78.9 9.4 %all-to-all-start.1 = ((bf16[32,2,1152]{2,1,0:T(2,128)(2,1)}), bf16[32,2,1152]{2,1,0:T(2,128)(2,1)S(1)}, u32[]{:S(2)}, u32[]{:S(2)}) async-start(bf16[32,2,1152]{2,1,0:T(2,128)(2,1)} %broadcast_in_dim.35), calls=%async_computation.1 | async-start | bytes 294912 | tf_op jit(solution)/shard_map/all_to_all | solution.py:35
  88.3 0.2 copy.71
  88.7 2.6 %collective-permute-start.3 = (bf16[1,1024,128]{2,1,0:T(8,128)(2,1)S(1)}, bf16[1,1024,128]{2,1,0:T(8,128)(2,1)S(1)}, u32[]{:S(2)}, u32[]{:S(2)}) collective-permute-start(bf16[1,1024,128]{2,1,0:T(8,128)(2,1)S(1)} %bitcast.130), channel_id=1, source_target_pairs={{0,1},{1,0},{2,3},{3,2},{4,5},{5,4},{6,7},{7,6},{8,9},{9,8},{10,11... | collective-permute-start | bytes 786440 | tf_op jit(solution)/shard_map/ppermute | solution.py:48
  91.7 0.8 collective-permute-done.3
  92.5 12.0 %all-to-all-done.1 = bf16[32,2,1152]{2,1,0:T(2,128)(2,1)S(1)} async-done(((bf16[32,2,1152]{2,1,0:T(2,128)(2,1)}), bf16[32,2,1152]{2,1,0:T(2,128)(2,1)S(1)}, u32[]{:S(2)}, u32[]{:S(2)}) %all-to-all-start.1) | async-done | bytes 147488 | tf_op jit(solution)/shard_map/all_to_all | solution.py:35
  104.9 0.3 convert_reduce_fusion.3
  105.3 0.7 copy-done.5
  106.0 0.2 fusion.1
  106.2 0.7 broadcast_in_dim.37
  106.9 8.9 %all-to-all-start.2 = ((bf16[32,32,128]{2,1,0:T(8,128)(2,1)}), bf16[32,32,128]{2,1,0:T(8,128)(2,1)S(1)}, u32[]{:S(2)}, u32[]{:S(2)}) async-start(bf16[32,32,128]{2,1,0:T(8,128)(2,1)} %broadcast_in_dim.37), calls=%async_computation.2 | async-start | bytes 524288 | tf_op jit(solution)/shard_map/all_to_all | solution.py:35
  116.0 10.6 %all-to-all-done.2 = bf16[32,32,128]{2,1,0:T(8,128)(2,1)S(1)} async-done(((bf16[32,32,128]{2,1,0:T(8,128)(2,1)}), bf16[32,32,128]{2,1,0:T(8,128)(2,1)S(1)}, u32[]{:S(2)}, u32[]{:S(2)}) %all-to-all-start.2) | async-done | bytes 262176 | tf_op jit(solution)/shard_map/all_to_all | solution.py:35
  127.0 0.3 convolution_convert_fusion.1
  127.5 0.7 pad_maximum_fusion
  128.2 3.8 %all-to-all-start.3 = ((bf16[8,72,256]{2,1,0:T(8,128)(2,1)}), bf16[8,72,256]{2,1,0:T(8,128)(2,1)S(1)}, u32[]{:S(2)}, u32[]{:S(2)}) async-start(bf16[8,72,256]{2,1,0:T(8,128)(2,1)} %pad_maximum_fusion), calls=%async_computation.3 | async-start | bytes 589824 | tf_op jit(solution)/shard_map/all_to_all | solution.py:233
  132.1 3.5 %collective-permute-start.4 = (bf16[1,512,128]{2,1,0:T(8,128)(2,1)S(1)}, bf16[1,512,128]{2,1,0:T(8,128)(2,1)S(1)}, u32[]{:S(2)}, u32[]{:S(2)}) collective-permute-start(bf16[1,512,128]{2,1,0:T(8,128)(2,1)S(1)} %get-tuple-element.27), channel_id=1, source_target_pairs={{0,1},{1,0},{2,3},{3,2},{4,5},{5,4},{6,7},{7,6},{8,9},{9,8},{10,11... | collective-permute-start | bytes 393224 | tf_op jit(solution)/shard_map/ppermute | solution.py:48
  135.7 3.1 %collective-permute-start.5 = (bf16[1,512,128]{2,1,0:T(8,128)(2,1)S(1)}, bf16[1,512,128]{2,1,0:T(8,128)(2,1)S(1)}, u32[]{:S(2)}, u32[]{:S(2)}) collective-permute-start(bf16[1,512,128]{2,1,0:T(8,128)(2,1)S(1)} %get-tuple-element.26), channel_id=1, source_target_pairs={{0,2},{1,3},{2,0},{3,1},{4,6},{5,7},{6,4},{7,5},{8,10},{9,11},{10,... | collective-permute-start | bytes 393224 | tf_op jit(solution)/shard_map/ppermute | solution.py:48
  138.8 2.4 %collective-permute-start.6 = (bf16[1,512,128]{2,1,0:T(8,128)(2,1)S(1)}, bf16[1,512,128]{2,1,0:T(8,128)(2,1)S(1)}, u32[]{:S(2)}, u32[]{:S(2)}) collective-permute-start(bf16[1,512,128]{2,1,0:T(8,128)(2,1)S(1)} %get-tuple-element.25), channel_id=1, source_target_pairs={{0,3},{1,2},{2,1},{3,0},{4,7},{5,6},{6,5},{7,4},{8,11},{9,10},{10,... | collective-permute-start | bytes 393224 | tf_op jit(solution)/shard_map/ppermute | solution.py:48
  141.2 7.8 %collective-permute-done.5 = bf16[1,512,128]{2,1,0:T(8,128)(2,1)S(1)} collective-permute-done((bf16[1,512,128]{2,1,0:T(8,128)(2,1)S(1)}, bf16[1,512,128]{2,1,0:T(8,128)(2,1)S(1)}, u32[]{:S(2)}, u32[]{:S(2)}) %collective-permute-start.5) | collective-permute-done | bytes 131104 | tf_op jit(solution)/shard_map/ppermute | solution.py:48
  149.1 4.0 %collective-permute-done.6 = bf16[1,512,128]{2,1,0:T(8,128)(2,1)S(1)} collective-permute-done((bf16[1,512,128]{2,1,0:T(8,128)(2,1)S(1)}, bf16[1,512,128]{2,1,0:T(8,128)(2,1)S(1)}, u32[]{:S(2)}, u32[]{:S(2)}) %collective-permute-start.6) | collective-permute-done | bytes 131104 | tf_op jit(solution)/shard_map/ppermute | solution.py:48
  153.3 29.6 %all_to_all.30 = bf16[8,64,256]{2,1,0:T(8,128)(2,1)S(1)} all-to-all(bf16[8,64,256]{2,1,0:T(8,128)(2,1)S(1)} %broadcast_in_dim.41), channel_id=1, replica_groups=mesh['grp'=2,'dp'=8,'kh'=8,'kl'=2,'tp'=2] {'kh'}, dimensions={0} | all-to-all | bytes 524288 | tf_op jit(solution)/shard_map/all_to_all | solution.py:35
  182.9 0.3 convolution_convert_fusion
  183.2 15.8 %all_to_all.31 = bf16[32,32,128]{2,1,0:T(8,128)(2,1)S(1)} all-to-all(bf16[32,32,128]{2,1,0:T(8,128)(2,1)S(1)} %bitcast.123), channel_id=1, replica_groups=mesh['grp'=2,'dp'=8,'kh'=8,'kl'=2,'tp'=2] {'dp','kl','tp'}, dimensions={0} | all-to-all | bytes 524288 | tf_op jit(solution)/shard_map/all_to_all | solution.py:247
  199.1 0.6 add_convert_fusion
  (109 shorter events, 5.2 us)
Async XLA Ops:
  0.0 75.8 %copy-start = (f32[2,16,64,128]{3,2,1,0:T(8,128)S(1)}, f32[2,16,64,128]{3,2,1,0:T(8,128)}, u32[]{:S(2)}) copy-start(f32[2,16,64,128]{3,2,1,0:T(8,128)} %param.44) | copy-start | bytes 3145732
  0.0 0.7 copy-start.15
  3.3 59.5 %collective-permute-start = (bf16[1,136,512]{1,2,0:T(8,128)(2,1)}, bf16[1,136,512]{1,2,0:T(8,128)(2,1)}, u32[]{:S(2)}, u32[]{:S(2)}) collective-permute-start(bf16[1,136,512]{1,2,0:T(8,128)(2,1)} %get-tuple-element.23), channel_id=1, source_target_pairs={{0,1},{1,0},{2,3},{3,2},{4,5},{5,4},{6,7},{7,6},{8,9},{9,8},{10,11... | collective-permute-start | bytes 417800 | tf_op jit(solution)/shard_map/ppermute | solution.py:48
  46.7 17.2 %collective-permute-start.1 = (bf16[1,136,512]{1,2,0:T(8,128)(2,1)}, bf16[1,136,512]{1,2,0:T(8,128)(2,1)}, u32[]{:S(2)}, u32[]{:S(2)}) collective-permute-start(bf16[1,136,512]{1,2,0:T(8,128)(2,1)} %get-tuple-element.24), channel_id=1, source_target_pairs={{0,2},{1,3},{2,0},{3,1},{4,6},{5,7},{6,4},{7,5},{8,10},{9,11},{10,... | collective-permute-start | bytes 417800 | tf_op jit(solution)/shard_map/ppermute | solution.py:48
  48.7 20.0 %collective-permute-start.2 = (bf16[1,136,512]{1,2,0:T(8,128)(2,1)}, bf16[1,136,512]{1,2,0:T(8,128)(2,1)}, u32[]{:S(2)}, u32[]{:S(2)}) collective-permute-start(bf16[1,136,512]{1,2,0:T(8,128)(2,1)} %get-tuple-element.21), channel_id=1, source_target_pairs={{0,3},{1,2},{2,1},{3,0},{4,7},{5,6},{6,5},{7,4},{8,11},{9,10},{10,... | collective-permute-start | bytes 417800 | tf_op jit(solution)/shard_map/ppermute | solution.py:48
  54.8 4.1 %copy-start.7 = (f32[4,1024]{1,0:T(4,128)S(1)}, f32[4,1024]{1,0:T(4,128)}, u32[]{:S(2)}) copy-start(f32[4,1024]{1,0:T(4,128)} %param.32) | copy-start | bytes 49156
  54.8 17.3 %all-to-all-start = ((bf16[16,2,3200]{2,1,0:T(2,128)(2,1)}), bf16[16,2,3200]{2,1,0:T(2,128)(2,1)S(1)}, u32[]{:S(2)}, u32[]{:S(2)}) async-start(bf16[16,2,3200]{2,1,0:T(2,128)(2,1)} %shard_map.235), calls=%async_computation | async-start | bytes 409600 | tf_op jit(solution)/shard_map/all_to_all | solution.py:141
  58.9 0.7 copy-start.9
  59.6 0.7 copy-start.6
  60.3 0.7 copy-start.16
  60.3 0.8 copy-start.10
  61.1 0.7 copy-start.17
  61.1 1.0 copy-start.4
  61.2 1.1 copy-start.1
  72.3 0.7 copy-start.8
  73.2 0.7 copy-start.12
  73.2 0.7 copy-start.11
  74.4 0.7 copy-start.14
  75.8 2.2 %copy-start.13 = (f32[1024]{0:T(1024)S(1)}, f32[1024]{0:T(1024)}, u32[]{:S(2)}) copy-start(f32[1024]{0:T(1024)} %param.45) | copy-start | bytes 12292
  77.6 10.7 %copy-start.2 = (bf16[1024,256]{1,0:T(8,128)(2,1)S(1)}, bf16[1024,256]{1,0:T(8,128)(2,1)}, u32[]{:S(2)}) copy-start(bf16[1024,256]{1,0:T(8,128)(2,1)} %param.46) | copy-start | bytes 1572868
  78.9 25.7 %all-to-all-start.1 = ((bf16[32,2,1152]{2,1,0:T(2,128)(2,1)}), bf16[32,2,1152]{2,1,0:T(2,128)(2,1)S(1)}, u32[]{:S(2)}, u32[]{:S(2)}) async-start(bf16[32,2,1152]{2,1,0:T(2,128)(2,1)} %broadcast_in_dim.35), calls=%async_computation.1 | async-start | bytes 294912 | tf_op jit(solution)/shard_map/all_to_all | solution.py:35
  88.7 3.8 %collective-permute-start.3 = (bf16[1,1024,128]{2,1,0:T(8,128)(2,1)S(1)}, bf16[1,1024,128]{2,1,0:T(8,128)(2,1)S(1)}, u32[]{:S(2)}, u32[]{:S(2)}) collective-permute-start(bf16[1,1024,128]{2,1,0:T(8,128)(2,1)S(1)} %bitcast.130), channel_id=1, source_target_pairs={{0,1},{1,0},{2,3},{3,2},{4,5},{5,4},{6,7},{7,6},{8,9},{9,8},{10,11... | collective-permute-start | bytes 786440 | tf_op jit(solution)/shard_map/ppermute | solution.py:48
  105.2 0.7 copy-start.5
  106.9 19.7 %all-to-all-start.2 = ((bf16[32,32,128]{2,1,0:T(8,128)(2,1)}), bf16[32,32,128]{2,1,0:T(8,128)(2,1)S(1)}, u32[]{:S(2)}, u32[]{:S(2)}) async-start(bf16[32,32,128]{2,1,0:T(8,128)(2,1)} %broadcast_in_dim.37), calls=%async_computation.2 | async-start | bytes 524288 | tf_op jit(solution)/shard_map/all_to_all | solution.py:35
  128.2 3.8 %copy-start.3 = (bf16[2048,128]{1,0:T(8,128)(2,1)S(1)}, bf16[2048,128]{1,0:T(8,128)(2,1)}, u32[]{:S(2)}) copy-start(bf16[2048,128]{1,0:T(8,128)(2,1)} %param.49) | copy-start | bytes 1572868
  128.2 24.9 %all-to-all-start.3 = ((bf16[8,72,256]{2,1,0:T(8,128)(2,1)}), bf16[8,72,256]{2,1,0:T(8,128)(2,1)S(1)}, u32[]{:S(2)}, u32[]{:S(2)}) async-start(bf16[8,72,256]{2,1,0:T(8,128)(2,1)} %pad_maximum_fusion), calls=%async_computation.3 | async-start | bytes 589824 | tf_op jit(solution)/shard_map/all_to_all | solution.py:233
  132.1 9.1 %collective-permute-start.4 = (bf16[1,512,128]{2,1,0:T(8,128)(2,1)S(1)}, bf16[1,512,128]{2,1,0:T(8,128)(2,1)S(1)}, u32[]{:S(2)}, u32[]{:S(2)}) collective-permute-start(bf16[1,512,128]{2,1,0:T(8,128)(2,1)S(1)} %get-tuple-element.27), channel_id=1, source_target_pairs={{0,1},{1,0},{2,3},{3,2},{4,5},{5,4},{6,7},{7,6},{8,9},{9,8},{10,11... | collective-permute-start | bytes 393224 | tf_op jit(solution)/shard_map/ppermute | solution.py:48
  135.7 13.4 %collective-permute-start.5 = (bf16[1,512,128]{2,1,0:T(8,128)(2,1)S(1)}, bf16[1,512,128]{2,1,0:T(8,128)(2,1)S(1)}, u32[]{:S(2)}, u32[]{:S(2)}) collective-permute-start(bf16[1,512,128]{2,1,0:T(8,128)(2,1)S(1)} %get-tuple-element.26), channel_id=1, source_target_pairs={{0,2},{1,3},{2,0},{3,1},{4,6},{5,7},{6,4},{7,5},{8,10},{9,11},{10,... | collective-permute-start | bytes 393224 | tf_op jit(solution)/shard_map/ppermute | solution.py:48
  138.8 14.3 %collective-permute-start.6 = (bf16[1,512,128]{2,1,0:T(8,128)(2,1)S(1)}, bf16[1,512,128]{2,1,0:T(8,128)(2,1)S(1)}, u32[]{:S(2)}, u32[]{:S(2)}) collective-permute-start(bf16[1,512,128]{2,1,0:T(8,128)(2,1)S(1)} %get-tuple-element.25), channel_id=1, source_target_pairs={{0,3},{1,2},{2,1},{3,0},{4,7},{5,6},{6,5},{7,4},{8,11},{9,10},{10,... | collective-permute-start | bytes 393224 | tf_op jit(solution)/shard_map/ppermute | solution.py:48

commit v4 on v1

v4 whole, which is shorter than its diff:
```python
import jax
import jax.numpy as jnp
from jax import lax
from jax.experimental import pallas as pl
from jax.experimental.pallas import tpu as pltpu
from jax.sharding import PartitionSpec as P

D = 4096
HEAD_DIM = 64
TAPS = 4
SSM_WIDTH = 2048
LANES = 128
SPARE = 8

EPS = 1e-06
BF16 = jnp.bfloat16
F32 = jnp.float32


def two_words(x):
    high = lax.reduce_precision(x, 8, 7)
    return high.astype(BF16), (x - high).astype(BF16)


def to_everyone(shard, axes):
    size = lax.axis_size(axes)
    return lax.all_to_all(
        jnp.broadcast_to(shard[None], (size, *shard.shape)), axes, 0, 0, tiled=True
    )


def from_partner(x):
    size = lax.axis_size("tp")
    return lax.ppermute(x, "tp", [(i, (i + 1) % size) for i in range(size)])


def exchanged(weight, dim, core):
    half = weight.shape[dim] // 2
    mine = lax.dynamic_slice_in_dim(weight, core * half, half, dim)
    other = lax.dynamic_slice_in_dim(weight, (1 - core) * half, half, dim)
    return mine, from_partner(other)


def in_core_order(mine, other, core, dim):
    return jnp.where(
        core == 0,
        jnp.concatenate([mine, other], axis=dim),
        jnp.concatenate([other, mine], axis=dim),
    )


def contract_last(a, b):
    return lax.dot_general(a, b, (((1,), (1,)), ((), ())), preferred_element_type=F32)


def project_body(x_ref, gain_ref, gate_ref, input_ref, b_ref, c_ref, step_ref, out_ref):
    stream = x_ref[...].astype(F32)
    scaled = (stream * gain_ref[...]).astype(BF16)
    dests, each = out_ref.shape[:2]
    at = 0

    def put(block):
        for k in range(dests):
            out_ref[k, :, at : at + block.shape[1]] = block[k * each : (k + 1) * each].astype(BF16)

    step = contract_last(scaled, step_ref[...])
    step_high = step.astype(BF16)
    step_low = (step - step_high.astype(F32)).astype(BF16)
    heads = step.shape[1]
    row = lax.broadcasted_iota(jnp.int32, (heads, LANES), 0)
    lane = lax.broadcasted_iota(jnp.int32, (heads, LANES), 1)
    tail = jnp.dot(step_high, (lane == row).astype(BF16), preferred_element_type=F32)
    tail += jnp.dot(step_low, (lane == row + heads).astype(BF16), preferred_element_type=F32)
    squares = jnp.sum(stream * stream, axis=1, keepdims=True)
    high = squares.astype(BF16).astype(F32)
    lane = lax.broadcasted_iota(jnp.int32, tail.shape, 1)
    tail += jnp.where(lane == 2 * heads, high, 0.0)
    tail += jnp.where(lane == 2 * heads + 1, squares - high, 0.0)
    for ref in (gate_ref, input_ref, b_ref, c_ref):
        put(jnp.dot(scaled, ref[...], preferred_element_type=F32))
        at += ref.shape[1]
    put(tail)


def project(inputs, gain_in, matrices, w_step, dests):
    rows = inputs.shape[0]
    width = sum(w.shape[1] for w in matrices) + LANES
    return pl.pallas_call(
        project_body,
        out_shape=jax.ShapeDtypeStruct((dests, rows // dests, width), BF16),
    )(inputs, gain_in[None], *matrices, w_step.T)


def prepare_body(steps_ref, lengths_ref, log_ref, state_ref, faded_ref, all_ref, high_ref, low_ref):
    seqs, heads, block = steps_ref.shape
    rate = -jnp.exp(log_ref[...])
    position = lax.broadcasted_iota(jnp.int32, (heads, block), 1)
    after = lax.broadcasted_iota(jnp.int32, (block, block), 0) > lax.broadcasted_iota(
        jnp.int32, (block, block), 1
    )
    for b in range(seqs):
        masked = jnp.where(position < lengths_ref[b], steps_ref[b], 0.0)
        later = jnp.dot(
            masked, after.astype(F32), precision=lax.Precision.HIGHEST, preferred_element_type=F32
        )
        faded_ref[b] = jnp.exp(rate * later) * masked
        total = jnp.sum(masked, axis=1, keepdims=True)
        all_ref[b] = jnp.broadcast_to(jnp.exp(rate * total), (heads, block))
        high = state_ref[b].astype(BF16)
        high_ref[b] = high
        low_ref[b] = (state_ref[b] - high.astype(F32)).astype(BF16)


def prepare(block_step, lengths, decay_log, state):
    steps = jnp.swapaxes(block_step, 1, 2)
    flat = state.reshape(state.shape[0], -1, state.shape[3])
    shape = jax.ShapeDtypeStruct
    whole = pl.BlockSpec(memory_space=pltpu.VMEM)
    return pl.pallas_call(
        prepare_body,
        in_specs=[whole, pl.BlockSpec(memory_space=pltpu.SMEM), whole, whole],
        out_shape=(
            shape(steps.shape, F32),
            shape(steps.shape, F32),
            shape(flat.shape, BF16),
            shape(flat.shape, BF16),
        ),
    )(steps, lengths, decay_log[:, None], flat)


def on_chip(x):
    return pltpu.with_memory_space_constraint(x, pltpu.VMEM)


def silu(v):
    return v / (1.0 + jnp.exp(-v))


def mix_body(
    arrived_ref,
    conv_input_ref,
    conv_b_ref,
    conv_c_ref,
    tail_input_ref,
    tail_b_ref,
    tail_c_ref,
    bias_ref,
    log_ref,
    faded_ref,
    all_ref,
    high_ref,
    low_ref,
    values_ref,
    keys_ref,
    gain_ref,
    out_ref,
):
    seqs, heads = faded_ref.shape[:2]
    channels = gain_ref.shape[1]
    states = conv_c_ref.shape[1]
    n_state = high_ref.shape[2]
    per_group = heads * n_state // states
    total = jnp.sum(arrived_ref[...].astype(F32), axis=0)
    tail = total[:, 2 * channels + 2 * states :]
    lane = lax.broadcasted_iota(jnp.int32, tail.shape, 1)
    is_square = (lane == 2 * heads) | (lane == 2 * heads + 1)
    squares = jnp.sum(jnp.where(is_square, tail, 0.0), axis=1, keepdims=True)
    inverse = lax.rsqrt(squares / D + EPS)
    steps = (tail + pltpu.roll(tail, tail.shape[1] - heads, 1)) * inverse
    gate = silu(total[:, :channels] * inverse)

    def convolved(at, weights, history):
        summed = weights[TAPS - 1 :] * (total[:, at : at + weights.shape[1]] * inverse)
        for k in range(TAPS - 1):
            summed = summed + weights[k : k + 1] * history[k].astype(F32)
        return silu(summed)

    current = convolved(channels, conv_input_ref, tail_input_ref)
    b_now = convolved(2 * channels, conv_b_ref, tail_b_ref)
    c_now = convolved(2 * channels + states, conv_c_ref, tail_c_ref)

    rate = -jnp.exp(log_ref[...])
    head = lax.broadcasted_iota(jnp.int32, (heads, LANES), 0)
    column = lax.broadcasted_iota(jnp.int32, (heads, LANES), 1)
    key_head = lax.broadcasted_iota(jnp.int32, (heads, states), 0)
    key_lane = lax.broadcasted_iota(jnp.int32, (heads, states), 1)
    own_keys = key_lane // n_state == key_head // per_group
    out_head = lax.broadcasted_iota(jnp.int32, (heads, channels), 0)
    out_lane = lax.broadcasted_iota(jnp.int32, (heads, channels), 1)
    own_lanes = out_lane // HEAD_DIM == out_head
    head_state = lax.broadcasted_iota(jnp.int32, (heads, n_state), 0)

    def by_head(row):
        out = jnp.zeros((heads, n_state), F32)
        for g in range(states // n_state):
            part = row[:, g * n_state : (g + 1) * n_state]
            out = jnp.where(head_state // per_group == g, part, out)
        return out

    rows = []
    for b in range(seqs):
        one = slice(b, b + 1)
        step = jnp.sum(jnp.where(column == head, steps[one], 0.0), axis=1, keepdims=True)
        step = step + bias_ref[...]
        step = jnp.maximum(step, 0.0) + jnp.log1p(jnp.exp(-jnp.abs(step)))
        fade = jnp.exp(rate * step)
        query = jnp.where(own_keys, c_now[one], 0.0).astype(BF16)
        scores = contract_last(query, keys_ref[b])
        weights = (faded_ref[b] * fade * scores).astype(BF16)
        mixed = jnp.dot(weights, values_ref[b], preferred_element_type=F32)
        c_heads = by_head(c_now[one])
        c_high = c_heads.astype(BF16)
        c_low = (c_heads - c_high.astype(F32)).astype(BF16)
        readout = contract_last(c_high, high_ref[b])
        readout = readout + contract_last(c_low, high_ref[b])
        readout = readout + contract_last(c_high, low_ref[b])
        own = step * jnp.sum(c_heads * by_head(b_now[one]), axis=1, keepdims=True)
        carried = fade * all_ref[b][:, :1]
        mixed = mixed + carried * readout + own * current[one]
        rows.append(jnp.sum(jnp.where(own_lanes, mixed, 0.0), axis=0, keepdims=True))
    mixed = jnp.concatenate(rows, axis=0) * gate
    squares = jnp.sum(mixed * mixed, axis=1, keepdims=True)
    high = squares.astype(BF16).astype(F32)
    words = jnp.where(lane == 0, high, jnp.where(lane == 1, squares - high, 0.0))
    row = jnp.concatenate([mixed * gain_ref[...], words], axis=1).astype(BF16)
    for k in range(out_ref.shape[0]):
        out_ref[k] = row


def mix(arrived, convs, tails, step_bias, decay_log, prepared, values, keys, gain, copies):
    tails = [jnp.swapaxes(t, 0, 1) for t in tails]
    columns = (step_bias[:, None], decay_log[:, None])
    operands = (arrived, *convs, *tails, *columns, *prepared, values, keys, gain[None])
    width = gain.shape[0] + LANES
    return pl.pallas_call(
        mix_body,
        out_shape=jax.ShapeDtypeStruct((copies, values.shape[0], width), BF16),
    )(*[on_chip(x) for x in operands])


def layer(
    inputs,
    gain_in,
    w_gate,
    w_input,
    w_bproj,
    w_cproj,
    w_step,
    conv_input,
    conv_bproj,
    conv_cproj,
    tail_input,
    tail_bproj,
    tail_cproj,
    step_bias,
    decay_log,
    block_input,
    block_bproj,
    block_step,
    lengths,
    state,
    gain_mix,
    w_out,
    gain_mlp,
    w_up,
    w_down,
):
    core = lax.axis_index("tp")
    n_kv, n_dp, n_tp = lax.axis_size("kv"), lax.axis_size("dp"), lax.axis_size("tp")
    rows = inputs.shape[0]
    sent = project(inputs, gain_in, (w_gate, w_input, w_bproj, w_cproj), w_step, n_kv)
    arrived = lax.all_to_all(sent, "kv", 0, 0, tiled=True)
    prepared = prepare(block_step, lengths, decay_log, state)
    whole = mix(
        arrived,
        (conv_input, conv_bproj, conv_cproj),
        (tail_input, tail_bproj, tail_cproj),
        step_bias,
        decay_log,
        prepared,
        block_input,
        block_bproj,
        gain_mix,
        n_kv * n_tp,
    )
    width = gain_mix.shape[0]
    whole = lax.all_to_all(whole, ("kv", "tp"), 0, 0, tiled=True)

    out_mine, out_other = exchanged(w_out, 1, core)
    up_mine, up_other = exchanged(w_up, 1, core)
    up_gain = jnp.concatenate([gain_mlp, from_partner(gain_mlp)])
    column_count = out_mine.shape[1]
    residual = lax.dynamic_slice_in_dim(inputs, core * column_count, column_count, 1)
    whole, out_mine, out_other, up_mine, up_other, up_gain, residual = lax.optimization_barrier(
        (whole, out_mine, out_other, up_mine, up_other, up_gain, residual)
    )
    out_weight = jnp.concatenate([out_mine, out_other], axis=0)
    up_weight = jnp.concatenate([up_mine, up_other], axis=0)

    whole = whole.reshape(n_kv, n_tp, rows // n_kv, -1)
    whole = jnp.moveaxis(whole, 1, 0).reshape(n_tp, rows, -1)
    total_sq = jnp.sum(whole[:, :, width : width + 2].astype(F32), axis=(0, 2))
    halves = whole[:, :, :width]
    channels = jnp.concatenate(
        [
            lax.dynamic_index_in_dim(halves, core, 0, keepdims=False),
            lax.dynamic_index_in_dim(halves, 1 - core, 0, keepdims=False),
        ],
        axis=1,
    )
    mixed_in = jnp.dot(channels, out_weight, preferred_element_type=F32)
    mixed_in = mixed_in * lax.rsqrt(total_sq / SSM_WIDTH + EPS)[:, None]
    hidden = (residual.astype(F32) + mixed_in).astype(BF16)

    all_hidden = to_everyone(hidden, ("dp", "tp")).reshape(n_dp, n_tp, rows, -1)
    seqs = n_dp * rows
    all_hidden = jnp.moveaxis(all_hidden, 1, 0).reshape(n_tp, seqs, -1)
    all_hidden = jnp.concatenate(
        [
            lax.dynamic_index_in_dim(all_hidden, core, 0, keepdims=False),
            lax.dynamic_index_in_dim(all_hidden, 1 - core, 0, keepdims=False),
        ],
        axis=1,
    ).astype(F32)
    row_sq = jnp.sum(all_hidden * all_hidden, axis=1)
    lifted = (all_hidden * up_gain).astype(BF16)
    raised = lax.dot_general(
        up_weight, lifted, (((0,), (1,)), ((), ())), preferred_element_type=F32
    ).astype(BF16)
    arrived = lax.all_to_all(raised.reshape(n_kv, -1, seqs), "kv", 0, 0, tiled=True)
    down_mine, down_other = exchanged(w_down, 0, core)
    down_weight = in_core_order(down_mine, down_other, core, 1)
    down_weight = jnp.pad(down_weight.reshape(n_kv, -1, down_weight.shape[1]), ((0, 0), (0, SPARE), (0, 0)))
    down_weight = down_weight.reshape(-1, down_weight.shape[2])
    words = jnp.concatenate(
        [*[w[None] for w in two_words(row_sq)], jnp.zeros((SPARE - 2, seqs), BF16)], axis=0
    )
    arrived, down_weight, words = lax.optimization_barrier((arrived, down_weight, words))
    shares = jnp.sum(arrived.astype(F32), axis=0)
    units = jnp.square(jax.nn.relu(shares)).astype(BF16)
    hidden_units = lax.all_gather(jnp.concatenate([units, words], axis=0), "kv", axis=0, tiled=True)
    lowered = lax.dot_general(
        hidden_units, down_weight, (((0,), (0,)), ((), ())), preferred_element_type=F32
    ).astype(BF16)
    lowered = lowered.reshape(n_dp, rows, n_tp, -1)
    lowered = jnp.moveaxis(lowered, 2, 1).reshape(n_dp * n_tp, rows, -1)
    lowered = lax.all_to_all(lowered, ("dp", "tp"), 0, 0, tiled=True)
    lowered = jnp.sum(lowered.astype(F32), axis=0)
    unit_count = units.shape[0]
    sq_words = hidden_units.reshape(n_kv, -1, seqs)[:, unit_count : unit_count + 2]
    sq_sum = jnp.sum(sq_words.astype(F32), axis=(0, 1))
    sq_sum = lax.dynamic_slice_in_dim(sq_sum, lax.axis_index("dp") * rows, rows, 0)
    return (hidden.astype(F32) + lowered / (sq_sum / D + EPS)[:, None]).astype(BF16)


def solution(mesh):
    return jax.shard_map(
        layer,
        mesh=mesh,
        in_specs=(
            P(("grp", "dp"), "kv"),
            P("kv"),
            P("kv", "tp"),
            P("kv", "tp"),
            P("kv", "tp"),
            P("kv", "tp"),
            P("kv", "tp"),
            P(None, "tp"),
            P(None, "tp"),
            P(None, "tp"),
            P(("grp", "dp", "kv"), None, "tp"),
            P(("grp", "dp", "kv"), None, "tp"),
            P(("grp", "dp", "kv"), None, "tp"),
            P("tp"),
            P("tp"),
            P(("grp", "dp", "kv"), None, "tp"),
            P(("grp", "dp", "kv"), None, "tp"),
            P(("grp", "dp", "kv"), None, "tp"),
            P(("grp", "dp", "kv")),
            P(("grp", "dp", "kv"), "tp", None, None),
            P("tp"),
            P("tp", "kv"),
            P(("kv", "tp")),
            P(("kv", "tp"), "dp"),
            P("dp", ("kv", "tp")),
        ),
        out_specs=P(("grp", "dp"), ("kv", "tp")),
        check_vma=False,
    )
```

time: 201 us -> 194 us (0.965)
  waiting for transfers between devices: 55.3 us -> 48.3 us
  Pallas kernels: 0 us -> 6.6 us
  matrix products: 7.82 us -> 1.75 us
  starting transfers between devices: 76.7 us -> 80.6 us
  blocking collectives: 49.5 us -> 46.2 us
  other arithmetic: 4.62 us -> 1.63 us
  local copies, waits for them, and re-layouts: 5.53 us -> 7.84 us
    all_to_all x4, waiting for transfers between devices: 55.3 us -> 46.1 us  [the longest x1 21.3 us: layer(): lax.all_to_all(raised.reshape(n_kv, -1, seqs), 'kv', 0, 0, tiled=True)]
    pallas_call x0 -> x3, Pallas kernels: none -> 6.6 us  [the longest x1 2.54 us: prepare(): pl.pallas_call(prepare_body, in_specs=[whole, pl.BlockSpec(memory_space=p...]
    dot_general x11 -> x3, matrix products: 7.82 us -> 1.75 us  [the longest x1 1.16 us: layer(): lax.dot_general(up_weight, lifted, (((0,), (1,)), ((), ())), preferred_el...]
    unnamed x45 -> x43, local copies, waits for them, and re-layouts: 0.54 us -> 5.56 us
    all_to_all x1, blocking collectives: 21.7 us -> 17.6 us  [to_everyone(): lax.all_to_all(jnp.broadcast_to(shard[None], (size, *shard.shape)), axes,...]
    all_to_all x4, starting transfers between devices: 67.7 us -> 71.5 us  [the longest x1 44.2 us: layer(): arrived = lax.all_to_all(sent, 'kv', 0, 0, tiled=True)]
    ppermute x4, waiting for transfers between devices: 0.01 us -> 2.18 us  [from_partner(): return lax.ppermute(x, 'tp', [(i, (i + 1) % size) for i in range(size)])]
  transfers between devices with their start and end apart: 8 -> 8, of which waited for: 4 -> 6; matrix products, arithmetic and copies ran while one was open for 1% -> 1% of each run, Pallas kernels for 0% -> 1%
where the time goes in v4:
time: 194 us; the launch traced here: 193 us
  starting transfers between devices  80.6 us (42%)
  waiting for transfers between devices  48.3 us (25%)
  blocking collectives  46.2 us (24%)
  local copies, waits for them, and re-layouts  7.84 us (4%)
  Pallas kernels  6.6 us (3%)
    all_to_all x1, starting transfers between devices, layer(): arrived = lax.all_to_all(sent, 'kv', 0, 0, tiled=True)  44.2 us
    all_gather x1, blocking collectives, layer(): lax.all_gather(jnp.concatenate([units, words], axis=0), 'kv', axis=0, til...  28.7 us
    all_to_all x1, waiting for transfers between devices, layer(): lax.all_to_all(raised.reshape(n_kv, -1, seqs), 'kv', 0, 0, tiled=True)  21.3 us
    all_to_all x1, blocking collectives, to_everyone(): lax.all_to_all(jnp.broadcast_to(shard[None], (size, *shard.shape)), axes,...  17.6 us
    all_to_all x1, starting transfers between devices, layer(): lowered = lax.all_to_all(lowered, ('dp', 'tp'), 0, 0, tiled=True)  12.6 us
    all_to_all x1, starting transfers between devices, layer(): whole = lax.all_to_all(whole, ('kv', 'tp'), 0, 0, tiled=True)  10.6 us
    all_to_all x1, waiting for transfers between devices, layer(): lowered = lax.all_to_all(lowered, ('dp', 'tp'), 0, 0, tiled=True)  9.14 us
    ppermute x4, starting transfers between devices, from_partner(): return lax.ppermute(x, 'tp', [(i, (i + 1) % size) for i in range(size)])  9.11 us
  transfers between devices with their start and end apart: 8, of which 6 were waited for; matrix products, arithmetic and copies ran while one was open for 1% of the time, Pallas kernels for 1%

profile of v4, /device:TPU:65, one launch (start us, length us, event | category | flops | bytes accessed | tf_op | source)
XLA Modules:
  0.0 193.4 jit_solution(1407568878632482734)
XLA Ops:
  0.0 2.5 %shard_map.235 = bf16[16,2,3200]{2,1,0:T(2,128)(2,1)} custom-call(bf16[32,256]{1,0:T(8,128)(2,1)} %x_ref.1, f32[1,256]{1,0:T(1,128)} %bitcast.54, bf16[256,1024]{1,0:T(8,128)(2,1)} %gate_ref.1, bf16[256,1024]{1,0:T(8,128)(2,1)} %input_ref.1, bf16[256,512]{1,0:T(8,128)(2,1)} %b_ref.1, bf16[256,512]{1,0:T(8,128)(2,1)} %c_ref.1, bf16[16,256]{1,0:T(8,128)(2,1)} %bitcast.52), custom_call_target="tpu_custom_call" | custom-call | tf_op jit(solution)/shard_map/pallas_call | solution.py:88
  2.5 44.2 %all-to-all-start = ((bf16[16,2,3200]{2,1,0:T(2,128)(2,1)}), bf16[16,2,3200]{2,1,0:T(2,128)(2,1)S(1)}, u32[]{:S(2)}, u32[]{:S(2)}) async-start(bf16[16,2,3200]{2,1,0:T(2,128)(2,1)} %shard_map.235), calls=%async_computation | async-start | bytes 409600 | tf_op jit(solution)/shard_map/all_to_all | solution.py:272
  46.8 0.0 copy-start.18
  46.8 0.6 copy-done.18
  47.4 0.1 copy.54.bias_ref
  47.5 0.7 copy-done.19
  48.2 0.7 copy.55.log_ref
  48.8 0.0 copy-start.9
  48.9 0.0 copy-start.12
  48.9 0.0 copy-start.13
  48.9 2.5 %shard_map.236 = (f32[2,16,128]{2,1,0:T(8,128)}, f32[2,16,128]{2,1,0:T(8,128)}, bf16[2,1024,128]{2,1,0:T(8,128)(2,1)}, bf16[2,1024,128]{2,1,0:T(8,128)(2,1)}) custom-call(f32[2,16,128]{2,1,0:T(8,128)} %bitcast.51, s32[2]{0:T(128)} %lengths_ref.1, f32[16,1]{1,0:T(8,128)} %copy.55.log_ref, f32[2,1024,128]{2,1,0:T(8,128)} %bitcast.41), custom_call_target="tpu_custom_call" | custom-call | tf_op jit(solution)/shard_map/pallas_call | solution.py:119
  51.4 7.5 %all-to-all-done.arrived_ref = bf16[16,2,3200]{2,1,0:T(2,128)(2,1)S(1)} async-done(((bf16[16,2,3200]{2,1,0:T(2,128)(2,1)}), bf16[16,2,3200]{2,1,0:T(2,128)(2,1)S(1)}, u32[]{:S(2)}, u32[]{:S(2)}) %all-to-all-start) | async-done | bytes 204832 | tf_op jit(solution)/shard_map/all_to_all | solution.py:272
  59.0 0.6 copy-done.11
  59.6 1.0 copy-done.1
  60.7 1.0 copy-done.2
  61.7 0.7 copy-done.6
  62.4 0.7 copy-done.7
  63.1 1.5 shard_map.237
  64.7 10.6 %all-to-all-start.1 = ((bf16[32,2,1152]{2,1,0:T(2,128)(2,1)}), bf16[32,2,1152]{2,1,0:T(2,128)(2,1)S(1)}, u32[]{:S(2)}, u32[]{:S(2)}) async-start(bf16[32,2,1152]{2,1,0:T(2,128)(2,1)} %shard_map.237), calls=%async_computation.1 | async-start | bytes 294912 | tf_op jit(solution)/shard_map/all_to_all | solution.py:287
  75.3 0.0 copy-start.15
  75.3 2.8 %collective-permute-start = (bf16[1024,128]{1,0:T(8,128)(2,1)S(1)}, bf16[1024,128]{1,0:T(8,128)(2,1)S(1)}, u32[]{:S(2)}, u32[]{:S(2)}) collective-permute-start(bf16[1024,128]{1,0:T(8,128)(2,1)S(1)} %get-tuple-element.37), channel_id=1, source_target_pairs={{0,1},{1,0},{2,3},{3,2},{4,5},{5,4},{6,7},{7,6},{8,9},{9,8},{10,11... | collective-permute-start | bytes 786440 | tf_op jit(solution)/shard_map/ppermute | solution.py:34
  78.2 2.0 %collective-permute-start.1 = (bf16[128,1024]{1,0:T(8,128)(2,1)S(1)}, bf16[128,1024]{1,0:T(8,128)(2,1)S(1)}, u32[]{:S(2)}, u32[]{:S(2)}) collective-permute-start(bf16[128,1024]{1,0:T(8,128)(2,1)S(1)} %get-tuple-element.35), channel_id=1, source_target_pairs={{0,1},{1,0},{2,3},{3,2},{4,5},{5,4},{6,7},{7,6},{8,9},{9,8},{10,11... | collective-permute-start | bytes 786440 | tf_op jit(solution)/shard_map/ppermute | solution.py:34
  80.2 2.4 %collective-permute-start.2 = (f32[128]{0:T(128)S(1)}, f32[128]{0:T(128)S(1)}, u32[]{:S(2)}, u32[]{:S(2)}) collective-permute-start(f32[128]{0:T(128)S(1)} %copy-done.20), channel_id=1, source_target_pairs={{0,1},{1,0},{2,3},{3,2},{4,5},{5,4},{6,7},{7,6},{8,9},{9,8},{10,11... | collective-permute-start | bytes 1544 | tf_op jit(solution)/shard_map/ppermute | solution.py:34
  82.6 0.8 collective-permute-done.2
  83.4 8.1 %all-to-all-done.1 = bf16[32,2,1152]{2,1,0:T(2,128)(2,1)S(1)} async-done(((bf16[32,2,1152]{2,1,0:T(2,128)(2,1)}), bf16[32,2,1152]{2,1,0:T(2,128)(2,1)S(1)}, u32[]{:S(2)}, u32[]{:S(2)}) %all-to-all-start.1) | async-done | bytes 147488 | tf_op jit(solution)/shard_map/all_to_all | solution.py:287
  91.6 0.1 copy.56
  91.7 0.3 convert_reduce_fusion.3
  92.0 0.1 slice.12
  92.1 0.3 constant_dynamic-slice_fusion.3
  92.4 0.2 add_convert_fusion.1
  92.7 17.6 %all_to_all.25 = bf16[16,32,128]{2,1,0:T(8,128)(2,1)S(1)} all-to-all(bf16[16,32,128]{2,1,0:T(8,128)(2,1)S(1)} %broadcast_in_dim.31), channel_id=1, replica_groups=mesh['grp'=2,'dp'=8,'kv'=16,'tp'=2] {'dp','tp'}, dimensions={0} | all-to-all | bytes 262144 | tf_op jit(solution)/shard_map/all_to_all | solution.py:27
  110.3 1.2 convolution_convert_fusion
  111.5 4.1 %all-to-all-start.3 = ((bf16[16,64,256]{2,1,0:T(8,128)(2,1)}), bf16[16,64,256]{2,1,0:T(8,128)(2,1)S(1)}, u32[]{:S(2)}, u32[]{:S(2)}) async-start(bf16[16,64,256]{2,1,0:T(8,128)(2,1)} %bitcast.19), calls=%async_computation.3 | async-start | bytes 1048576 | tf_op jit(solution)/shard_map/all_to_all | solution.py:330
  115.7 2.0 %collective-permute-start.3 = (bf16[1024,128]{1,0:T(8,128)(2,1)S(1)}, bf16[1024,128]{1,0:T(8,128)(2,1)S(1)}, u32[]{:S(2)}, u32[]{:S(2)}) collective-permute-start(bf16[1024,128]{1,0:T(8,128)(2,1)S(1)} %get-tuple-element.34), channel_id=1, source_target_pairs={{0,1},{1,0},{2,3},{3,2},{4,5},{5,4},{6,7},{7,6},{8,9},{9,8},{10,11... | collective-permute-start | bytes 786440 | tf_op jit(solution)/shard_map/ppermute | solution.py:34
  117.7 0.1 pad.9.clone
  117.8 1.4 collective-permute-done.3
  119.2 0.2 maximum_select_fusion
  119.4 0.1 fusion.7
  119.6 0.1 maximum_maximum_fusion
  119.6 21.3 %all-to-all-done.3 = bf16[16,64,256]{2,1,0:T(8,128)(2,1)S(1)} async-done(((bf16[16,64,256]{2,1,0:T(8,128)(2,1)}), bf16[16,64,256]{2,1,0:T(8,128)(2,1)S(1)}, u32[]{:S(2)}, u32[]{:S(2)}) %all-to-all-start.3) | async-done | bytes 524320 | tf_op jit(solution)/shard_map/all_to_all | solution.py:330
  141.0 0.1 convert_reduce_fusion
  141.1 28.7 %all_gather.3 = bf16[1152,256]{1,0:T(8,128)(2,1)S(1)} all-gather(bf16[72,256]{1,0:T(8,128)(2,1)S(1)} %pad_maximum_fusion.2), channel_id=1, replica_groups=mesh['grp'=2,'dp'=8,'kv'=16,'tp'=2] {'kv'}, dimensions={0}, use_global_device_ids=true | all-gather | bytes 626688 | tf_op jit(solution)/shard_map/all_gather | solution.py:341
  169.7 0.4 convolution_convert_fusion.1
  170.2 0.7 copy.58
  170.8 12.6 %all-to-all-start.4 = ((bf16[16,32,128]{2,1,0:T(8,128)(2,1)}), bf16[16,32,128]{2,1,0:T(8,128)(2,1)S(1)}, u32[]{:S(2)}, u32[]{:S(2)}) async-start(bf16[16,32,128]{2,1,0:T(8,128)(2,1)} %bitcast.25), calls=%async_computation.4 | async-start | bytes 262144 | tf_op jit(solution)/shard_map/all_to_all | solution.py:347
  183.5 0.1 multiply_add_fusion
  183.6 9.1 %all-to-all-done.4 = bf16[16,32,128]{2,1,0:T(8,128)(2,1)S(1)} async-done(((bf16[16,32,128]{2,1,0:T(8,128)(2,1)}), bf16[16,32,128]{2,1,0:T(8,128)(2,1)S(1)}, u32[]{:S(2)}, u32[]{:S(2)}) %all-to-all-start.4) | async-done | bytes 131104 | tf_op jit(solution)/shard_map/all_to_all | solution.py:347
  192.7 0.7 add_convert_fusion
  (51 shorter events, 0.5 us)
Async XLA Ops:
  2.5 56.4 %all-to-all-start = ((bf16[16,2,3200]{2,1,0:T(2,128)(2,1)}), bf16[16,2,3200]{2,1,0:T(2,128)(2,1)S(1)}, u32[]{:S(2)}, u32[]{:S(2)}) async-start(bf16[16,2,3200]{2,1,0:T(2,128)(2,1)} %shard_map.235), calls=%async_computation | async-start | bytes 409600 | tf_op jit(solution)/shard_map/all_to_all | solution.py:272
  46.8 0.7 copy-start.18
  47.5 0.7 copy-start.19
  48.8 10.1 %copy-start = (bf16[2,128,1024]{2,1,0:T(8,128)(2,1)S(1)}, bf16[2,128,1024]{2,1,0:T(8,128)(2,1)}, u32[]{:S(2)}) copy-start(bf16[2,128,1024]{2,1,0:T(8,128)(2,1)} %values_ref.1) | copy-start | bytes 1572868
  48.8 10.1 %copy-start.3 = (bf16[2,128,512]{2,1,0:T(8,128)(2,1)S(1)}, bf16[2,128,512]{2,1,0:T(8,128)(2,1)}, u32[]{:S(2)}) copy-start(bf16[2,128,512]{2,1,0:T(8,128)(2,1)} %keys_ref.1) | copy-start | bytes 786436
  48.8 10.1 %copy-start.5 = (f32[4,1024]{1,0:T(4,128)S(1)}, f32[4,1024]{1,0:T(4,128)}, u32[]{:S(2)}) copy-start(f32[4,1024]{1,0:T(4,128)} %conv_input_ref.1) | copy-start | bytes 49156
  48.8 10.1 %copy-start.8 = (bf16[2,3,1024]{2,0,1:T(2,128)(2,1)S(1)}, bf16[2,3,1024]{2,0,1:T(2,128)(2,1)}, u32[]{:S(2)}) copy-start(bf16[2,3,1024]{2,0,1:T(2,128)(2,1)} %param.35) | copy-start | bytes 36868
  48.8 10.1 %copy-start.9 = (f32[4,512]{1,0:T(4,128)S(1)}, f32[4,512]{1,0:T(4,128)}, u32[]{:S(2)}) copy-start(f32[4,512]{1,0:T(4,128)} %conv_b_ref.1) | copy-start | bytes 24580
  48.9 10.1 %copy-start.10 = (f32[4,512]{1,0:T(4,128)S(1)}, f32[4,512]{1,0:T(4,128)}, u32[]{:S(2)}) copy-start(f32[4,512]{1,0:T(4,128)} %conv_c_ref.1) | copy-start | bytes 24580
  48.9 10.1 %copy-start.12 = (bf16[2,3,512]{2,0,1:T(2,128)(2,1)S(1)}, bf16[2,3,512]{2,0,1:T(2,128)(2,1)}, u32[]{:S(2)}) copy-start(bf16[2,3,512]{2,0,1:T(2,128)(2,1)} %param.37) | copy-start | bytes 18436
  48.9 10.1 %copy-start.13 = (f32[1024]{0:T(1024)S(1)}, f32[1024]{0:T(1024)}, u32[]{:S(2)}) copy-start(f32[1024]{0:T(1024)} %param.45) | copy-start | bytes 12292
  51.4 7.6 %copy-start.4 = (f32[16,1]{1,0:T(8,128)S(1)}, f32[16,1]{1,0:T(8,128)}, u32[]{:S(2)}) copy-start(f32[16,1]{1,0:T(8,128)} %copy.55.log_ref) | copy-start | bytes 196
  58.9 0.7 copy-start.11
  59.6 1.0 copy-start.1
  60.7 1.0 copy-start.2
  61.7 0.7 copy-start.6
  62.4 0.7 copy-start.7
  63.1 12.1 %copy-start.14 = (bf16[1024,256]{1,0:T(8,128)(2,1)S(1)}, bf16[1024,256]{1,0:T(8,128)(2,1)}, u32[]{:S(2)}) copy-start(bf16[1024,256]{1,0:T(8,128)(2,1)} %param.46) | copy-start | bytes 1572868
  64.7 26.9 %all-to-all-start.1 = ((bf16[32,2,1152]{2,1,0:T(2,128)(2,1)}), bf16[32,2,1152]{2,1,0:T(2,128)(2,1)S(1)}, u32[]{:S(2)}, u32[]{:S(2)}) async-start(bf16[32,2,1152]{2,1,0:T(2,128)(2,1)} %shard_map.237), calls=%async_computation.1 | async-start | bytes 294912 | tf_op jit(solution)/shard_map/all_to_all | solution.py:287
  75.3 2.8 %copy-start.15 = (bf16[128,2048]{1,0:T(8,128)(2,1)S(1)}, bf16[128,2048]{1,0:T(8,128)(2,1)}, u32[]{:S(2)}) copy-start(bf16[128,2048]{1,0:T(8,128)(2,1)} %param.48) | copy-start | bytes 1572868
  75.3 8.1 %collective-permute-start = (bf16[1024,128]{1,0:T(8,128)(2,1)S(1)}, bf16[1024,128]{1,0:T(8,128)(2,1)S(1)}, u32[]{:S(2)}, u32[]{:S(2)}) collective-permute-start(bf16[1024,128]{1,0:T(8,128)(2,1)S(1)} %get-tuple-element.37), channel_id=1, source_target_pairs={{0,1},{1,0},{2,3},{3,2},{4,5},{5,4},{6,7},{7,6},{8,9},{9,8},{10,11... | collective-permute-start | bytes 786440 | tf_op jit(solution)/shard_map/ppermute | solution.py:34
  78.1 4.5 %copy-start.17 = (bf16[32,256]{1,0:T(8,128)(2,1)S(1)}, bf16[32,256]{1,0:T(8,128)(2,1)}, u32[]{:S(2)}) copy-start(bf16[32,256]{1,0:T(8,128)(2,1)} %x_ref.1) | copy-start | bytes 49156
  78.2 2.0 %copy-start.20 = (f32[128]{0:T(128)S(1)}, f32[128]{0:T(128)}, u32[]{:S(2)}) copy-start(f32[128]{0:T(128)} %param.47) | copy-start | bytes 1540
  78.2 5.2 %collective-permute-start.1 = (bf16[128,1024]{1,0:T(8,128)(2,1)S(1)}, bf16[128,1024]{1,0:T(8,128)(2,1)S(1)}, u32[]{:S(2)}, u32[]{:S(2)}) collective-permute-start(bf16[128,1024]{1,0:T(8,128)(2,1)S(1)} %get-tuple-element.35), channel_id=1, source_target_pairs={{0,1},{1,0},{2,3},{3,2},{4,5},{5,4},{6,7},{7,6},{8,9},{9,8},{10,11... | collective-permute-start | bytes 786440 | tf_op jit(solution)/shard_map/ppermute | solution.py:34
  80.2 3.2 %collective-permute-start.2 = (f32[128]{0:T(128)S(1)}, f32[128]{0:T(128)S(1)}, u32[]{:S(2)}, u32[]{:S(2)}) collective-permute-start(f32[128]{0:T(128)S(1)} %copy-done.20), channel_id=1, source_target_pairs={{0,1},{1,0},{2,3},{3,2},{4,5},{5,4},{6,7},{7,6},{8,9},{9,8},{10,11... | collective-permute-start | bytes 1544 | tf_op jit(solution)/shard_map/ppermute | solution.py:34
  111.5 4.2 %copy-start.16 = (bf16[2048,128]{1,0:T(8,128)(2,1)S(1)}, bf16[2048,128]{1,0:T(8,128)(2,1)}, u32[]{:S(2)}) copy-start(bf16[2048,128]{1,0:T(8,128)(2,1)} %param.49) | copy-start | bytes 1572868
  111.5 29.5 %all-to-all-start.3 = ((bf16[16,64,256]{2,1,0:T(8,128)(2,1)}), bf16[16,64,256]{2,1,0:T(8,128)(2,1)S(1)}, u32[]{:S(2)}, u32[]{:S(2)}) async-start(bf16[16,64,256]{2,1,0:T(8,128)(2,1)} %bitcast.19), calls=%async_computation.3 | async-start | bytes 1048576 | tf_op jit(solution)/shard_map/all_to_all | solution.py:330
  115.7 3.5 %collective-permute-start.3 = (bf16[1024,128]{1,0:T(8,128)(2,1)S(1)}, bf16[1024,128]{1,0:T(8,128)(2,1)S(1)}, u32[]{:S(2)}, u32[]{:S(2)}) collective-permute-start(bf16[1024,128]{1,0:T(8,128)(2,1)S(1)} %get-tuple-element.34), channel_id=1, source_target_pairs={{0,1},{1,0},{2,3},{3,2},{4,5},{5,4},{6,7},{7,6},{8,9},{9,8},{10,11... | collective-permute-start | bytes 786440 | tf_op jit(solution)/shard_map/ppermute | solution.py:34
  170.8 21.9 %all-to-all-start.4 = ((bf16[16,32,128]{2,1,0:T(8,128)(2,1)}), bf16[16,32,128]{2,1,0:T(8,128)(2,1)S(1)}, u32[]{:S(2)}, u32[]{:S(2)}) async-start(bf16[16,32,128]{2,1,0:T(8,128)(2,1)} %bitcast.25), calls=%async_computation.4 | async-start | bytes 262144 | tf_op jit(solution)/shard_map/all_to_all | solution.py:347

commit v5 on v4

--- a/solution.py
+++ b/solution.py
@@ -91,7 +91,8 @@
     )(inputs, gain_in[None], *matrices, w_step.T)
 
 
-def prepare_body(steps_ref, lengths_ref, log_ref, state_ref, faded_ref, all_ref, high_ref, low_ref):
+def prepare_body(steps_ref, lengths_ref, log_ref, state_ref, *refs):
+    faded_ref, all_ref, high_ref, low_ref = refs[-4:]
     seqs, heads, block = steps_ref.shape
     rate = -jnp.exp(log_ref[...])
     position = lax.broadcasted_iota(jnp.int32, (heads, block), 1)
@@ -111,21 +112,21 @@
         low_ref[b] = (state_ref[b] - high.astype(F32)).astype(BF16)
 
 
-def prepare(block_step, lengths, decay_log, state):
+def prepare(block_step, lengths, log_column, state, others):
     steps = jnp.swapaxes(block_step, 1, 2)
     flat = state.reshape(state.shape[0], -1, state.shape[3])
-    shape = jax.ShapeDtypeStruct
+    shape = pltpu.VMEM
     whole = pl.BlockSpec(memory_space=pltpu.VMEM)
     return pl.pallas_call(
         prepare_body,
-        in_specs=[whole, pl.BlockSpec(memory_space=pltpu.SMEM), whole, whole],
+        in_specs=[whole, pl.BlockSpec(memory_space=pltpu.SMEM)] + [whole] * (2 + len(others)),
         out_shape=(
             shape(steps.shape, F32),
             shape(steps.shape, F32),
             shape(flat.shape, BF16),
             shape(flat.shape, BF16),
         ),
-    )(steps, lengths, decay_log[:, None], flat)
+    )(steps, lengths, log_column, flat, *others)
 
 
 def on_chip(x):
@@ -227,15 +228,14 @@
         out_ref[k] = row
 
 
-def mix(arrived, convs, tails, step_bias, decay_log, prepared, values, keys, gain, copies):
-    tails = [jnp.swapaxes(t, 0, 1) for t in tails]
-    columns = (step_bias[:, None], decay_log[:, None])
-    operands = (arrived, *convs, *tails, *columns, *prepared, values, keys, gain[None])
-    width = gain.shape[0] + LANES
+def mix(arrived, convs, tails, columns, prepared, values, keys, gain, copies):
+    operands = (on_chip(arrived), *convs, *tails, *columns, *[on_chip(x) for x in prepared])
+    operands += (values, keys, gain)
+    width = gain.shape[1] + LANES
     return pl.pallas_call(
         mix_body,
         out_shape=jax.ShapeDtypeStruct((copies, values.shape[0], width), BF16),
-    )(*[on_chip(x) for x in operands])
+    )(*operands)
 
 
 def layer(
@@ -270,19 +270,13 @@
     rows = inputs.shape[0]
     sent = project(inputs, gain_in, (w_gate, w_input, w_bproj, w_cproj), w_step, n_kv)
     arrived = lax.all_to_all(sent, "kv", 0, 0, tiled=True)
-    prepared = prepare(block_step, lengths, decay_log, state)
-    whole = mix(
-        arrived,
-        (conv_input, conv_bproj, conv_cproj),
-        (tail_input, tail_bproj, tail_cproj),
-        step_bias,
-        decay_log,
-        prepared,
-        block_input,
-        block_bproj,
-        gain_mix,
-        n_kv * n_tp,
-    )
+    convs = [on_chip(x) for x in (conv_input, conv_bproj, conv_cproj)]
+    tails = [on_chip(jnp.swapaxes(x, 0, 1)) for x in (tail_input, tail_bproj, tail_cproj)]
+    columns = [on_chip(x[:, None]) for x in (step_bias, decay_log)]
+    values, keys, gain = [on_chip(x) for x in (block_input, block_bproj, gain_mix[None])]
+    others = (*convs, *tails, columns[0], values, keys, gain)
+    prepared = prepare(block_step, lengths, columns[1], state, others)
+    whole = mix(arrived, convs, tails, columns, prepared, values, keys, gain, n_kv * n_tp)
     width = gain_mix.shape[0]
     whole = lax.all_to_all(whole, ("kv", "tp"), 0, 0, tiled=True)
 

time: 194 us -> 190 us (0.979)
  local copies, waits for them, and re-layouts: 7.84 us -> 2.44 us
  waiting for transfers between devices: 48.3 us -> 50.5 us
    unnamed x43 -> x33, local copies, waits for them, and re-layouts: 5.56 us -> 0.77 us
    all_to_all x1, waiting for transfers between devices: 7.49 us -> 9.68 us  [layer(): arrived = lax.all_to_all(sent, 'kv', 0, 0, tiled=True)]
where the time goes in v5:
time: 190 us
  starting transfers between devices  80.7 us (42%)
  waiting for transfers between devices  50.5 us (27%)
  blocking collectives  46.3 us (24%)
  Pallas kernels  5.72 us (3%)
  local copies, waits for them, and re-layouts  2.44 us (1%)
    all_to_all x1, starting transfers between devices, layer(): arrived = lax.all_to_all(sent, 'kv', 0, 0, tiled=True)  44.4 us
    all_gather x1, blocking collectives, layer(): lax.all_gather(jnp.concatenate([units, words], axis=0), 'kv', axis=0, til...  28.8 us
    all_to_all x1, waiting for transfers between devices, layer(): lax.all_to_all(raised.reshape(n_kv, -1, seqs), 'kv', 0, 0, tiled=True)  21.3 us
    all_to_all x1, blocking collectives, to_everyone(): lax.all_to_all(jnp.broadcast_to(shard[None], (size, *shard.shape)), axes,...  17.6 us
    all_to_all x1, starting transfers between devices, layer(): lowered = lax.all_to_all(lowered, ('dp', 'tp'), 0, 0, tiled=True)  12.6 us
    all_to_all x1, starting transfers between devices, layer(): whole = lax.all_to_all(whole, ('kv', 'tp'), 0, 0, tiled=True)  10.6 us
    all_to_all x1, waiting for transfers between devices, layer(): arrived = lax.all_to_all(sent, 'kv', 0, 0, tiled=True)  9.68 us
    all_to_all x1, waiting for transfers between devices, layer(): lowered = lax.all_to_all(lowered, ('dp', 'tp'), 0, 0, tiled=True)  9.14 us
  transfers between devices with their start and end apart: 8, of which 6 were waited for; matrix products, arithmetic and copies ran while one was open for 1% of the time, Pallas kernels for 1%

profile of v5, /device:TPU:65, one launch (start us, length us, event | category | flops | bytes accessed | tf_op | source)
XLA Modules:
  0.0 189.5 jit_solution(9668117172894302873)
XLA Ops:
  0.0 2.6 %shard_map.235 = bf16[16,2,3200]{2,1,0:T(2,128)(2,1)} custom-call(bf16[32,256]{1,0:T(8,128)(2,1)} %x_ref.1, f32[1,256]{1,0:T(1,128)} %bitcast.58, bf16[256,1024]{1,0:T(8,128)(2,1)} %gate_ref.1, bf16[256,1024]{1,0:T(8,128)(2,1)} %input_ref.1, bf16[256,512]{1,0:T(8,128)(2,1)} %b_ref.1, bf16[256,512]{1,0:T(8,128)(2,1)} %c_ref.1, bf16[16,256]{1,0:T(8,128)(2,1)} %bitcast.56), custom_call_target="tpu_custom_call" | custom-call | tf_op jit(solution)/shard_map/pallas_call | solution.py:88
  2.6 0.0 copy-start.4
  2.6 0.0 copy-start.5
  2.6 0.0 copy-start.6
  2.6 0.0 copy-start.7
  2.7 44.4 %all-to-all-start = ((bf16[16,2,3200]{2,1,0:T(2,128)(2,1)}), bf16[16,2,3200]{2,1,0:T(2,128)(2,1)S(1)}, u32[]{:S(2)}, u32[]{:S(2)}) async-start(bf16[16,2,3200]{2,1,0:T(2,128)(2,1)} %shard_map.235), calls=%async_computation | async-start | bytes 409600 | tf_op jit(solution)/shard_map/all_to_all | solution.py:272
  47.0 0.0 copy-start.2
  47.0 0.1 copy.60.refs_6_.bias_ref
  47.1 0.1 copy.61.log_ref
  47.3 0.5 copy-done.2
  47.7 0.1 copy-done.3
  47.8 0.1 copy-done.8
  47.9 1.6 shard_map.236
  49.5 9.7 %all-to-all-done.arrived_ref = bf16[16,2,3200]{2,1,0:T(2,128)(2,1)S(1)} async-done(((bf16[16,2,3200]{2,1,0:T(2,128)(2,1)}), bf16[16,2,3200]{2,1,0:T(2,128)(2,1)S(1)}, u32[]{:S(2)}, u32[]{:S(2)}) %all-to-all-start) | async-done | bytes 204832 | tf_op jit(solution)/shard_map/all_to_all | solution.py:272
  59.2 1.5 shard_map.237
  60.7 10.6 %all-to-all-start.1 = ((bf16[32,2,1152]{2,1,0:T(2,128)(2,1)}), bf16[32,2,1152]{2,1,0:T(2,128)(2,1)S(1)}, u32[]{:S(2)}, u32[]{:S(2)}) async-start(bf16[32,2,1152]{2,1,0:T(2,128)(2,1)} %shard_map.237), calls=%async_computation.1 | async-start | bytes 294912 | tf_op jit(solution)/shard_map/all_to_all | solution.py:281
  71.3 0.0 copy-start.10
  71.4 2.8 %collective-permute-start = (bf16[1024,128]{1,0:T(8,128)(2,1)S(1)}, bf16[1024,128]{1,0:T(8,128)(2,1)S(1)}, u32[]{:S(2)}, u32[]{:S(2)}) collective-permute-start(bf16[1024,128]{1,0:T(8,128)(2,1)S(1)} %get-tuple-element.37), channel_id=1, source_target_pairs={{0,1},{1,0},{2,3},{3,2},{4,5},{5,4},{6,7},{7,6},{8,9},{9,8},{10,11... | collective-permute-start | bytes 786440 | tf_op jit(solution)/shard_map/ppermute | solution.py:34
  74.2 0.0 copy-start.12
  74.2 0.0 copy-start.15
  74.2 2.0 %collective-permute-start.1 = (bf16[128,1024]{1,0:T(8,128)(2,1)S(1)}, bf16[128,1024]{1,0:T(8,128)(2,1)S(1)}, u32[]{:S(2)}, u32[]{:S(2)}) collective-permute-start(bf16[128,1024]{1,0:T(8,128)(2,1)S(1)} %get-tuple-element.35), channel_id=1, source_target_pairs={{0,1},{1,0},{2,3},{3,2},{4,5},{5,4},{6,7},{7,6},{8,9},{9,8},{10,11... | collective-permute-start | bytes 786440 | tf_op jit(solution)/shard_map/ppermute | solution.py:34
  76.2 2.4 %collective-permute-start.2 = (f32[128]{0:T(128)S(1)}, f32[128]{0:T(128)S(1)}, u32[]{:S(2)}, u32[]{:S(2)}) collective-permute-start(f32[128]{0:T(128)S(1)} %copy-done.15), channel_id=1, source_target_pairs={{0,1},{1,0},{2,3},{3,2},{4,5},{5,4},{6,7},{7,6},{8,9},{9,8},{10,11... | collective-permute-start | bytes 1544 | tf_op jit(solution)/shard_map/ppermute | solution.py:34
  78.7 0.8 collective-permute-done.2
  79.5 0.0 collective-permute-done
  79.5 8.1 %all-to-all-done.1 = bf16[32,2,1152]{2,1,0:T(2,128)(2,1)S(1)} async-done(((bf16[32,2,1152]{2,1,0:T(2,128)(2,1)}), bf16[32,2,1152]{2,1,0:T(2,128)(2,1)S(1)}, u32[]{:S(2)}, u32[]{:S(2)}) %all-to-all-start.1) | async-done | bytes 147488 | tf_op jit(solution)/shard_map/all_to_all | solution.py:281
  87.6 0.1 copy.62
  87.7 0.3 convert_reduce_fusion.3
  88.1 0.1 slice.12
  88.2 0.3 constant_dynamic-slice_fusion.3
  88.5 0.2 add_convert_fusion.1
  88.8 17.6 %all_to_all.25 = bf16[16,32,128]{2,1,0:T(8,128)(2,1)S(1)} all-to-all(bf16[16,32,128]{2,1,0:T(8,128)(2,1)S(1)} %broadcast_in_dim.30), channel_id=1, replica_groups=mesh['grp'=2,'dp'=8,'kv'=16,'tp'=2] {'dp','tp'}, dimensions={0} | all-to-all | bytes 262144 | tf_op jit(solution)/shard_map/all_to_all | solution.py:27
  106.4 1.2 convolution_convert_fusion
  107.6 4.1 %all-to-all-start.3 = ((bf16[16,64,256]{2,1,0:T(8,128)(2,1)}), bf16[16,64,256]{2,1,0:T(8,128)(2,1)S(1)}, u32[]{:S(2)}, u32[]{:S(2)}) async-start(bf16[16,64,256]{2,1,0:T(8,128)(2,1)} %bitcast.19), calls=%async_computation.3 | async-start | bytes 1048576 | tf_op jit(solution)/shard_map/all_to_all | solution.py:324
  111.8 2.0 %collective-permute-start.3 = (bf16[1024,128]{1,0:T(8,128)(2,1)S(1)}, bf16[1024,128]{1,0:T(8,128)(2,1)S(1)}, u32[]{:S(2)}, u32[]{:S(2)}) collective-permute-start(bf16[1024,128]{1,0:T(8,128)(2,1)S(1)} %get-tuple-element.34), channel_id=1, source_target_pairs={{0,1},{1,0},{2,3},{3,2},{4,5},{5,4},{6,7},{7,6},{8,9},{9,8},{10,11... | collective-permute-start | bytes 786440 | tf_op jit(solution)/shard_map/ppermute | solution.py:34
  113.7 0.1 pad.9.clone
  113.8 1.4 collective-permute-done.3
  115.2 0.2 maximum_select_fusion
  115.5 0.1 fusion.7
  115.6 0.1 maximum_maximum_fusion
  115.7 21.3 %all-to-all-done.3 = bf16[16,64,256]{2,1,0:T(8,128)(2,1)S(1)} async-done(((bf16[16,64,256]{2,1,0:T(8,128)(2,1)}), bf16[16,64,256]{2,1,0:T(8,128)(2,1)S(1)}, u32[]{:S(2)}, u32[]{:S(2)}) %all-to-all-start.3) | async-done | bytes 524320 | tf_op jit(solution)/shard_map/all_to_all | solution.py:324
  137.0 0.1 convert_reduce_fusion
  137.1 28.8 %all_gather.3 = bf16[1152,256]{1,0:T(8,128)(2,1)S(1)} all-gather(bf16[72,256]{1,0:T(8,128)(2,1)S(1)} %pad_maximum_fusion.2), channel_id=1, replica_groups=mesh['grp'=2,'dp'=8,'kv'=16,'tp'=2] {'kv'}, dimensions={0}, use_global_device_ids=true | all-gather | bytes 626688 | tf_op jit(solution)/shard_map/all_gather | solution.py:335
  165.9 0.4 convolution_convert_fusion.1
  166.3 0.7 copy.64
  167.0 12.6 %all-to-all-start.4 = ((bf16[16,32,128]{2,1,0:T(8,128)(2,1)}), bf16[16,32,128]{2,1,0:T(8,128)(2,1)S(1)}, u32[]{:S(2)}, u32[]{:S(2)}) async-start(bf16[16,32,128]{2,1,0:T(8,128)(2,1)} %bitcast.25), calls=%async_computation.4 | async-start | bytes 262144 | tf_op jit(solution)/shard_map/all_to_all | solution.py:341
  179.6 0.1 multiply_add_fusion
  179.7 9.1 %all-to-all-done.4 = bf16[16,32,128]{2,1,0:T(8,128)(2,1)S(1)} async-done(((bf16[16,32,128]{2,1,0:T(8,128)(2,1)}), bf16[16,32,128]{2,1,0:T(8,128)(2,1)S(1)}, u32[]{:S(2)}, u32[]{:S(2)}) %all-to-all-start.4) | async-done | bytes 131104 | tf_op jit(solution)/shard_map/all_to_all | solution.py:341
  188.8 0.7 add_convert_fusion
  (41 shorter events, 0.5 us)
Async XLA Ops:
  0.0 47.2 %copy-start = (bf16[2,128,1024]{2,1,0:T(8,128)(2,1)S(1)}, bf16[2,128,1024]{2,1,0:T(8,128)(2,1)}, u32[]{:S(2)}) copy-start(bf16[2,128,1024]{2,1,0:T(8,128)(2,1)} %values_ref.1) | copy-start | bytes 1572868
  2.6 44.4 %copy-start.13 = (f32[16]{0:T(128)S(1)}, f32[16]{0:T(128)}, u32[]{:S(2)}) copy-start(f32[16]{0:T(128)} %param.38) | copy-start | bytes 196
  2.6 44.5 %copy-start.14 = (f32[16]{0:T(128)S(1)}, f32[16]{0:T(128)}, u32[]{:S(2)}) copy-start(f32[16]{0:T(128)} %param.39) | copy-start | bytes 196
  2.6 44.6 %copy-start.1 = (bf16[2,128,512]{2,1,0:T(8,128)(2,1)S(1)}, bf16[2,128,512]{2,1,0:T(8,128)(2,1)}, u32[]{:S(2)}) copy-start(bf16[2,128,512]{2,1,0:T(8,128)(2,1)} %keys_ref.1) | copy-start | bytes 786436
  2.6 44.6 %copy-start.4 = (f32[4,512]{1,0:T(4,128)S(1)}, f32[4,512]{1,0:T(4,128)}, u32[]{:S(2)}) copy-start(f32[4,512]{1,0:T(4,128)} %conv_b_ref.1) | copy-start | bytes 24580
  2.6 44.6 %copy-start.5 = (f32[4,512]{1,0:T(4,128)S(1)}, f32[4,512]{1,0:T(4,128)}, u32[]{:S(2)}) copy-start(f32[4,512]{1,0:T(4,128)} %conv_c_ref.1) | copy-start | bytes 24580
  2.6 44.6 %copy-start.6 = (bf16[2,3,512]{2,0,1:T(2,128)(2,1)S(1)}, bf16[2,3,512]{2,0,1:T(2,128)(2,1)}, u32[]{:S(2)}) copy-start(bf16[2,3,512]{2,0,1:T(2,128)(2,1)} %param.36) | copy-start | bytes 18436
  2.6 44.6 %copy-start.7 = (bf16[2,3,512]{2,0,1:T(2,128)(2,1)S(1)}, bf16[2,3,512]{2,0,1:T(2,128)(2,1)}, u32[]{:S(2)}) copy-start(bf16[2,3,512]{2,0,1:T(2,128)(2,1)} %param.37) | copy-start | bytes 18436
  2.7 56.5 %all-to-all-start = ((bf16[16,2,3200]{2,1,0:T(2,128)(2,1)}), bf16[16,2,3200]{2,1,0:T(2,128)(2,1)S(1)}, u32[]{:S(2)}, u32[]{:S(2)}) async-start(bf16[16,2,3200]{2,1,0:T(2,128)(2,1)} %shard_map.235), calls=%async_computation | async-start | bytes 409600 | tf_op jit(solution)/shard_map/all_to_all | solution.py:272
  47.0 0.7 copy-start.2
  47.1 0.7 copy-start.3
  47.2 0.7 copy-start.8
  59.2 12.1 %copy-start.9 = (bf16[1024,256]{1,0:T(8,128)(2,1)S(1)}, bf16[1024,256]{1,0:T(8,128)(2,1)}, u32[]{:S(2)}) copy-start(bf16[1024,256]{1,0:T(8,128)(2,1)} %param.46) | copy-start | bytes 1572868
  60.7 26.9 %all-to-all-start.1 = ((bf16[32,2,1152]{2,1,0:T(2,128)(2,1)}), bf16[32,2,1152]{2,1,0:T(2,128)(2,1)S(1)}, u32[]{:S(2)}, u32[]{:S(2)}) async-start(bf16[32,2,1152]{2,1,0:T(2,128)(2,1)} %shard_map.237), calls=%async_computation.1 | async-start | bytes 294912 | tf_op jit(solution)/shard_map/all_to_all | solution.py:281
  71.3 2.8 %copy-start.10 = (bf16[128,2048]{1,0:T(8,128)(2,1)S(1)}, bf16[128,2048]{1,0:T(8,128)(2,1)}, u32[]{:S(2)}) copy-start(bf16[128,2048]{1,0:T(8,128)(2,1)} %param.48) | copy-start | bytes 1572868
  71.4 8.1 %collective-permute-start = (bf16[1024,128]{1,0:T(8,128)(2,1)S(1)}, bf16[1024,128]{1,0:T(8,128)(2,1)S(1)}, u32[]{:S(2)}, u32[]{:S(2)}) collective-permute-start(bf16[1024,128]{1,0:T(8,128)(2,1)S(1)} %get-tuple-element.37), channel_id=1, source_target_pairs={{0,1},{1,0},{2,3},{3,2},{4,5},{5,4},{6,7},{7,6},{8,9},{9,8},{10,11... | collective-permute-start | bytes 786440 | tf_op jit(solution)/shard_map/ppermute | solution.py:34
  74.2 4.5 %copy-start.12 = (bf16[32,256]{1,0:T(8,128)(2,1)S(1)}, bf16[32,256]{1,0:T(8,128)(2,1)}, u32[]{:S(2)}) copy-start(bf16[32,256]{1,0:T(8,128)(2,1)} %x_ref.1) | copy-start | bytes 49156
  74.2 2.0 %copy-start.15 = (f32[128]{0:T(128)S(1)}, f32[128]{0:T(128)}, u32[]{:S(2)}) copy-start(f32[128]{0:T(128)} %param.47) | copy-start | bytes 1540
  74.2 5.2 %collective-permute-start.1 = (bf16[128,1024]{1,0:T(8,128)(2,1)S(1)}, bf16[128,1024]{1,0:T(8,128)(2,1)S(1)}, u32[]{:S(2)}, u32[]{:S(2)}) collective-permute-start(bf16[128,1024]{1,0:T(8,128)(2,1)S(1)} %get-tuple-element.35), channel_id=1, source_target_pairs={{0,1},{1,0},{2,3},{3,2},{4,5},{5,4},{6,7},{7,6},{8,9},{9,8},{10,11... | collective-permute-start | bytes 786440 | tf_op jit(solution)/shard_map/ppermute | solution.py:34
  76.2 3.2 %collective-permute-start.2 = (f32[128]{0:T(128)S(1)}, f32[128]{0:T(128)S(1)}, u32[]{:S(2)}, u32[]{:S(2)}) collective-permute-start(f32[128]{0:T(128)S(1)} %copy-done.15), channel_id=1, source_target_pairs={{0,1},{1,0},{2,3},{3,2},{4,5},{5,4},{6,7},{7,6},{8,9},{9,8},{10,11... | collective-permute-start | bytes 1544 | tf_op jit(solution)/shard_map/ppermute | solution.py:34
  107.6 4.2 %copy-start.11 = (bf16[2048,128]{1,0:T(8,128)(2,1)S(1)}, bf16[2048,128]{1,0:T(8,128)(2,1)}, u32[]{:S(2)}) copy-start(bf16[2048,128]{1,0:T(8,128)(2,1)} %param.49) | copy-start | bytes 1572868
  107.6 29.5 %all-to-all-start.3 = ((bf16[16,64,256]{2,1,0:T(8,128)(2,1)}), bf16[16,64,256]{2,1,0:T(8,128)(2,1)S(1)}, u32[]{:S(2)}, u32[]{:S(2)}) async-start(bf16[16,64,256]{2,1,0:T(8,128)(2,1)} %bitcast.19), calls=%async_computation.3 | async-start | bytes 1048576 | tf_op jit(solution)/shard_map/all_to_all | solution.py:324
  111.8 3.5 %collective-permute-start.3 = (bf16[1024,128]{1,0:T(8,128)(2,1)S(1)}, bf16[1024,128]{1,0:T(8,128)(2,1)S(1)}, u32[]{:S(2)}, u32[]{:S(2)}) collective-permute-start(bf16[1024,128]{1,0:T(8,128)(2,1)S(1)} %get-tuple-element.34), channel_id=1, source_target_pairs={{0,1},{1,0},{2,3},{3,2},{4,5},{5,4},{6,7},{7,6},{8,9},{9,8},{10,11... | collective-permute-start | bytes 786440 | tf_op jit(solution)/shard_map/ppermute | solution.py:34
  167.0 21.8 %all-to-all-start.4 = ((bf16[16,32,128]{2,1,0:T(8,128)(2,1)}), bf16[16,32,128]{2,1,0:T(8,128)(2,1)S(1)}, u32[]{:S(2)}, u32[]{:S(2)}) async-start(bf16[16,32,128]{2,1,0:T(8,128)(2,1)} %bitcast.25), calls=%async_computation.4 | async-start | bytes 262144 | tf_op jit(solution)/shard_map/all_to_all | solution.py:341

commit v6 on v5

--- a/solution.py
+++ b/solution.py
@@ -3,6 +3,7 @@
 from jax import lax
 from jax.experimental import pallas as pl
 from jax.experimental.pallas import tpu as pltpu
+from jax.sharding import Mesh
 from jax.sharding import PartitionSpec as P
 
 D = 4096
@@ -11,6 +12,8 @@
 SSM_WIDTH = 2048
 LANES = 128
 SPARE = 8
+KV = ("kh", "kl")
+TEAM = ("kl", "tp")
 
 EPS = 1e-06
 BF16 = jnp.bfloat16
@@ -29,21 +32,17 @@
     )
 
 
-def from_partner(x):
-    size = lax.axis_size("tp")
-    return lax.ppermute(x, "tp", [(i, (i + 1) % size) for i in range(size)])
-
-
-def exchanged(weight, dim, core):
-    half = weight.shape[dim] // 2
-    mine = lax.dynamic_slice_in_dim(weight, core * half, half, dim)
-    other = lax.dynamic_slice_in_dim(weight, (1 - core) * half, half, dim)
-    return mine, from_partner(other)
-
-
-def in_core_order(mine, other, core, dim):
+def swapped(array, dim, here, axis):
+    half = array.shape[dim] // 2
+    size = lax.axis_size(axis)
+    mine = lax.dynamic_slice_in_dim(array, here * half, half, dim)
+    other = lax.dynamic_slice_in_dim(array, (1 - here) * half, half, dim)
+    return mine, lax.ppermute(other, axis, [(i, (i + 1) % size) for i in range(size)])
+
+
+def in_order(mine, other, here, dim):
     return jnp.where(
-        core == 0,
+        here == 0,
         jnp.concatenate([mine, other], axis=dim),
         jnp.concatenate([other, mine], axis=dim),
     )
@@ -266,30 +265,35 @@
     w_down,
 ):
     core = lax.axis_index("tp")
-    n_kv, n_dp, n_tp = lax.axis_size("kv"), lax.axis_size("dp"), lax.axis_size("tp")
+    side = lax.axis_index("kl")
+    n_kv, n_dp, n_tp = lax.axis_size(KV), lax.axis_size("dp"), lax.axis_size("tp")
+    n_far, n_team = lax.axis_size("kh"), lax.axis_size(TEAM)
     rows = inputs.shape[0]
     sent = project(inputs, gain_in, (w_gate, w_input, w_bproj, w_cproj), w_step, n_kv)
-    arrived = lax.all_to_all(sent, "kv", 0, 0, tiled=True)
+    arrived = lax.all_to_all(sent, KV, 0, 0, tiled=True)
     convs = [on_chip(x) for x in (conv_input, conv_bproj, conv_cproj)]
     tails = [on_chip(jnp.swapaxes(x, 0, 1)) for x in (tail_input, tail_bproj, tail_cproj)]
     columns = [on_chip(x[:, None]) for x in (step_bias, decay_log)]
     values, keys, gain = [on_chip(x) for x in (block_input, block_bproj, gain_mix[None])]
     others = (*convs, *tails, columns[0], values, keys, gain)
     prepared = prepare(block_step, lengths, columns[1], state, others)
+    scaled_up = (w_up.astype(F32) * gain_mlp[:, None]).astype(BF16)
+    up_mine, up_other = swapped(scaled_up, 1, core, "tp")
+    up_half = in_order(up_mine, up_other, core, 0)
+    arrived, up_half = lax.optimization_barrier((arrived, up_half))
     whole = mix(arrived, convs, tails, columns, prepared, values, keys, gain, n_kv * n_tp)
     width = gain_mix.shape[0]
-    whole = lax.all_to_all(whole, ("kv", "tp"), 0, 0, tiled=True)
-
-    out_mine, out_other = exchanged(w_out, 1, core)
-    up_mine, up_other = exchanged(w_up, 1, core)
-    up_gain = jnp.concatenate([gain_mlp, from_partner(gain_mlp)])
+    whole = lax.all_to_all(whole, (*KV, "tp"), 0, 0, tiled=True)
+
+    out_mine, out_other = swapped(w_out, 1, core, "tp")
+    up_mine, up_other = swapped(up_half, 1, side, "kl")
+    up_weight = in_order(up_mine, up_other, side, 0)
     column_count = out_mine.shape[1]
     residual = lax.dynamic_slice_in_dim(inputs, core * column_count, column_count, 1)
-    whole, out_mine, out_other, up_mine, up_other, up_gain, residual = lax.optimization_barrier(
-        (whole, out_mine, out_other, up_mine, up_other, up_gain, residual)
+    whole, out_mine, out_other, up_weight, residual = lax.optimization_barrier(
+        (whole, out_mine, out_other, up_weight, residual)
     )
     out_weight = jnp.concatenate([out_mine, out_other], axis=0)
-    up_weight = jnp.concatenate([up_mine, up_other], axis=0)
 
     whole = whole.reshape(n_kv, n_tp, rows // n_kv, -1)
     whole = jnp.moveaxis(whole, 1, 0).reshape(n_tp, rows, -1)
@@ -306,25 +310,18 @@
     mixed_in = mixed_in * lax.rsqrt(total_sq / SSM_WIDTH + EPS)[:, None]
     hidden = (residual.astype(F32) + mixed_in).astype(BF16)
 
-    all_hidden = to_everyone(hidden, ("dp", "tp")).reshape(n_dp, n_tp, rows, -1)
+    all_hidden = to_everyone(hidden, ("dp", *TEAM)).reshape(n_dp, n_team, rows, -1)
     seqs = n_dp * rows
-    all_hidden = jnp.moveaxis(all_hidden, 1, 0).reshape(n_tp, seqs, -1)
-    all_hidden = jnp.concatenate(
-        [
-            lax.dynamic_index_in_dim(all_hidden, core, 0, keepdims=False),
-            lax.dynamic_index_in_dim(all_hidden, 1 - core, 0, keepdims=False),
-        ],
-        axis=1,
-    ).astype(F32)
-    row_sq = jnp.sum(all_hidden * all_hidden, axis=1)
-    lifted = (all_hidden * up_gain).astype(BF16)
+    all_hidden = jnp.moveaxis(all_hidden, 1, 2).reshape(seqs, -1)
     raised = lax.dot_general(
-        up_weight, lifted, (((0,), (1,)), ((), ())), preferred_element_type=F32
+        up_weight, all_hidden, (((0,), (1,)), ((), ())), preferred_element_type=F32
     ).astype(BF16)
-    arrived = lax.all_to_all(raised.reshape(n_kv, -1, seqs), "kv", 0, 0, tiled=True)
-    down_mine, down_other = exchanged(w_down, 0, core)
-    down_weight = in_core_order(down_mine, down_other, core, 1)
-    down_weight = jnp.pad(down_weight.reshape(n_kv, -1, down_weight.shape[1]), ((0, 0), (0, SPARE), (0, 0)))
+    row_sq = jnp.sum(jnp.square(all_hidden.astype(F32)), axis=1)
+    arrived = lax.all_to_all(raised.reshape(n_far, -1, seqs), "kh", 0, 0, tiled=True)
+    down_half = in_order(*swapped(w_down, 0, core, "tp"), core, 1)
+    down_weight = in_order(*swapped(down_half, 0, side, "kl"), side, 1)
+    down_weight = down_weight.reshape(n_far, -1, down_weight.shape[1])
+    down_weight = jnp.pad(down_weight, ((0, 0), (0, SPARE), (0, 0)))
     down_weight = down_weight.reshape(-1, down_weight.shape[2])
     words = jnp.concatenate(
         [*[w[None] for w in two_words(row_sq)], jnp.zeros((SPARE - 2, seqs), BF16)], axis=0
@@ -332,52 +329,56 @@
     arrived, down_weight, words = lax.optimization_barrier((arrived, down_weight, words))
     shares = jnp.sum(arrived.astype(F32), axis=0)
     units = jnp.square(jax.nn.relu(shares)).astype(BF16)
-    hidden_units = lax.all_gather(jnp.concatenate([units, words], axis=0), "kv", axis=0, tiled=True)
+    hidden_units = to_everyone(jnp.concatenate([units, words], axis=0), "kh")
+    hidden_units = hidden_units.reshape(-1, seqs)
     lowered = lax.dot_general(
         hidden_units, down_weight, (((0,), (0,)), ((), ())), preferred_element_type=F32
     ).astype(BF16)
-    lowered = lowered.reshape(n_dp, rows, n_tp, -1)
-    lowered = jnp.moveaxis(lowered, 2, 1).reshape(n_dp * n_tp, rows, -1)
-    lowered = lax.all_to_all(lowered, ("dp", "tp"), 0, 0, tiled=True)
+    lowered = lowered.reshape(n_dp, rows, n_team, -1)
+    lowered = jnp.moveaxis(lowered, 2, 1).reshape(n_dp * n_team, rows, -1)
+    lowered = lax.all_to_all(lowered, ("dp", *TEAM), 0, 0, tiled=True)
     lowered = jnp.sum(lowered.astype(F32), axis=0)
     unit_count = units.shape[0]
-    sq_words = hidden_units.reshape(n_kv, -1, seqs)[:, unit_count : unit_count + 2]
+    sq_words = hidden_units.reshape(n_far, -1, seqs)[:, unit_count : unit_count + 2]
     sq_sum = jnp.sum(sq_words.astype(F32), axis=(0, 1))
     sq_sum = lax.dynamic_slice_in_dim(sq_sum, lax.axis_index("dp") * rows, rows, 0)
     return (hidden.astype(F32) + lowered / (sq_sum / D + EPS)[:, None]).astype(BF16)
 
 
 def solution(mesh):
+    sizes = [mesh.shape[name] for name in ("grp", "dp", "kv", "tp")]
+    pairs = mesh.devices.reshape(sizes[0], sizes[1], sizes[2] // 2, 2, sizes[3])
+    mesh = Mesh(pairs, ("grp", "dp", "kh", "kl", "tp"))
     return jax.shard_map(
         layer,
         mesh=mesh,
         in_specs=(
-            P(("grp", "dp"), "kv"),
-            P("kv"),
-            P("kv", "tp"),
-            P("kv", "tp"),
-            P("kv", "tp"),
-            P("kv", "tp"),
-            P("kv", "tp"),
+            P(("grp", "dp"), KV),
+            P(KV),
+            P(KV, "tp"),
+            P(KV, "tp"),
+            P(KV, "tp"),
+            P(KV, "tp"),
+            P(KV, "tp"),
             P(None, "tp"),
             P(None, "tp"),
             P(None, "tp"),
-            P(("grp", "dp", "kv"), None, "tp"),
-            P(("grp", "dp", "kv"), None, "tp"),
-            P(("grp", "dp", "kv"), None, "tp"),
+            P(("grp", "dp", *KV), None, "tp"),
+            P(("grp", "dp", *KV), None, "tp"),
+            P(("grp", "dp", *KV), None, "tp"),
             P("tp"),
             P("tp"),
-            P(("grp", "dp", "kv"), None, "tp"),
-            P(("grp", "dp", "kv"), None, "tp"),
-            P(("grp", "dp", "kv"), None, "tp"),
-            P(("grp", "dp", "kv")),
-            P(("grp", "dp", "kv"), "tp", None, None),
+            P(("grp", "dp", *KV), None, "tp"),
+            P(("grp", "dp", *KV), None, "tp"),
+            P(("grp", "dp", *KV), None, "tp"),
+            P(("grp", "dp", *KV)),
+            P(("grp", "dp", *KV), "tp", None, None),
             P("tp"),
-            P("tp", "kv"),
-            P(("kv", "tp")),
-            P(("kv", "tp"), "dp"),
-            P("dp", ("kv", "tp")),
+            P("tp", KV),
+            P((*KV, "tp")),
+            P((*KV, "tp"), "dp"),
+            P("dp", (*KV, "tp")),
         ),
-        out_specs=P(("grp", "dp"), ("kv", "tp")),
+        out_specs=P(("grp", "dp"), (*KV, "tp")),
         check_vma=False,
     )

time: 190 us -> 184 us (0.968)
  blocking collectives: 46.3 us -> 23 us
  starting transfers between devices: 80.7 us -> 99.1 us
  waiting for transfers between devices: 50.5 us -> 47.2 us
    all_gather x1 -> x0, blocking collectives: 28.8 us -> none  [layer(): lax.all_gather(jnp.concatenate([units, words], axis=0), 'kv', axis=0, til...]
    all_to_all x4 -> x5, starting transfers between devices: 71.6 us -> 84.1 us  [the longest x1 44.2 us: layer(): arrived = lax.all_to_all(sent, KV, 0, 0, tiled=True)]
    all_to_all x4 -> x5, waiting for transfers between devices: 48.3 us -> 38.3 us  [the longest x1 16.3 us: layer(): lax.all_to_all(raised.reshape(n_far, -1, seqs), 'kh', 0, 0, tiled=True)]
    ppermute x4 -> x5, waiting for transfers between devices: 2.18 us -> 8.86 us  [swapped(): lax.ppermute(other, axis, [(i, (i + 1) % size) for i in range(size)])]
    ppermute x4 -> x5, starting transfers between devices: 9.11 us -> 14.9 us  [swapped(): lax.ppermute(other, axis, [(i, (i + 1) % size) for i in range(size)])]
    all_to_all x1, blocking collectives: 17.6 us -> 23 us  [to_everyone(): lax.all_to_all(jnp.broadcast_to(shard[None], (size, *shard.shape)), axes,...]
  transfers between devices with their start and end apart: 8 -> 10, of which waited for: 6 -> 7; matrix products, arithmetic and copies ran while one was open for 1% -> 2% of each run, Pallas kernels for 1% -> 1%
where the time goes in v6:
time: 184 us; the launch traced here: 183 us
  starting transfers between devices  99.1 us (54%)
  waiting for transfers between devices  47.2 us (26%)
  blocking collectives  23 us (12%)
  Pallas kernels  5.72 us (3%)
  local copies, waits for them, and re-layouts  4.16 us (2%)
  other arithmetic  2.23 us (1%)
    all_to_all x1, starting transfers between devices, layer(): arrived = lax.all_to_all(sent, KV, 0, 0, tiled=True)  44.2 us
    all_to_all x1, blocking collectives, to_everyone(): lax.all_to_all(jnp.broadcast_to(shard[None], (size, *shard.shape)), axes,...  23 us
    all_to_all x1, waiting for transfers between devices, layer(): lax.all_to_all(raised.reshape(n_far, -1, seqs), 'kh', 0, 0, tiled=True)  16.3 us
    ppermute x5, starting transfers between devices, swapped(): lax.ppermute(other, axis, [(i, (i + 1) % size) for i in range(size)])  14.9 us
    all_to_all x1, starting transfers between devices, layer(): lowered = lax.all_to_all(lowered, ('dp', *TEAM), 0, 0, tiled=True)  11.8 us
    all_to_all x1, waiting for transfers between devices, layer(): lowered = lax.all_to_all(lowered, ('dp', *TEAM), 0, 0, tiled=True)  10.8 us
    all_to_all x1, starting transfers between devices, layer(): whole = lax.all_to_all(whole, (*KV, 'tp'), 0, 0, tiled=True)  10.6 us
    all_to_all x1, starting transfers between devices, to_everyone(): lax.all_to_all(jnp.broadcast_to(shard[None], (size, *shard.shape)), axes,...  9.49 us
  transfers between devices with their start and end apart: 10, of which 7 were waited for; matrix products, arithmetic and copies ran while one was open for 2% of the time, Pallas kernels for 1%

profile of v6, /device:TPU:65, one launch (start us, length us, event | category | flops | bytes accessed | tf_op | source)
XLA Modules:
  0.0 183.4 jit_solution(5353995268595781140)
XLA Ops:
  0.0 2.6 %shard_map.235 = bf16[16,2,3200]{2,1,0:T(2,128)(2,1)} custom-call(bf16[32,256]{1,0:T(8,128)(2,1)} %x_ref.1, f32[1,256]{1,0:T(1,128)} %bitcast.58, bf16[256,1024]{1,0:T(8,128)(2,1)} %gate_ref.1, bf16[256,1024]{1,0:T(8,128)(2,1)} %input_ref.1, bf16[256,512]{1,0:T(8,128)(2,1)} %b_ref.1, bf16[256,512]{1,0:T(8,128)(2,1)} %c_ref.1, bf16[16,256]{1,0:T(8,128)(2,1)} %bitcast.57), custom_call_target="tpu_custom_call" | custom-call | tf_op jit(solution)/shard_map/pallas_call | solution.py:87
  2.6 44.2 %all-to-all-start = ((bf16[16,2,3200]{2,1,0:T(2,128)(2,1)}), bf16[16,2,3200]{2,1,0:T(2,128)(2,1)S(1)}, u32[]{:S(2)}, u32[]{:S(2)}) async-start(bf16[16,2,3200]{2,1,0:T(2,128)(2,1)} %shard_map.235), calls=%async_computation | async-start | bytes 409600 | tf_op jit(solution)/shard_map/all_to_all | solution.py:273
  46.9 0.6 copy-done.13
  47.5 0.2 multiply_convert_fusion
  47.8 3.2 %collective-permute-start = (bf16[128,1024]{1,0:T(8,128)(2,1)S(1)}, bf16[128,1024]{1,0:T(8,128)(2,1)S(1)}, u32[]{:S(2)}, u32[]{:S(2)}) collective-permute-start(bf16[128,1024]{1,0:T(8,128)(2,1)S(1)} %get-tuple-element.42), channel_id=1, source_target_pairs={{0,1},{1,0},{2,3},{3,2},{4,5},{5,4},{6,7},{7,6},{8,9},{9,8},{10,11... | collective-permute-start | bytes 786440 | tf_op jit(solution)/shard_map/ppermute | solution.py:40
  51.1 0.1 copy.68.refs_6_.bias_ref
  51.2 0.1 copy.69.log_ref
  51.3 0.4 copy-done.6
  51.8 0.1 copy-done.3
  51.9 1.6 shard_map.236
  53.5 0.1 maximum_select_fusion
  53.6 5.4 %all-to-all-done.arrived_ref = bf16[16,2,3200]{2,1,0:T(2,128)(2,1)S(1)} async-done(((bf16[16,2,3200]{2,1,0:T(2,128)(2,1)}), bf16[16,2,3200]{2,1,0:T(2,128)(2,1)S(1)}, u32[]{:S(2)}, u32[]{:S(2)}) %all-to-all-start) | async-done | bytes 204832 | tf_op jit(solution)/shard_map/all_to_all | solution.py:273
  59.0 1.5 shard_map.237
  60.5 10.6 %all-to-all-start.1 = ((bf16[32,2,1152]{2,1,0:T(2,128)(2,1)}), bf16[32,2,1152]{2,1,0:T(2,128)(2,1)S(1)}, u32[]{:S(2)}, u32[]{:S(2)}) async-start(bf16[32,2,1152]{2,1,0:T(2,128)(2,1)} %shard_map.237), calls=%async_computation.1 | async-start | bytes 294912 | tf_op jit(solution)/shard_map/all_to_all | solution.py:286
  71.2 3.4 %collective-permute-start.2 = (bf16[256,512]{1,0:T(8,128)(2,1)S(1)}, bf16[256,512]{1,0:T(8,128)(2,1)S(1)}, u32[]{:S(2)}, u32[]{:S(2)}) collective-permute-start(bf16[256,512]{1,0:T(8,128)(2,1)S(1)} %get-tuple-element.38), channel_id=1, source_target_pairs={{0,2},{2,0},{1,3},{3,1},{4,6},{6,4},{5,7},{7,5},{8,10},{10,8},{9,1... | collective-permute-start | bytes 786440 | tf_op jit(solution)/shard_map/ppermute | solution.py:40
  74.7 2.6 %collective-permute-start.1 = (bf16[1024,128]{1,0:T(8,128)(2,1)S(1)}, bf16[1024,128]{1,0:T(8,128)(2,1)S(1)}, u32[]{:S(2)}, u32[]{:S(2)}) collective-permute-start(bf16[1024,128]{1,0:T(8,128)(2,1)S(1)} %get-tuple-element.39), channel_id=1, source_target_pairs={{0,1},{1,0},{2,3},{3,2},{4,5},{5,4},{6,7},{7,6},{8,9},{9,8},{10,11... | collective-permute-start | bytes 786440 | tf_op jit(solution)/shard_map/ppermute | solution.py:40
  77.3 7.7 %collective-permute-done.2 = bf16[256,512]{1,0:T(8,128)(2,1)S(1)} collective-permute-done((bf16[256,512]{1,0:T(8,128)(2,1)S(1)}, bf16[256,512]{1,0:T(8,128)(2,1)S(1)}, u32[]{:S(2)}, u32[]{:S(2)}) %collective-permute-start.2) | collective-permute-done | bytes 262176 | tf_op jit(solution)/shard_map/ppermute | solution.py:40
  85.0 0.2 maximum_select_fusion.1
  85.3 2.2 %all-to-all-done.1 = bf16[32,2,1152]{2,1,0:T(2,128)(2,1)S(1)} async-done(((bf16[32,2,1152]{2,1,0:T(2,128)(2,1)}), bf16[32,2,1152]{2,1,0:T(2,128)(2,1)S(1)}, u32[]{:S(2)}, u32[]{:S(2)}) %all-to-all-start.1) | async-done | bytes 147488 | tf_op jit(solution)/shard_map/all_to_all | solution.py:286
  87.4 0.1 copy.70
  87.5 0.3 convert_reduce_fusion.2
  87.9 0.1 slice.12
  88.0 0.3 constant_dynamic-slice_fusion.5
  88.3 0.2 add_convert_fusion.1
  88.5 0.7 broadcast_in_dim.36
  89.3 9.5 %all-to-all-start.2 = ((bf16[32,32,128]{2,1,0:T(8,128)(2,1)}), bf16[32,32,128]{2,1,0:T(8,128)(2,1)S(1)}, u32[]{:S(2)}, u32[]{:S(2)}) async-start(bf16[32,32,128]{2,1,0:T(8,128)(2,1)} %broadcast_in_dim.36), calls=%async_computation.2 | async-start | bytes 524288 | tf_op jit(solution)/shard_map/all_to_all | solution.py:30
  98.8 2.6 %collective-permute-start.3 = (bf16[1024,128]{1,0:T(8,128)(2,1)S(1)}, bf16[1024,128]{1,0:T(8,128)(2,1)S(1)}, u32[]{:S(2)}, u32[]{:S(2)}) collective-permute-start(bf16[1024,128]{1,0:T(8,128)(2,1)S(1)} %get-tuple-element.36), channel_id=1, source_target_pairs={{0,1},{1,0},{2,3},{3,2},{4,5},{5,4},{6,7},{7,6},{8,9},{9,8},{10,11... | collective-permute-start | bytes 786440 | tf_op jit(solution)/shard_map/ppermute | solution.py:40
  101.5 1.1 collective-permute-done.3
  102.6 0.2 maximum_select_fusion.2
  102.9 3.0 %collective-permute-start.4 = (bf16[512,256]{1,0:T(8,128)(2,1)S(1)}, bf16[512,256]{1,0:T(8,128)(2,1)S(1)}, u32[]{:S(2)}, u32[]{:S(2)}) collective-permute-start(bf16[512,256]{1,0:T(8,128)(2,1)S(1)} %get-tuple-element.34), channel_id=1, source_target_pairs={{0,2},{2,0},{1,3},{3,1},{4,6},{6,4},{5,7},{7,5},{8,10},{10,8},{9,1... | collective-permute-start | bytes 786440 | tf_op jit(solution)/shard_map/ppermute | solution.py:40
  105.9 3.7 %all-to-all-done.2 = bf16[32,32,128]{2,1,0:T(8,128)(2,1)S(1)} async-done(((bf16[32,32,128]{2,1,0:T(8,128)(2,1)}), bf16[32,32,128]{2,1,0:T(8,128)(2,1)S(1)}, u32[]{:S(2)}, u32[]{:S(2)}) %all-to-all-start.2) | async-done | bytes 262176 | tf_op jit(solution)/shard_map/all_to_all | solution.py:30
  109.6 0.1 copy.71
  109.7 1.1 convolution_convert_fusion
  110.8 8.1 %all-to-all-start.3 = ((bf16[8,64,256]{2,1,0:T(8,128)(2,1)}), bf16[8,64,256]{2,1,0:T(8,128)(2,1)S(1)}, u32[]{:S(2)}, u32[]{:S(2)}) async-start(bf16[8,64,256]{2,1,0:T(8,128)(2,1)} %bitcast.16), calls=%async_computation.3 | async-start | bytes 524288 | tf_op jit(solution)/shard_map/all_to_all | solution.py:320
  118.9 0.1 pad.9.clone
  119.0 0.1 maximum_select_fusion.3
  119.2 0.1 multiply_reduce_fusion
  119.3 0.1 reduce_sum.49
  119.4 0.1 maximum_maximum_fusion
  119.4 16.3 %all-to-all-done.3 = bf16[8,64,256]{2,1,0:T(8,128)(2,1)S(1)} async-done(((bf16[8,64,256]{2,1,0:T(8,128)(2,1)}), bf16[8,64,256]{2,1,0:T(8,128)(2,1)S(1)}, u32[]{:S(2)}, u32[]{:S(2)}) %all-to-all-start.3) | async-done | bytes 262176 | tf_op jit(solution)/shard_map/all_to_all | solution.py:320
  135.9 23.0 %all_to_all.30 = bf16[8,72,256]{2,1,0:T(8,128)(2,1)S(1)} all-to-all(bf16[8,72,256]{2,1,0:T(8,128)(2,1)S(1)} %broadcast_in_dim.38), channel_id=1, replica_groups=mesh['grp'=2,'dp'=8,'kh'=8,'kl'=2,'tp'=2] {'kh'}, dimensions={0} | all-to-all | bytes 589824 | tf_op jit(solution)/shard_map/all_to_all | solution.py:30
  158.8 0.4 convolution_convert_fusion.1
  159.2 0.1 reshape.84
  159.3 0.8 copy.72
  160.1 11.8 %all-to-all-start.5 = ((bf16[32,32,128]{2,1,0:T(8,128)(2,1)}), bf16[32,32,128]{2,1,0:T(8,128)(2,1)S(1)}, u32[]{:S(2)}, u32[]{:S(2)}) async-start(bf16[32,32,128]{2,1,0:T(8,128)(2,1)} %bitcast.23), calls=%async_computation.5 | async-start | bytes 524288 | tf_op jit(solution)/shard_map/all_to_all | solution.py:339
  171.9 0.1 multiply_add_fusion
  172.0 10.8 %all-to-all-done.5 = bf16[32,32,128]{2,1,0:T(8,128)(2,1)S(1)} async-done(((bf16[32,32,128]{2,1,0:T(8,128)(2,1)}), bf16[32,32,128]{2,1,0:T(8,128)(2,1)S(1)}, u32[]{:S(2)}, u32[]{:S(2)}) %all-to-all-start.5) | async-done | bytes 262176 | tf_op jit(solution)/shard_map/all_to_all | solution.py:339
  182.8 0.7 add_convert_fusion
  (50 shorter events, 0.6 us)
Async XLA Ops:
  0.0 46.8 %copy-start.11 = (bf16[128,2048]{1,0:T(8,128)(2,1)S(1)}, bf16[128,2048]{1,0:T(8,128)(2,1)}, u32[]{:S(2)}) copy-start(bf16[128,2048]{1,0:T(8,128)(2,1)} %param.48) | copy-start | bytes 1572868
  2.6 56.4 %all-to-all-start = ((bf16[16,2,3200]{2,1,0:T(2,128)(2,1)}), bf16[16,2,3200]{2,1,0:T(2,128)(2,1)S(1)}, u32[]{:S(2)}, u32[]{:S(2)}) async-start(bf16[16,2,3200]{2,1,0:T(2,128)(2,1)} %shard_map.235), calls=%async_computation | async-start | bytes 409600 | tf_op jit(solution)/shard_map/all_to_all | solution.py:273
  46.8 0.7 copy-start.13
  47.6 3.4 %copy-start.14 = (f32[16]{0:T(128)S(1)}, f32[16]{0:T(128)}, u32[]{:S(2)}) copy-start(f32[16]{0:T(128)} %param.38) | copy-start | bytes 196
  47.7 3.5 %copy-start.15 = (f32[16]{0:T(128)S(1)}, f32[16]{0:T(128)}, u32[]{:S(2)}) copy-start(f32[16]{0:T(128)} %param.39) | copy-start | bytes 196
  47.7 3.6 %copy-start = (bf16[2,128,1024]{2,1,0:T(8,128)(2,1)S(1)}, bf16[2,128,1024]{2,1,0:T(8,128)(2,1)}, u32[]{:S(2)}) copy-start(bf16[2,128,1024]{2,1,0:T(8,128)(2,1)} %values_ref.1) | copy-start | bytes 1572868
  47.7 3.6 %copy-start.1 = (bf16[2,128,512]{2,1,0:T(8,128)(2,1)S(1)}, bf16[2,128,512]{2,1,0:T(8,128)(2,1)}, u32[]{:S(2)}) copy-start(bf16[2,128,512]{2,1,0:T(8,128)(2,1)} %keys_ref.1) | copy-start | bytes 786436
  47.7 3.6 %copy-start.4 = (f32[4,512]{1,0:T(4,128)S(1)}, f32[4,512]{1,0:T(4,128)}, u32[]{:S(2)}) copy-start(f32[4,512]{1,0:T(4,128)} %conv_b_ref.1) | copy-start | bytes 24580
  47.7 3.6 %copy-start.5 = (f32[4,512]{1,0:T(4,128)S(1)}, f32[4,512]{1,0:T(4,128)}, u32[]{:S(2)}) copy-start(f32[4,512]{1,0:T(4,128)} %conv_c_ref.1) | copy-start | bytes 24580
  47.7 3.6 %copy-start.7 = (bf16[2,3,512]{2,0,1:T(2,128)(2,1)S(1)}, bf16[2,3,512]{2,0,1:T(2,128)(2,1)}, u32[]{:S(2)}) copy-start(bf16[2,3,512]{2,0,1:T(2,128)(2,1)} %param.37) | copy-start | bytes 18436
  47.7 3.6 %copy-start.8 = (f32[1024]{0:T(1024)S(1)}, f32[1024]{0:T(1024)}, u32[]{:S(2)}) copy-start(f32[1024]{0:T(1024)} %param.45) | copy-start | bytes 12292
  47.8 5.7 %collective-permute-start = (bf16[128,1024]{1,0:T(8,128)(2,1)S(1)}, bf16[128,1024]{1,0:T(8,128)(2,1)S(1)}, u32[]{:S(2)}, u32[]{:S(2)}) collective-permute-start(bf16[128,1024]{1,0:T(8,128)(2,1)S(1)} %get-tuple-element.42), channel_id=1, source_target_pairs={{0,1},{1,0},{2,3},{3,2},{4,5},{5,4},{6,7},{7,6},{8,9},{9,8},{10,11... | collective-permute-start | bytes 786440 | tf_op jit(solution)/shard_map/ppermute | solution.py:40
  51.1 0.7 copy-start.6
  51.1 0.7 copy-start.2
  51.2 0.7 copy-start.3
  60.5 26.9 %all-to-all-start.1 = ((bf16[32,2,1152]{2,1,0:T(2,128)(2,1)}), bf16[32,2,1152]{2,1,0:T(2,128)(2,1)S(1)}, u32[]{:S(2)}, u32[]{:S(2)}) async-start(bf16[32,2,1152]{2,1,0:T(2,128)(2,1)} %shard_map.237), calls=%async_computation.1 | async-start | bytes 294912 | tf_op jit(solution)/shard_map/all_to_all | solution.py:286
  71.1 3.5 %copy-start.9 = (bf16[1024,256]{1,0:T(8,128)(2,1)S(1)}, bf16[1024,256]{1,0:T(8,128)(2,1)}, u32[]{:S(2)}) copy-start(bf16[1024,256]{1,0:T(8,128)(2,1)} %param.46) | copy-start | bytes 1572868
  71.2 13.9 %collective-permute-start.2 = (bf16[256,512]{1,0:T(8,128)(2,1)S(1)}, bf16[256,512]{1,0:T(8,128)(2,1)S(1)}, u32[]{:S(2)}, u32[]{:S(2)}) collective-permute-start(bf16[256,512]{1,0:T(8,128)(2,1)S(1)} %get-tuple-element.38), channel_id=1, source_target_pairs={{0,2},{2,0},{1,3},{3,1},{4,6},{6,4},{5,7},{7,5},{8,10},{10,8},{9,1... | collective-permute-start | bytes 786440 | tf_op jit(solution)/shard_map/ppermute | solution.py:40
  74.6 2.7 %copy-start.12 = (bf16[32,256]{1,0:T(8,128)(2,1)S(1)}, bf16[32,256]{1,0:T(8,128)(2,1)}, u32[]{:S(2)}) copy-start(bf16[32,256]{1,0:T(8,128)(2,1)} %x_ref.1) | copy-start | bytes 49156
  74.7 10.6 %collective-permute-start.1 = (bf16[1024,128]{1,0:T(8,128)(2,1)S(1)}, bf16[1024,128]{1,0:T(8,128)(2,1)S(1)}, u32[]{:S(2)}, u32[]{:S(2)}) collective-permute-start(bf16[1024,128]{1,0:T(8,128)(2,1)S(1)} %get-tuple-element.39), channel_id=1, source_target_pairs={{0,1},{1,0},{2,3},{3,2},{4,5},{5,4},{6,7},{7,6},{8,9},{9,8},{10,11... | collective-permute-start | bytes 786440 | tf_op jit(solution)/shard_map/ppermute | solution.py:40
  88.5 10.2 %copy-start.10 = (bf16[2048,128]{1,0:T(8,128)(2,1)S(1)}, bf16[2048,128]{1,0:T(8,128)(2,1)}, u32[]{:S(2)}) copy-start(bf16[2048,128]{1,0:T(8,128)(2,1)} %param.49) | copy-start | bytes 1572868
  89.3 20.3 %all-to-all-start.2 = ((bf16[32,32,128]{2,1,0:T(8,128)(2,1)}), bf16[32,32,128]{2,1,0:T(8,128)(2,1)S(1)}, u32[]{:S(2)}, u32[]{:S(2)}) async-start(bf16[32,32,128]{2,1,0:T(8,128)(2,1)} %broadcast_in_dim.36), calls=%async_computation.2 | async-start | bytes 524288 | tf_op jit(solution)/shard_map/all_to_all | solution.py:30
  98.8 3.8 %collective-permute-start.3 = (bf16[1024,128]{1,0:T(8,128)(2,1)S(1)}, bf16[1024,128]{1,0:T(8,128)(2,1)S(1)}, u32[]{:S(2)}, u32[]{:S(2)}) collective-permute-start(bf16[1024,128]{1,0:T(8,128)(2,1)S(1)} %get-tuple-element.36), channel_id=1, source_target_pairs={{0,1},{1,0},{2,3},{3,2},{4,5},{5,4},{6,7},{7,6},{8,9},{9,8},{10,11... | collective-permute-start | bytes 786440 | tf_op jit(solution)/shard_map/ppermute | solution.py:40
  102.9 16.1 %collective-permute-start.4 = (bf16[512,256]{1,0:T(8,128)(2,1)S(1)}, bf16[512,256]{1,0:T(8,128)(2,1)S(1)}, u32[]{:S(2)}, u32[]{:S(2)}) collective-permute-start(bf16[512,256]{1,0:T(8,128)(2,1)S(1)} %get-tuple-element.34), channel_id=1, source_target_pairs={{0,2},{2,0},{1,3},{3,1},{4,6},{6,4},{5,7},{7,5},{8,10},{10,8},{9,1... | collective-permute-start | bytes 786440 | tf_op jit(solution)/shard_map/ppermute | solution.py:40
  110.8 25.0 %all-to-all-start.3 = ((bf16[8,64,256]{2,1,0:T(8,128)(2,1)}), bf16[8,64,256]{2,1,0:T(8,128)(2,1)S(1)}, u32[]{:S(2)}, u32[]{:S(2)}) async-start(bf16[8,64,256]{2,1,0:T(8,128)(2,1)} %bitcast.16), calls=%async_computation.3 | async-start | bytes 524288 | tf_op jit(solution)/shard_map/all_to_all | solution.py:320
  160.1 22.7 %all-to-all-start.5 = ((bf16[32,32,128]{2,1,0:T(8,128)(2,1)}), bf16[32,32,128]{2,1,0:T(8,128)(2,1)S(1)}, u32[]{:S(2)}, u32[]{:S(2)}) async-start(bf16[32,32,128]{2,1,0:T(8,128)(2,1)} %bitcast.23), calls=%async_computation.5 | async-start | bytes 524288 | tf_op jit(solution)/shard_map/all_to_all | solution.py:339

commit v7 on v6

--- a/solution.py
+++ b/solution.py
@@ -235,6 +235,36 @@
         mix_body,
         out_shape=jax.ShapeDtypeStruct((copies, values.shape[0], width), BF16),
     )(*operands)
+
+
+def lower_body(units_ref, weight_ref, out_ref):
+    tiles, height, seqs = units_ref.shape
+    rows = out_ref.shape[1]
+    team = weight_ref.shape[2] // LANES
+    lowered = jnp.zeros((seqs, weight_ref.shape[2]), F32)
+    squares = jnp.zeros((seqs, LANES), F32)
+    row = lax.broadcasted_iota(jnp.int32, (SPARE, LANES), 0)
+    both = (row < 2).astype(BF16)
+    for k in range(tiles):
+        tile = units_ref[k].T
+        lowered = lowered + jnp.dot(
+            tile[:, : height - SPARE], weight_ref[k], preferred_element_type=F32
+        )
+        squares = squares + jnp.dot(
+            tile[:, height - SPARE :], both, preferred_element_type=F32
+        )
+    scale = 1.0 / (squares / D + EPS)
+    for m in range(team):
+        block = (lowered[:, m * LANES : (m + 1) * LANES] * scale).astype(BF16)
+        for d in range(seqs // rows):
+            out_ref[d * team + m] = block[d * rows : (d + 1) * rows]
+
+
+def lower(units, weight, rows):
+    dests = units.shape[2] // rows * (weight.shape[2] // LANES)
+    return pl.pallas_call(
+        lower_body, out_shape=pltpu.VMEM((dests, rows, LANES), BF16)
+    )(on_chip(units), on_chip(weight))
 
 
 def layer(
@@ -288,10 +318,11 @@
     out_mine, out_other = swapped(w_out, 1, core, "tp")
     up_mine, up_other = swapped(up_half, 1, side, "kl")
     up_weight = in_order(up_mine, up_other, side, 0)
+    down_half = in_order(*swapped(w_down, 0, core, "tp"), core, 1)
     column_count = out_mine.shape[1]
     residual = lax.dynamic_slice_in_dim(inputs, core * column_count, column_count, 1)
-    whole, out_mine, out_other, up_weight, residual = lax.optimization_barrier(
-        (whole, out_mine, out_other, up_weight, residual)
+    whole, out_mine, out_other, up_weight, down_half, residual = lax.optimization_barrier(
+        (whole, out_mine, out_other, up_weight, down_half, residual)
     )
     out_weight = jnp.concatenate([out_mine, out_other], axis=0)
 
@@ -310,7 +341,11 @@
     mixed_in = mixed_in * lax.rsqrt(total_sq / SSM_WIDTH + EPS)[:, None]
     hidden = (residual.astype(F32) + mixed_in).astype(BF16)
 
-    all_hidden = to_everyone(hidden, ("dp", *TEAM)).reshape(n_dp, n_team, rows, -1)
+    all_hidden = to_everyone(hidden, ("dp", *TEAM))
+    down_weight = in_order(*swapped(down_half, 0, side, "kl"), side, 1)
+    down_weight = down_weight.reshape(n_far, -1, down_weight.shape[1])
+    all_hidden, down_weight = lax.optimization_barrier((all_hidden, down_weight))
+    all_hidden = all_hidden.reshape(n_dp, n_team, rows, -1)
     seqs = n_dp * rows
     all_hidden = jnp.moveaxis(all_hidden, 1, 2).reshape(seqs, -1)
     raised = lax.dot_general(
@@ -318,31 +353,16 @@
     ).astype(BF16)
     row_sq = jnp.sum(jnp.square(all_hidden.astype(F32)), axis=1)
     arrived = lax.all_to_all(raised.reshape(n_far, -1, seqs), "kh", 0, 0, tiled=True)
-    down_half = in_order(*swapped(w_down, 0, core, "tp"), core, 1)
-    down_weight = in_order(*swapped(down_half, 0, side, "kl"), side, 1)
-    down_weight = down_weight.reshape(n_far, -1, down_weight.shape[1])
-    down_weight = jnp.pad(down_weight, ((0, 0), (0, SPARE), (0, 0)))
-    down_weight = down_weight.reshape(-1, down_weight.shape[2])
     words = jnp.concatenate(
         [*[w[None] for w in two_words(row_sq)], jnp.zeros((SPARE - 2, seqs), BF16)], axis=0
     )
-    arrived, down_weight, words = lax.optimization_barrier((arrived, down_weight, words))
+    arrived, words = lax.optimization_barrier((arrived, words))
     shares = jnp.sum(arrived.astype(F32), axis=0)
     units = jnp.square(jax.nn.relu(shares)).astype(BF16)
     hidden_units = to_everyone(jnp.concatenate([units, words], axis=0), "kh")
-    hidden_units = hidden_units.reshape(-1, seqs)
-    lowered = lax.dot_general(
-        hidden_units, down_weight, (((0,), (0,)), ((), ())), preferred_element_type=F32
-    ).astype(BF16)
-    lowered = lowered.reshape(n_dp, rows, n_team, -1)
-    lowered = jnp.moveaxis(lowered, 2, 1).reshape(n_dp * n_team, rows, -1)
+    lowered = lower(hidden_units, down_weight, rows)
     lowered = lax.all_to_all(lowered, ("dp", *TEAM), 0, 0, tiled=True)
-    lowered = jnp.sum(lowered.astype(F32), axis=0)
-    unit_count = units.shape[0]
-    sq_words = hidden_units.reshape(n_far, -1, seqs)[:, unit_count : unit_count + 2]
-    sq_sum = jnp.sum(sq_words.astype(F32), axis=(0, 1))
-    sq_sum = lax.dynamic_slice_in_dim(sq_sum, lax.axis_index("dp") * rows, rows, 0)
-    return (hidden.astype(F32) + lowered / (sq_sum / D + EPS)[:, None]).astype(BF16)
+    return (hidden.astype(F32) + jnp.sum(lowered.astype(F32), axis=0)).astype(BF16)
 
 
 def solution(mesh):

time: 184 us -> 187 us (1.016)
  blocking collectives: 23 us -> 48.5 us
  waiting for transfers between devices: 47.2 us -> 34 us
  starting transfers between devices: 99.1 us -> 87.1 us
  other arithmetic: 2.23 us -> 4.12 us
    all_to_all x0 -> x1, blocking collectives: none -> 25.4 us  [layer(): lowered = lax.all_to_all(lowered, ('dp', *TEAM), 0, 0, tiled=True)]
    all_to_all x1 -> x0, starting transfers between devices: 11.8 us -> none  [layer(): lowered = lax.all_to_all(lowered, ('dp', *TEAM), 0, 0, tiled=True)]
    all_to_all x1 -> x0, waiting for transfers between devices: 10.8 us -> none  [layer(): lowered = lax.all_to_all(lowered, ('dp', *TEAM), 0, 0, tiled=True)]
    ppermute x5, waiting for transfers between devices: 8.86 us -> 13.5 us  [swapped(): lax.ppermute(other, axis, [(i, (i + 1) % size) for i in range(size)])]
    all_to_all x1, waiting for transfers between devices: 5.36 us -> 1.61 us  [layer(): arrived = lax.all_to_all(sent, KV, 0, 0, tiled=True)]
    all_to_all x1, waiting for transfers between devices: 3.7 us -> 0.34 us  [to_everyone(): lax.all_to_all(jnp.broadcast_to(shard[None], (size, *shard.shape)), axes,...]
    select_n x4, other arithmetic: 0.66 us -> 2.72 us  [in_order(): jnp.where(here == 0, jnp.concatenate([mine, other], axis=dim), jnp.concat...]
  transfers between devices with their start and end apart: 10 -> 9, of which waited for: 7 -> 6; matrix products, arithmetic and copies ran while one was open for 2% -> 2% of each run, Pallas kernels for 1% -> 2%
where the time goes in v7:
time: 187 us; the launch traced here: 186 us
  starting transfers between devices  87.1 us (47%)
  blocking collectives  48.5 us (26%)
  waiting for transfers between devices  34 us (18%)
  Pallas kernels  6.7 us (4%)
  other arithmetic  4.12 us (2%)
  local copies, waits for them, and re-layouts  3.95 us (2%)
    all_to_all x1, starting transfers between devices, layer(): arrived = lax.all_to_all(sent, KV, 0, 0, tiled=True)  44.2 us
    all_to_all x1, blocking collectives, layer(): lowered = lax.all_to_all(lowered, ('dp', *TEAM), 0, 0, tiled=True)  25.4 us
    all_to_all x1, blocking collectives, to_everyone(): lax.all_to_all(jnp.broadcast_to(shard[None], (size, *shard.shape)), axes,...  23.1 us
    all_to_all x1, waiting for transfers between devices, layer(): lax.all_to_all(raised.reshape(n_far, -1, seqs), 'kh', 0, 0, tiled=True)  16.4 us
    ppermute x5, starting transfers between devices, swapped(): lax.ppermute(other, axis, [(i, (i + 1) % size) for i in range(size)])  14.5 us
    ppermute x5, waiting for transfers between devices, swapped(): lax.ppermute(other, axis, [(i, (i + 1) % size) for i in range(size)])  13.5 us
    all_to_all x1, starting transfers between devices, layer(): whole = lax.all_to_all(whole, (*KV, 'tp'), 0, 0, tiled=True)  10.8 us
    all_to_all x1, starting transfers between devices, to_everyone(): lax.all_to_all(jnp.broadcast_to(shard[None], (size, *shard.shape)), axes,...  9.41 us
  transfers between devices with their start and end apart: 9, of which 6 were waited for; matrix products, arithmetic and copies ran while one was open for 2% of the time, Pallas kernels for 2%

profile of v7, /device:TPU:65, one launch (start us, length us, event | category | flops | bytes accessed | tf_op | source)
XLA Modules:
  0.0 186.0 jit_solution(12140405652990834668)
XLA Ops:
  0.0 2.6 %shard_map.235 = bf16[16,2,3200]{2,1,0:T(2,128)(2,1)} custom-call(bf16[32,256]{1,0:T(8,128)(2,1)} %x_ref.1, f32[1,256]{1,0:T(1,128)} %bitcast.49, bf16[256,1024]{1,0:T(8,128)(2,1)} %gate_ref.1, bf16[256,1024]{1,0:T(8,128)(2,1)} %input_ref.1, bf16[256,512]{1,0:T(8,128)(2,1)} %b_ref.1, bf16[256,512]{1,0:T(8,128)(2,1)} %c_ref.1, bf16[16,256]{1,0:T(8,128)(2,1)} %bitcast.48), custom_call_target="tpu_custom_call" | custom-call | tf_op jit(solution)/shard_map/pallas_call | solution.py:87
  2.6 44.2 %all-to-all-start = ((bf16[16,2,3200]{2,1,0:T(2,128)(2,1)}), bf16[16,2,3200]{2,1,0:T(2,128)(2,1)S(1)}, u32[]{:S(2)}, u32[]{:S(2)}) async-start(bf16[16,2,3200]{2,1,0:T(2,128)(2,1)} %shard_map.235), calls=%async_computation | async-start | bytes 409600 | tf_op jit(solution)/shard_map/all_to_all | solution.py:303
  46.8 0.0 copy-start.13
  46.9 0.6 copy-done.13
  47.5 0.2 multiply_convert_fusion
  47.7 0.0 copy-start
  47.7 3.2 %collective-permute-start = (bf16[128,1024]{1,0:T(8,128)(2,1)S(1)}, bf16[128,1024]{1,0:T(8,128)(2,1)}, u32[]{:S(2)}, u32[]{:S(2)}) collective-permute-start(bf16[128,1024]{1,0:T(8,128)(2,1)S(1)} %get-tuple-element.46), channel_id=1, source_target_pairs={{0,1},{1,0},{2,3},{3,2},{4,5},{5,4},{6,7},{7,6},{8,9},{9,8},{10,11... | collective-permute-start | bytes 786440 | tf_op jit(solution)/shard_map/ppermute | solution.py:40
  51.1 2.0 %collective-permute-start.3 = (bf16[1024,128]{1,0:T(8,128)(2,1)S(1)}, bf16[1024,128]{1,0:T(8,128)(2,1)}, u32[]{:S(2)}, u32[]{:S(2)}) collective-permute-start(bf16[1024,128]{1,0:T(8,128)(2,1)S(1)} %get-tuple-element.40), channel_id=1, source_target_pairs={{0,1},{1,0},{2,3},{3,2},{4,5},{5,4},{6,7},{7,6},{8,9},{9,8},{10,11... | collective-permute-start | bytes 786440 | tf_op jit(solution)/shard_map/ppermute | solution.py:40
  53.1 0.6 copy-done.14
  53.8 0.1 copy.37.refs_6_.bias_ref
  53.8 0.1 copy.38.log_ref
  54.0 0.5 copy-done.4
  54.4 0.1 copy-done.2
  54.6 0.0 copy-done.3
  54.6 1.6 shard_map.236
  56.2 1.2 maximum_select_fusion
  57.4 1.6 all-to-all-done.arrived_ref
  59.0 1.5 shard_map.237
  60.5 10.8 %all-to-all-start.1 = ((bf16[32,2,1152]{2,1,0:T(2,128)(2,1)}), bf16[32,2,1152]{2,1,0:T(2,128)(2,1)S(1)}, u32[]{:S(2)}, u32[]{:S(2)}) async-start(bf16[32,2,1152]{2,1,0:T(2,128)(2,1)} %shard_map.237), calls=%async_computation.1 | async-start | bytes 294912 | tf_op jit(solution)/shard_map/all_to_all | solution.py:316
  71.4 3.4 %collective-permute-start.2 = (bf16[256,512]{1,0:T(8,128)(2,1)S(1)}, bf16[256,512]{1,0:T(8,128)(2,1)S(1)}, u32[]{:S(2)}, u32[]{:S(2)}) collective-permute-start(bf16[256,512]{1,0:T(8,128)(2,1)S(1)} %get-tuple-element.42), channel_id=1, source_target_pairs={{0,2},{2,0},{1,3},{3,1},{4,6},{6,4},{5,7},{7,5},{8,10},{10,8},{9,1... | collective-permute-start | bytes 786440 | tf_op jit(solution)/shard_map/ppermute | solution.py:40
  74.9 2.6 %collective-permute-start.1 = (bf16[1024,128]{1,0:T(8,128)(2,1)S(1)}, bf16[1024,128]{1,0:T(8,128)(2,1)S(1)}, u32[]{:S(2)}, u32[]{:S(2)}) collective-permute-start(bf16[1024,128]{1,0:T(8,128)(2,1)S(1)} %get-tuple-element.43), channel_id=1, source_target_pairs={{0,1},{1,0},{2,3},{3,2},{4,5},{5,4},{6,7},{7,6},{8,9},{9,8},{10,11... | collective-permute-start | bytes 786440 | tf_op jit(solution)/shard_map/ppermute | solution.py:40
  77.6 1.2 maximum_select_fusion.2
  78.7 6.5 %collective-permute-done.2 = bf16[256,512]{1,0:T(8,128)(2,1)S(1)} collective-permute-done((bf16[256,512]{1,0:T(8,128)(2,1)S(1)}, bf16[256,512]{1,0:T(8,128)(2,1)S(1)}, u32[]{:S(2)}, u32[]{:S(2)}) %collective-permute-start.2) | collective-permute-done | bytes 262176 | tf_op jit(solution)/shard_map/ppermute | solution.py:40
  85.3 0.2 maximum_select_fusion.1
  85.5 2.2 %all-to-all-done.1 = bf16[32,2,1152]{2,1,0:T(2,128)(2,1)S(1)} async-done(((bf16[32,2,1152]{2,1,0:T(2,128)(2,1)}), bf16[32,2,1152]{2,1,0:T(2,128)(2,1)S(1)}, u32[]{:S(2)}, u32[]{:S(2)}) %all-to-all-start.1) | async-done | bytes 147488 | tf_op jit(solution)/shard_map/all_to_all | solution.py:316
  87.6 0.1 copy.39
  87.8 0.3 convert_reduce_fusion.2
  88.1 0.1 slice.8
  88.2 0.3 constant_dynamic-slice_fusion.3
  88.5 0.2 add_convert_fusion.1
  88.8 0.7 broadcast_in_dim.35
  89.5 9.4 %all-to-all-start.2 = ((bf16[32,32,128]{2,1,0:T(8,128)(2,1)}), bf16[32,32,128]{2,1,0:T(8,128)(2,1)S(1)}, u32[]{:S(2)}, u32[]{:S(2)}) async-start(bf16[32,32,128]{2,1,0:T(8,128)(2,1)} %broadcast_in_dim.35), calls=%async_computation.2 | async-start | bytes 524288 | tf_op jit(solution)/shard_map/all_to_all | solution.py:30
  99.0 3.3 %collective-permute-start.4 = (bf16[512,256]{1,0:T(8,128)(2,1)S(1)}, bf16[512,256]{1,0:T(8,128)(2,1)S(1)}, u32[]{:S(2)}, u32[]{:S(2)}) collective-permute-start(bf16[512,256]{1,0:T(8,128)(2,1)S(1)} %get-tuple-element.38), channel_id=1, source_target_pairs={{0,2},{2,0},{1,3},{3,1},{4,6},{6,4},{5,7},{7,5},{8,10},{10,8},{9,1... | collective-permute-start | bytes 786440 | tf_op jit(solution)/shard_map/ppermute | solution.py:40
  102.3 7.0 %collective-permute-done.4 = bf16[512,256]{1,0:T(8,128)(2,1)S(1)} collective-permute-done((bf16[512,256]{1,0:T(8,128)(2,1)S(1)}, bf16[512,256]{1,0:T(8,128)(2,1)S(1)}, u32[]{:S(2)}, u32[]{:S(2)}) %collective-permute-start.4) | collective-permute-done | bytes 262176 | tf_op jit(solution)/shard_map/ppermute | solution.py:40
  109.2 0.1 maximum_select_fusion.3.weight_ref
  109.4 0.3 all-to-all-done.2
  109.7 0.1 copy.40
  109.8 1.1 convolution_convert_fusion
  110.9 8.1 %all-to-all-start.3 = ((bf16[8,64,256]{2,1,0:T(8,128)(2,1)}), bf16[8,64,256]{2,1,0:T(8,128)(2,1)S(1)}, u32[]{:S(2)}, u32[]{:S(2)}) async-start(bf16[8,64,256]{2,1,0:T(8,128)(2,1)} %bitcast.18), calls=%async_computation.3 | async-start | bytes 524288 | tf_op jit(solution)/shard_map/all_to_all | solution.py:355
  119.0 0.1 pad.4.clone
  119.1 0.1 multiply_reduce_fusion
  119.2 0.1 reduce_sum.40
  119.3 0.1 maximum_maximum_fusion
  119.4 16.4 %all-to-all-done.3 = bf16[8,64,256]{2,1,0:T(8,128)(2,1)S(1)} async-done(((bf16[8,64,256]{2,1,0:T(8,128)(2,1)}), bf16[8,64,256]{2,1,0:T(8,128)(2,1)S(1)}, u32[]{:S(2)}, u32[]{:S(2)}) %all-to-all-start.3) | async-done | bytes 262176 | tf_op jit(solution)/shard_map/all_to_all | solution.py:355
  135.9 23.1 %all_to_all.30.units_ref = bf16[8,72,256]{2,1,0:T(8,128)(2,1)S(1)} all-to-all(bf16[8,72,256]{2,1,0:T(8,128)(2,1)S(1)} %broadcast_in_dim.37), channel_id=1, replica_groups=mesh['grp'=2,'dp'=8,'kh'=8,'kl'=2,'tp'=2] {'kh'}, dimensions={0} | all-to-all | bytes 589824 | tf_op jit(solution)/shard_map/all_to_all | solution.py:30
  159.0 1.0 shard_map.238
  160.0 25.4 %all_to_all.31 = bf16[32,32,128]{2,1,0:T(8,128)(2,1)S(1)} all-to-all(bf16[32,32,128]{2,1,0:T(8,128)(2,1)S(1)} %shard_map.238), channel_id=1, replica_groups=mesh['grp'=2,'dp'=8,'kh'=8,'kl'=2,'tp'=2] {'dp','kl','tp'}, dimensions={0} | all-to-all | bytes 524288 | tf_op jit(solution)/shard_map/all_to_all | solution.py:364
  185.4 0.6 add_convert_fusion
  (43 shorter events, 0.5 us)
Async XLA Ops:
  0.0 46.8 %copy-start.11 = (bf16[128,2048]{1,0:T(8,128)(2,1)S(1)}, bf16[128,2048]{1,0:T(8,128)(2,1)}, u32[]{:S(2)}) copy-start(bf16[128,2048]{1,0:T(8,128)(2,1)} %param.48) | copy-start | bytes 1572868
  2.6 56.4 %all-to-all-start = ((bf16[16,2,3200]{2,1,0:T(2,128)(2,1)}), bf16[16,2,3200]{2,1,0:T(2,128)(2,1)S(1)}, u32[]{:S(2)}, u32[]{:S(2)}) async-start(bf16[16,2,3200]{2,1,0:T(2,128)(2,1)} %shard_map.235), calls=%async_computation | async-start | bytes 409600 | tf_op jit(solution)/shard_map/all_to_all | solution.py:303
  46.8 0.7 copy-start.13
  47.7 3.3 %copy-start.9 = (bf16[2048,128]{1,0:T(8,128)(2,1)S(1)}, bf16[2048,128]{1,0:T(8,128)(2,1)}, u32[]{:S(2)}) copy-start(bf16[2048,128]{1,0:T(8,128)(2,1)} %param.49) | copy-start | bytes 1572868
  47.7 6.2 %copy-start = (bf16[2,128,1024]{2,1,0:T(8,128)(2,1)S(1)}, bf16[2,128,1024]{2,1,0:T(8,128)(2,1)}, u32[]{:S(2)}) copy-start(bf16[2,128,1024]{2,1,0:T(8,128)(2,1)} %values_ref.1) | copy-start | bytes 1572868
  47.7 6.2 %copy-start.1 = (bf16[2,128,512]{2,1,0:T(8,128)(2,1)S(1)}, bf16[2,128,512]{2,1,0:T(8,128)(2,1)}, u32[]{:S(2)}) copy-start(bf16[2,128,512]{2,1,0:T(8,128)(2,1)} %keys_ref.1) | copy-start | bytes 786436
  47.7 8.4 %collective-permute-start = (bf16[128,1024]{1,0:T(8,128)(2,1)S(1)}, bf16[128,1024]{1,0:T(8,128)(2,1)}, u32[]{:S(2)}, u32[]{:S(2)}) collective-permute-start(bf16[128,1024]{1,0:T(8,128)(2,1)S(1)} %get-tuple-element.46), channel_id=1, source_target_pairs={{0,1},{1,0},{2,3},{3,2},{4,5},{5,4},{6,7},{7,6},{8,9},{9,8},{10,11... | collective-permute-start | bytes 786440 | tf_op jit(solution)/shard_map/ppermute | solution.py:40
  51.0 2.8 %copy-start.15 = (f32[16]{0:T(128)S(1)}, f32[16]{0:T(128)}, u32[]{:S(2)}) copy-start(f32[16]{0:T(128)} %param.39) | copy-start | bytes 196
  51.0 2.9 %copy-start.5 = (f32[4,512]{1,0:T(4,128)S(1)}, f32[4,512]{1,0:T(4,128)}, u32[]{:S(2)}) copy-start(f32[4,512]{1,0:T(4,128)} %conv_c_ref.1) | copy-start | bytes 24580
  51.0 2.9 %copy-start.6 = (bf16[2,3,512]{2,0,1:T(2,128)(2,1)S(1)}, bf16[2,3,512]{2,0,1:T(2,128)(2,1)}, u32[]{:S(2)}) copy-start(bf16[2,3,512]{2,0,1:T(2,128)(2,1)} %param.36) | copy-start | bytes 18436
  51.0 2.9 %copy-start.7 = (bf16[2,3,512]{2,0,1:T(2,128)(2,1)S(1)}, bf16[2,3,512]{2,0,1:T(2,128)(2,1)}, u32[]{:S(2)}) copy-start(bf16[2,3,512]{2,0,1:T(2,128)(2,1)} %param.37) | copy-start | bytes 18436
  51.1 26.4 %collective-permute-start.3 = (bf16[1024,128]{1,0:T(8,128)(2,1)S(1)}, bf16[1024,128]{1,0:T(8,128)(2,1)}, u32[]{:S(2)}, u32[]{:S(2)}) collective-permute-start(bf16[1024,128]{1,0:T(8,128)(2,1)S(1)} %get-tuple-element.40), channel_id=1, source_target_pairs={{0,1},{1,0},{2,3},{3,2},{4,5},{5,4},{6,7},{7,6},{8,9},{9,8},{10,11... | collective-permute-start | bytes 786440 | tf_op jit(solution)/shard_map/ppermute | solution.py:40
  53.1 0.9 copy-start.8
  53.1 0.7 copy-start.14
  53.8 0.7 copy-start.4
  53.8 0.7 copy-start.2
  53.8 0.7 copy-start.3
  60.5 27.1 %all-to-all-start.1 = ((bf16[32,2,1152]{2,1,0:T(2,128)(2,1)}), bf16[32,2,1152]{2,1,0:T(2,128)(2,1)S(1)}, u32[]{:S(2)}, u32[]{:S(2)}) async-start(bf16[32,2,1152]{2,1,0:T(2,128)(2,1)} %shard_map.237), calls=%async_computation.1 | async-start | bytes 294912 | tf_op jit(solution)/shard_map/all_to_all | solution.py:316
  71.3 3.5 %copy-start.10 = (bf16[1024,256]{1,0:T(8,128)(2,1)S(1)}, bf16[1024,256]{1,0:T(8,128)(2,1)}, u32[]{:S(2)}) copy-start(bf16[1024,256]{1,0:T(8,128)(2,1)} %param.46) | copy-start | bytes 1572868
  71.4 6.1 %copy-start.12 = (bf16[32,256]{1,0:T(8,128)(2,1)S(1)}, bf16[32,256]{1,0:T(8,128)(2,1)}, u32[]{:S(2)}) copy-start(bf16[32,256]{1,0:T(8,128)(2,1)} %x_ref.1) | copy-start | bytes 49156
  71.4 13.9 %collective-permute-start.2 = (bf16[256,512]{1,0:T(8,128)(2,1)S(1)}, bf16[256,512]{1,0:T(8,128)(2,1)S(1)}, u32[]{:S(2)}, u32[]{:S(2)}) collective-permute-start(bf16[256,512]{1,0:T(8,128)(2,1)S(1)} %get-tuple-element.42), channel_id=1, source_target_pairs={{0,2},{2,0},{1,3},{3,1},{4,6},{6,4},{5,7},{7,5},{8,10},{10,8},{9,1... | collective-permute-start | bytes 786440 | tf_op jit(solution)/shard_map/ppermute | solution.py:40
  74.9 10.6 %collective-permute-start.1 = (bf16[1024,128]{1,0:T(8,128)(2,1)S(1)}, bf16[1024,128]{1,0:T(8,128)(2,1)S(1)}, u32[]{:S(2)}, u32[]{:S(2)}) collective-permute-start(bf16[1024,128]{1,0:T(8,128)(2,1)S(1)} %get-tuple-element.43), channel_id=1, source_target_pairs={{0,1},{1,0},{2,3},{3,2},{4,5},{5,4},{6,7},{7,6},{8,9},{9,8},{10,11... | collective-permute-start | bytes 786440 | tf_op jit(solution)/shard_map/ppermute | solution.py:40
  89.5 20.2 %all-to-all-start.2 = ((bf16[32,32,128]{2,1,0:T(8,128)(2,1)}), bf16[32,32,128]{2,1,0:T(8,128)(2,1)S(1)}, u32[]{:S(2)}, u32[]{:S(2)}) async-start(bf16[32,32,128]{2,1,0:T(8,128)(2,1)} %broadcast_in_dim.35), calls=%async_computation.2 | async-start | bytes 524288 | tf_op jit(solution)/shard_map/all_to_all | solution.py:30
  99.0 10.3 %collective-permute-start.4 = (bf16[512,256]{1,0:T(8,128)(2,1)S(1)}, bf16[512,256]{1,0:T(8,128)(2,1)S(1)}, u32[]{:S(2)}, u32[]{:S(2)}) collective-permute-start(bf16[512,256]{1,0:T(8,128)(2,1)S(1)} %get-tuple-element.38), channel_id=1, source_target_pairs={{0,2},{2,0},{1,3},{3,1},{4,6},{6,4},{5,7},{7,5},{8,10},{10,8},{9,1... | collective-permute-start | bytes 786440 | tf_op jit(solution)/shard_map/ppermute | solution.py:40
  110.9 24.9 %all-to-all-start.3 = ((bf16[8,64,256]{2,1,0:T(8,128)(2,1)}), bf16[8,64,256]{2,1,0:T(8,128)(2,1)S(1)}, u32[]{:S(2)}, u32[]{:S(2)}) async-start(bf16[8,64,256]{2,1,0:T(8,128)(2,1)} %bitcast.18), calls=%async_computation.3 | async-start | bytes 524288 | tf_op jit(solution)/shard_map/all_to_all | solution.py:355

commit v8 on v7

--- a/solution.py
+++ b/solution.py
@@ -321,8 +321,8 @@
     down_half = in_order(*swapped(w_down, 0, core, "tp"), core, 1)
     column_count = out_mine.shape[1]
     residual = lax.dynamic_slice_in_dim(inputs, core * column_count, column_count, 1)
-    whole, out_mine, out_other, up_weight, down_half, residual = lax.optimization_barrier(
-        (whole, out_mine, out_other, up_weight, down_half, residual)
+    whole, out_mine, out_other, residual = lax.optimization_barrier(
+        (whole, out_mine, out_other, residual)
     )
     out_weight = jnp.concatenate([out_mine, out_other], axis=0)
 
@@ -344,7 +344,7 @@
     all_hidden = to_everyone(hidden, ("dp", *TEAM))
     down_weight = in_order(*swapped(down_half, 0, side, "kl"), side, 1)
     down_weight = down_weight.reshape(n_far, -1, down_weight.shape[1])
-    all_hidden, down_weight = lax.optimization_barrier((all_hidden, down_weight))
+    all_hidden, up_weight = lax.optimization_barrier((all_hidden, up_weight))
     all_hidden = all_hidden.reshape(n_dp, n_team, rows, -1)
     seqs = n_dp * rows
     all_hidden = jnp.moveaxis(all_hidden, 1, 2).reshape(seqs, -1)
@@ -356,7 +356,7 @@
     words = jnp.concatenate(
         [*[w[None] for w in two_words(row_sq)], jnp.zeros((SPARE - 2, seqs), BF16)], axis=0
     )
-    arrived, words = lax.optimization_barrier((arrived, words))
+    arrived, words, down_weight = lax.optimization_barrier((arrived, words, down_weight))
     shares = jnp.sum(arrived.astype(F32), axis=0)
     units = jnp.square(jax.nn.relu(shares)).astype(BF16)
     hidden_units = to_everyone(jnp.concatenate([units, words], axis=0), "kh")

time: 187 us -> 184 us (0.984)
  starting transfers between devices: 87.1 us -> 81.5 us
  waiting for transfers between devices: 34 us -> 38.7 us
  other arithmetic: 4.12 us -> 2.05 us
    all_to_all x1, waiting for transfers between devices: 2.16 us -> 12.5 us  [layer(): whole = lax.all_to_all(whole, (*KV, 'tp'), 0, 0, tiled=True)]
    ppermute x5, waiting for transfers between devices: 13.5 us -> 5.75 us  [swapped(): lax.ppermute(other, axis, [(i, (i + 1) % size) for i in range(size)])]
    all_to_all x1, starting transfers between devices: 8.12 us -> 3.61 us  [layer(): lax.all_to_all(raised.reshape(n_far, -1, seqs), 'kh', 0, 0, tiled=True)]
    all_to_all x1, waiting for transfers between devices: 1.61 us -> 5.36 us  [layer(): arrived = lax.all_to_all(sent, KV, 0, 0, tiled=True)]
    select_n x4, other arithmetic: 2.72 us -> 0.65 us  [in_order(): jnp.where(here == 0, jnp.concatenate([mine, other], axis=dim), jnp.concat...]
  transfers between devices with their start and end apart: 9 -> 9, of which waited for: 6 -> 6; matrix products, arithmetic and copies ran while one was open for 2% -> 2% of each run, Pallas kernels for 2% -> 1%
where the time goes in v8:
time: 184 us; the launch traced here: 183 us
  starting transfers between devices  81.5 us (44%)
  blocking collectives  48.9 us (27%)
  waiting for transfers between devices  38.7 us (21%)
  Pallas kernels  6.7 us (4%)
  local copies, waits for them, and re-layouts  3.29 us (2%)
  other arithmetic  2.05 us (1%)
    all_to_all x1, starting transfers between devices, layer(): arrived = lax.all_to_all(sent, KV, 0, 0, tiled=True)  44.2 us
    all_to_all x1, blocking collectives, to_everyone(): lax.all_to_all(jnp.broadcast_to(shard[None], (size, *shard.shape)), axes,...  24.7 us
    all_to_all x1, blocking collectives, layer(): lowered = lax.all_to_all(lowered, ('dp', *TEAM), 0, 0, tiled=True)  24.2 us
    all_to_all x1, waiting for transfers between devices, layer(): lax.all_to_all(raised.reshape(n_far, -1, seqs), 'kh', 0, 0, tiled=True)  15.1 us
    ppermute x5, starting transfers between devices, swapped(): lax.ppermute(other, axis, [(i, (i + 1) % size) for i in range(size)])  13.9 us
    all_to_all x1, waiting for transfers between devices, layer(): whole = lax.all_to_all(whole, (*KV, 'tp'), 0, 0, tiled=True)  12.5 us
    all_to_all x1, starting transfers between devices, layer(): whole = lax.all_to_all(whole, (*KV, 'tp'), 0, 0, tiled=True)  10.6 us
    all_to_all x1, starting transfers between devices, to_everyone(): lax.all_to_all(jnp.broadcast_to(shard[None], (size, *shard.shape)), axes,...  9.28 us
  transfers between devices with their start and end apart: 9, of which 6 were waited for; matrix products, arithmetic and copies ran while one was open for 2% of the time, Pallas kernels for 1%

profile of v8, /device:TPU:65, one launch (start us, length us, event | category | flops | bytes accessed | tf_op | source)
XLA Modules:
  0.0 182.9 jit_solution(7140664612901122714)
XLA Ops:
  0.0 2.6 %shard_map.235 = bf16[16,2,3200]{2,1,0:T(2,128)(2,1)} custom-call(bf16[32,256]{1,0:T(8,128)(2,1)} %x_ref.1, f32[1,256]{1,0:T(1,128)} %bitcast.49, bf16[256,1024]{1,0:T(8,128)(2,1)} %gate_ref.1, bf16[256,1024]{1,0:T(8,128)(2,1)} %input_ref.1, bf16[256,512]{1,0:T(8,128)(2,1)} %b_ref.1, bf16[256,512]{1,0:T(8,128)(2,1)} %c_ref.1, bf16[16,256]{1,0:T(8,128)(2,1)} %bitcast.48), custom_call_target="tpu_custom_call" | custom-call | tf_op jit(solution)/shard_map/pallas_call | solution.py:87
  2.6 44.2 %all-to-all-start = ((bf16[16,2,3200]{2,1,0:T(2,128)(2,1)}), bf16[16,2,3200]{2,1,0:T(2,128)(2,1)S(1)}, u32[]{:S(2)}, u32[]{:S(2)}) async-start(bf16[16,2,3200]{2,1,0:T(2,128)(2,1)} %shard_map.235), calls=%async_computation | async-start | bytes 409600 | tf_op jit(solution)/shard_map/all_to_all | solution.py:303
  46.9 0.6 copy-done.13
  47.5 0.2 multiply_convert_fusion
  47.7 0.0 copy-start
  47.7 0.0 copy-start.1
  47.7 0.0 copy-start.5
  47.8 3.2 %collective-permute-start = (bf16[128,1024]{1,0:T(8,128)(2,1)S(1)}, bf16[128,1024]{1,0:T(8,128)(2,1)S(1)}, u32[]{:S(2)}, u32[]{:S(2)}) collective-permute-start(bf16[128,1024]{1,0:T(8,128)(2,1)S(1)} %get-tuple-element.44), channel_id=1, source_target_pairs={{0,1},{1,0},{2,3},{3,2},{4,5},{5,4},{6,7},{7,6},{8,9},{9,8},{10,11... | collective-permute-start | bytes 786440 | tf_op jit(solution)/shard_map/ppermute | solution.py:40
  51.1 0.1 copy.37.refs_6_.bias_ref
  51.2 0.1 copy.38.log_ref
  51.3 0.4 copy-done.6
  51.7 0.0 copy-done.2
  51.8 0.1 copy-done.3
  51.9 1.6 shard_map.236
  53.5 0.1 maximum_select_fusion
  53.6 5.4 %all-to-all-done.arrived_ref = bf16[16,2,3200]{2,1,0:T(2,128)(2,1)S(1)} async-done(((bf16[16,2,3200]{2,1,0:T(2,128)(2,1)}), bf16[16,2,3200]{2,1,0:T(2,128)(2,1)S(1)}, u32[]{:S(2)}, u32[]{:S(2)}) %all-to-all-start) | async-done | bytes 204832 | tf_op jit(solution)/shard_map/all_to_all | solution.py:303
  59.0 1.5 shard_map.237
  60.5 10.6 %all-to-all-start.1 = ((bf16[32,2,1152]{2,1,0:T(2,128)(2,1)}), bf16[32,2,1152]{2,1,0:T(2,128)(2,1)S(1)}, u32[]{:S(2)}, u32[]{:S(2)}) async-start(bf16[32,2,1152]{2,1,0:T(2,128)(2,1)} %shard_map.237), calls=%async_computation.1 | async-start | bytes 294912 | tf_op jit(solution)/shard_map/all_to_all | solution.py:316
  71.2 2.6 %collective-permute-start.1 = (bf16[1024,128]{1,0:T(8,128)(2,1)S(1)}, bf16[1024,128]{1,0:T(8,128)(2,1)S(1)}, u32[]{:S(2)}, u32[]{:S(2)}) collective-permute-start(bf16[1024,128]{1,0:T(8,128)(2,1)S(1)} %get-tuple-element.41), channel_id=1, source_target_pairs={{0,1},{1,0},{2,3},{3,2},{4,5},{5,4},{6,7},{7,6},{8,9},{9,8},{10,11... | collective-permute-start | bytes 786440 | tf_op jit(solution)/shard_map/ppermute | solution.py:40
  73.8 1.1 collective-permute-done.1
  75.0 12.5 %all-to-all-done.1 = bf16[32,2,1152]{2,1,0:T(2,128)(2,1)S(1)} async-done(((bf16[32,2,1152]{2,1,0:T(2,128)(2,1)}), bf16[32,2,1152]{2,1,0:T(2,128)(2,1)S(1)}, u32[]{:S(2)}, u32[]{:S(2)}) %all-to-all-start.1) | async-done | bytes 147488 | tf_op jit(solution)/shard_map/all_to_all | solution.py:316
  87.4 0.1 copy.39
  87.5 0.3 convert_reduce_fusion.2
  87.9 0.1 slice.8
  88.0 0.3 constant_dynamic-slice_fusion.7
  88.3 0.2 add_convert_fusion.1
  88.5 0.7 broadcast_in_dim.35
  89.3 9.3 %all-to-all-start.2 = ((bf16[32,32,128]{2,1,0:T(8,128)(2,1)}), bf16[32,32,128]{2,1,0:T(8,128)(2,1)S(1)}, u32[]{:S(2)}, u32[]{:S(2)}) async-start(bf16[32,32,128]{2,1,0:T(8,128)(2,1)} %broadcast_in_dim.35), calls=%async_computation.2 | async-start | bytes 524288 | tf_op jit(solution)/shard_map/all_to_all | solution.py:30
  98.6 2.6 %collective-permute-start.3 = (bf16[1024,128]{1,0:T(8,128)(2,1)S(1)}, bf16[1024,128]{1,0:T(8,128)(2,1)S(1)}, u32[]{:S(2)}, u32[]{:S(2)}) collective-permute-start(bf16[1024,128]{1,0:T(8,128)(2,1)S(1)} %get-tuple-element.38), channel_id=1, source_target_pairs={{0,1},{1,0},{2,3},{3,2},{4,5},{5,4},{6,7},{7,6},{8,9},{9,8},{10,11... | collective-permute-start | bytes 786440 | tf_op jit(solution)/shard_map/ppermute | solution.py:40
  101.3 3.0 %collective-permute-start.2 = (bf16[256,512]{1,0:T(8,128)(2,1)S(1)}, bf16[256,512]{1,0:T(8,128)(2,1)S(1)}, u32[]{:S(2)}, u32[]{:S(2)}) collective-permute-start(bf16[256,512]{1,0:T(8,128)(2,1)S(1)} %get-tuple-element.40), channel_id=1, source_target_pairs={{0,2},{2,0},{1,3},{3,1},{4,6},{6,4},{5,7},{7,5},{8,10},{10,8},{9,1... | collective-permute-start | bytes 786440 | tf_op jit(solution)/shard_map/ppermute | solution.py:40
  104.3 0.2 maximum_select_fusion.2
  104.6 2.4 %collective-permute-start.4 = (bf16[512,256]{1,0:T(8,128)(2,1)S(1)}, bf16[512,256]{1,0:T(8,128)(2,1)S(1)}, u32[]{:S(2)}, u32[]{:S(2)}) collective-permute-start(bf16[512,256]{1,0:T(8,128)(2,1)S(1)} %get-tuple-element.36), channel_id=1, source_target_pairs={{0,2},{2,0},{1,3},{3,1},{4,6},{6,4},{5,7},{7,5},{8,10},{10,8},{9,1... | collective-permute-start | bytes 786440 | tf_op jit(solution)/shard_map/ppermute | solution.py:40
  107.0 4.1 %collective-permute-done.2 = bf16[256,512]{1,0:T(8,128)(2,1)S(1)} collective-permute-done((bf16[256,512]{1,0:T(8,128)(2,1)S(1)}, bf16[256,512]{1,0:T(8,128)(2,1)S(1)}, u32[]{:S(2)}, u32[]{:S(2)}) %collective-permute-start.2) | collective-permute-done | bytes 262176 | tf_op jit(solution)/shard_map/ppermute | solution.py:40
  111.1 0.2 maximum_select_fusion.1
  111.3 0.1 copy.40
  111.5 1.1 convolution_convert_fusion
  112.5 3.6 %all-to-all-start.3 = ((bf16[8,64,256]{2,1,0:T(8,128)(2,1)}), bf16[8,64,256]{2,1,0:T(8,128)(2,1)S(1)}, u32[]{:S(2)}, u32[]{:S(2)}) async-start(bf16[8,64,256]{2,1,0:T(8,128)(2,1)} %bitcast.16), calls=%async_computation.3 | async-start | bytes 524288 | tf_op jit(solution)/shard_map/all_to_all | solution.py:355
  116.2 0.1 pad.12.clone
  116.2 0.5 collective-permute-done.4
  116.7 0.1 maximum_select_fusion.3.weight_ref
  116.8 0.1 multiply_reduce_fusion
  117.0 0.1 reduce_sum.40
  117.1 0.1 maximum_maximum_fusion
  117.1 15.1 %all-to-all-done.3 = bf16[8,64,256]{2,1,0:T(8,128)(2,1)S(1)} async-done(((bf16[8,64,256]{2,1,0:T(8,128)(2,1)}), bf16[8,64,256]{2,1,0:T(8,128)(2,1)S(1)}, u32[]{:S(2)}, u32[]{:S(2)}) %all-to-all-start.3) | async-done | bytes 262176 | tf_op jit(solution)/shard_map/all_to_all | solution.py:355
  132.3 24.7 %all_to_all.30.units_ref = bf16[8,72,256]{2,1,0:T(8,128)(2,1)S(1)} all-to-all(bf16[8,72,256]{2,1,0:T(8,128)(2,1)S(1)} %broadcast_in_dim.37), channel_id=1, replica_groups=mesh['grp'=2,'dp'=8,'kh'=8,'kl'=2,'tp'=2] {'kh'}, dimensions={0} | all-to-all | bytes 589824 | tf_op jit(solution)/shard_map/all_to_all | solution.py:30
  157.0 1.0 shard_map.238
  158.0 24.2 %all_to_all.31 = bf16[32,32,128]{2,1,0:T(8,128)(2,1)S(1)} all-to-all(bf16[32,32,128]{2,1,0:T(8,128)(2,1)S(1)} %shard_map.238), channel_id=1, replica_groups=mesh['grp'=2,'dp'=8,'kh'=8,'kl'=2,'tp'=2] {'dp','kl','tp'}, dimensions={0} | all-to-all | bytes 524288 | tf_op jit(solution)/shard_map/all_to_all | solution.py:364
  182.3 0.6 add_convert_fusion
  (43 shorter events, 0.5 us)
Async XLA Ops:
  0.0 46.8 %copy-start.11 = (bf16[128,2048]{1,0:T(8,128)(2,1)S(1)}, bf16[128,2048]{1,0:T(8,128)(2,1)}, u32[]{:S(2)}) copy-start(bf16[128,2048]{1,0:T(8,128)(2,1)} %param.48) | copy-start | bytes 1572868
  2.6 56.4 %all-to-all-start = ((bf16[16,2,3200]{2,1,0:T(2,128)(2,1)}), bf16[16,2,3200]{2,1,0:T(2,128)(2,1)S(1)}, u32[]{:S(2)}, u32[]{:S(2)}) async-start(bf16[16,2,3200]{2,1,0:T(2,128)(2,1)} %shard_map.235), calls=%async_computation | async-start | bytes 409600 | tf_op jit(solution)/shard_map/all_to_all | solution.py:303
  46.8 0.7 copy-start.13
  47.6 3.4 %copy-start.14 = (f32[16]{0:T(128)S(1)}, f32[16]{0:T(128)}, u32[]{:S(2)}) copy-start(f32[16]{0:T(128)} %param.38) | copy-start | bytes 196
  47.7 3.5 %copy-start.15 = (f32[16]{0:T(128)S(1)}, f32[16]{0:T(128)}, u32[]{:S(2)}) copy-start(f32[16]{0:T(128)} %param.39) | copy-start | bytes 196
  47.7 3.6 %copy-start = (bf16[2,128,1024]{2,1,0:T(8,128)(2,1)S(1)}, bf16[2,128,1024]{2,1,0:T(8,128)(2,1)}, u32[]{:S(2)}) copy-start(bf16[2,128,1024]{2,1,0:T(8,128)(2,1)} %values_ref.1) | copy-start | bytes 1572868
  47.7 3.6 %copy-start.1 = (bf16[2,128,512]{2,1,0:T(8,128)(2,1)S(1)}, bf16[2,128,512]{2,1,0:T(8,128)(2,1)}, u32[]{:S(2)}) copy-start(bf16[2,128,512]{2,1,0:T(8,128)(2,1)} %keys_ref.1) | copy-start | bytes 786436
  47.7 3.6 %copy-start.4 = (f32[4,512]{1,0:T(4,128)S(1)}, f32[4,512]{1,0:T(4,128)}, u32[]{:S(2)}) copy-start(f32[4,512]{1,0:T(4,128)} %conv_b_ref.1) | copy-start | bytes 24580
  47.7 3.6 %copy-start.5 = (f32[4,512]{1,0:T(4,128)S(1)}, f32[4,512]{1,0:T(4,128)}, u32[]{:S(2)}) copy-start(f32[4,512]{1,0:T(4,128)} %conv_c_ref.1) | copy-start | bytes 24580
  47.7 3.6 %copy-start.7 = (bf16[2,3,512]{2,0,1:T(2,128)(2,1)S(1)}, bf16[2,3,512]{2,0,1:T(2,128)(2,1)}, u32[]{:S(2)}) copy-start(bf16[2,3,512]{2,0,1:T(2,128)(2,1)} %param.37) | copy-start | bytes 18436
  47.7 3.6 %copy-start.8 = (f32[1024]{0:T(1024)S(1)}, f32[1024]{0:T(1024)}, u32[]{:S(2)}) copy-start(f32[1024]{0:T(1024)} %param.45) | copy-start | bytes 12292
  47.8 5.7 %collective-permute-start = (bf16[128,1024]{1,0:T(8,128)(2,1)S(1)}, bf16[128,1024]{1,0:T(8,128)(2,1)S(1)}, u32[]{:S(2)}, u32[]{:S(2)}) collective-permute-start(bf16[128,1024]{1,0:T(8,128)(2,1)S(1)} %get-tuple-element.44), channel_id=1, source_target_pairs={{0,1},{1,0},{2,3},{3,2},{4,5},{5,4},{6,7},{7,6},{8,9},{9,8},{10,11... | collective-permute-start | bytes 786440 | tf_op jit(solution)/shard_map/ppermute | solution.py:40
  51.1 0.7 copy-start.6
  51.1 0.7 copy-start.2
  51.2 0.7 copy-start.3
  59.0 12.1 %copy-start.9 = (bf16[1024,256]{1,0:T(8,128)(2,1)S(1)}, bf16[1024,256]{1,0:T(8,128)(2,1)}, u32[]{:S(2)}) copy-start(bf16[1024,256]{1,0:T(8,128)(2,1)} %param.46) | copy-start | bytes 1572868
  60.5 26.9 %all-to-all-start.1 = ((bf16[32,2,1152]{2,1,0:T(2,128)(2,1)}), bf16[32,2,1152]{2,1,0:T(2,128)(2,1)S(1)}, u32[]{:S(2)}, u32[]{:S(2)}) async-start(bf16[32,2,1152]{2,1,0:T(2,128)(2,1)} %shard_map.237), calls=%async_computation.1 | async-start | bytes 294912 | tf_op jit(solution)/shard_map/all_to_all | solution.py:316
  71.1 2.7 %copy-start.12 = (bf16[32,256]{1,0:T(8,128)(2,1)S(1)}, bf16[32,256]{1,0:T(8,128)(2,1)}, u32[]{:S(2)}) copy-start(bf16[32,256]{1,0:T(8,128)(2,1)} %x_ref.1) | copy-start | bytes 49156
  71.2 3.8 %collective-permute-start.1 = (bf16[1024,128]{1,0:T(8,128)(2,1)S(1)}, bf16[1024,128]{1,0:T(8,128)(2,1)S(1)}, u32[]{:S(2)}, u32[]{:S(2)}) collective-permute-start(bf16[1024,128]{1,0:T(8,128)(2,1)S(1)} %get-tuple-element.41), channel_id=1, source_target_pairs={{0,1},{1,0},{2,3},{3,2},{4,5},{5,4},{6,7},{7,6},{8,9},{9,8},{10,11... | collective-permute-start | bytes 786440 | tf_op jit(solution)/shard_map/ppermute | solution.py:40
  88.5 10.0 %copy-start.10 = (bf16[2048,128]{1,0:T(8,128)(2,1)S(1)}, bf16[2048,128]{1,0:T(8,128)(2,1)}, u32[]{:S(2)}) copy-start(bf16[2048,128]{1,0:T(8,128)(2,1)} %param.49) | copy-start | bytes 1572868
  89.3 22.0 %all-to-all-start.2 = ((bf16[32,32,128]{2,1,0:T(8,128)(2,1)}), bf16[32,32,128]{2,1,0:T(8,128)(2,1)S(1)}, u32[]{:S(2)}, u32[]{:S(2)}) async-start(bf16[32,32,128]{2,1,0:T(8,128)(2,1)} %broadcast_in_dim.35), calls=%async_computation.2 | async-start | bytes 524288 | tf_op jit(solution)/shard_map/all_to_all | solution.py:30
  98.6 5.7 %collective-permute-start.3 = (bf16[1024,128]{1,0:T(8,128)(2,1)S(1)}, bf16[1024,128]{1,0:T(8,128)(2,1)S(1)}, u32[]{:S(2)}, u32[]{:S(2)}) collective-permute-start(bf16[1024,128]{1,0:T(8,128)(2,1)S(1)} %get-tuple-element.38), channel_id=1, source_target_pairs={{0,1},{1,0},{2,3},{3,2},{4,5},{5,4},{6,7},{7,6},{8,9},{9,8},{10,11... | collective-permute-start | bytes 786440 | tf_op jit(solution)/shard_map/ppermute | solution.py:40
  101.3 9.8 %collective-permute-start.2 = (bf16[256,512]{1,0:T(8,128)(2,1)S(1)}, bf16[256,512]{1,0:T(8,128)(2,1)S(1)}, u32[]{:S(2)}, u32[]{:S(2)}) collective-permute-start(bf16[256,512]{1,0:T(8,128)(2,1)S(1)} %get-tuple-element.40), channel_id=1, source_target_pairs={{0,2},{2,0},{1,3},{3,1},{4,6},{6,4},{5,7},{7,5},{8,10},{10,8},{9,1... | collective-permute-start | bytes 786440 | tf_op jit(solution)/shard_map/ppermute | solution.py:40
  104.6 12.1 %collective-permute-start.4 = (bf16[512,256]{1,0:T(8,128)(2,1)S(1)}, bf16[512,256]{1,0:T(8,128)(2,1)S(1)}, u32[]{:S(2)}, u32[]{:S(2)}) collective-permute-start(bf16[512,256]{1,0:T(8,128)(2,1)S(1)} %get-tuple-element.36), channel_id=1, source_target_pairs={{0,2},{2,0},{1,3},{3,1},{4,6},{6,4},{5,7},{7,5},{8,10},{10,8},{9,1... | collective-permute-start | bytes 786440 | tf_op jit(solution)/shard_map/ppermute | solution.py:40
  112.5 19.7 %all-to-all-start.3 = ((bf16[8,64,256]{2,1,0:T(8,128)(2,1)}), bf16[8,64,256]{2,1,0:T(8,128)(2,1)S(1)}, u32[]{:S(2)}, u32[]{:S(2)}) async-start(bf16[8,64,256]{2,1,0:T(8,128)(2,1)} %bitcast.16), calls=%async_computation.3 | async-start | bytes 524288 | tf_op jit(solution)/shard_map/all_to_all | solution.py:355

commit v9 on v8

--- a/solution.py
+++ b/solution.py
@@ -235,6 +235,38 @@
         mix_body,
         out_shape=jax.ShapeDtypeStruct((copies, values.shape[0], width), BF16),
     )(*operands)
+
+
+def emit_body(core_ref, whole_ref, mine_ref, other_ref, residual_ref, out_ref, hidden_ref, half_ref):
+    core = core_ref[0]
+    each = whole_ref.shape[1]
+    width = mine_ref.shape[0]
+    for k in range(whole_ref.shape[0] // 2):
+        at = slice(k * each, (k + 1) * each)
+        half_ref[0, at] = whole_ref[2 * k + core].astype(F32)
+        half_ref[1, at] = whole_ref[2 * k + 1 - core].astype(F32)
+    own, partner = half_ref[0], half_ref[1]
+    mixed = jnp.dot(own[:, :width].astype(BF16), mine_ref[...], preferred_element_type=F32)
+    mixed = mixed + jnp.dot(
+        partner[:, :width].astype(BF16), other_ref[...], preferred_element_type=F32
+    )
+    squares = jnp.sum(own[:, width:] + partner[:, width:], axis=1, keepdims=True)
+    mixed = mixed * lax.rsqrt(squares / SSM_WIDTH + EPS)
+    hidden = (residual_ref[...].astype(F32) + mixed).astype(BF16)
+    hidden_ref[...] = hidden
+    for m in range(out_ref.shape[0]):
+        out_ref[m] = hidden
+
+
+def emit(core, whole, mine, other, residual, copies):
+    shape = residual.shape
+    in_chip = pl.BlockSpec(memory_space=pltpu.VMEM)
+    return pl.pallas_call(
+        emit_body,
+        in_specs=[pl.BlockSpec(memory_space=pltpu.SMEM)] + [in_chip] * 4,
+        out_shape=(jax.ShapeDtypeStruct((copies, *shape), BF16), pltpu.VMEM(shape, BF16)),
+        scratch_shapes=[pltpu.VMEM((2, shape[0], whole.shape[2]), F32)],
+    )(core[None], *[on_chip(x) for x in (whole, mine, other, residual)])
 
 
 def lower_body(units_ref, weight_ref, out_ref):
@@ -310,38 +342,21 @@
     scaled_up = (w_up.astype(F32) * gain_mlp[:, None]).astype(BF16)
     up_mine, up_other = swapped(scaled_up, 1, core, "tp")
     up_half = in_order(up_mine, up_other, core, 0)
-    arrived, up_half = lax.optimization_barrier((arrived, up_half))
+    down_half = in_order(*swapped(w_down, 0, core, "tp"), core, 1)
+    arrived, up_half, down_half = lax.optimization_barrier((arrived, up_half, down_half))
     whole = mix(arrived, convs, tails, columns, prepared, values, keys, gain, n_kv * n_tp)
-    width = gain_mix.shape[0]
     whole = lax.all_to_all(whole, (*KV, "tp"), 0, 0, tiled=True)
 
     out_mine, out_other = swapped(w_out, 1, core, "tp")
     up_mine, up_other = swapped(up_half, 1, side, "kl")
     up_weight = in_order(up_mine, up_other, side, 0)
-    down_half = in_order(*swapped(w_down, 0, core, "tp"), core, 1)
     column_count = out_mine.shape[1]
     residual = lax.dynamic_slice_in_dim(inputs, core * column_count, column_count, 1)
     whole, out_mine, out_other, residual = lax.optimization_barrier(
         (whole, out_mine, out_other, residual)
     )
-    out_weight = jnp.concatenate([out_mine, out_other], axis=0)
-
-    whole = whole.reshape(n_kv, n_tp, rows // n_kv, -1)
-    whole = jnp.moveaxis(whole, 1, 0).reshape(n_tp, rows, -1)
-    total_sq = jnp.sum(whole[:, :, width : width + 2].astype(F32), axis=(0, 2))
-    halves = whole[:, :, :width]
-    channels = jnp.concatenate(
-        [
-            lax.dynamic_index_in_dim(halves, core, 0, keepdims=False),
-            lax.dynamic_index_in_dim(halves, 1 - core, 0, keepdims=False),
-        ],
-        axis=1,
-    )
-    mixed_in = jnp.dot(channels, out_weight, preferred_element_type=F32)
-    mixed_in = mixed_in * lax.rsqrt(total_sq / SSM_WIDTH + EPS)[:, None]
-    hidden = (residual.astype(F32) + mixed_in).astype(BF16)
-
-    all_hidden = to_everyone(hidden, ("dp", *TEAM))
+    copies, hidden = emit(core, whole, out_mine, out_other, residual, n_dp * n_team)
+    all_hidden = lax.all_to_all(copies, ("dp", *TEAM), 0, 0, tiled=True)
     down_weight = in_order(*swapped(down_half, 0, side, "kl"), side, 1)
     down_weight = down_weight.reshape(n_far, -1, down_weight.shape[1])
     all_hidden, up_weight = lax.optimization_barrier((all_hidden, up_weight))

time: 184 us -> 181 us (0.984)
  waiting for transfers between devices: 38.7 us -> 36 us
  other arithmetic: 2.05 us -> 4.03 us
  local copies, waits for them, and re-layouts: 3.29 us -> 1.38 us
    all_to_all x1, waiting for transfers between devices: 5.36 us -> 1.92 us  [layer(): arrived = lax.all_to_all(sent, KV, 0, 0, tiled=True)]
    all_to_all x1, blocking collectives: 24.7 us -> 22.7 us  [to_everyone(): lax.all_to_all(jnp.broadcast_to(shard[None], (size, *shard.shape)), axes,...]
    select_n x4, other arithmetic: 0.65 us -> 2.52 us  [in_order(): jnp.where(here == 0, jnp.concatenate([mine, other], axis=dim), jnp.concat...]
  transfers between devices with their start and end apart: 9 -> 9, of which waited for: 6 -> 7; matrix products, arithmetic and copies ran while one was open for 2% -> 3% of each run, Pallas kernels for 1% -> 1%
where the time goes in v9:
time: 181 us; the launch traced here: 180 us
  starting transfers between devices  81 us (45%)
  blocking collectives  48.7 us (27%)
  waiting for transfers between devices  36 us (20%)
  Pallas kernels  7.69 us (4%)
  other arithmetic  4.03 us (2%)
    all_to_all x1, starting transfers between devices, layer(): arrived = lax.all_to_all(sent, KV, 0, 0, tiled=True)  44.4 us
    all_to_all x1, blocking collectives, layer(): lowered = lax.all_to_all(lowered, ('dp', *TEAM), 0, 0, tiled=True)  26 us
    all_to_all x1, blocking collectives, to_everyone(): lax.all_to_all(jnp.broadcast_to(shard[None], (size, *shard.shape)), axes,...  22.7 us
    all_to_all x1, waiting for transfers between devices, layer(): lax.all_to_all(raised.reshape(n_far, -1, seqs), 'kh', 0, 0, tiled=True)  15.1 us
    ppermute x5, starting transfers between devices, swapped(): lax.ppermute(other, axis, [(i, (i + 1) % size) for i in range(size)])  13.2 us
    all_to_all x1, waiting for transfers between devices, layer(): whole = lax.all_to_all(whole, (*KV, 'tp'), 0, 0, tiled=True)  12.5 us
    all_to_all x1, starting transfers between devices, layer(): whole = lax.all_to_all(whole, (*KV, 'tp'), 0, 0, tiled=True)  10.6 us
    all_to_all x1, starting transfers between devices, layer(): all_hidden = lax.all_to_all(copies, ('dp', *TEAM), 0, 0, tiled=True)  9.27 us
  transfers between devices with their start and end apart: 9, of which 7 were waited for; matrix products, arithmetic and copies ran while one was open for 3% of the time, Pallas kernels for 1%

profile of v9, /device:TPU:65, one launch (start us, length us, event | category | flops | bytes accessed | tf_op | source)
XLA Modules:
  0.0 180.2 jit_solution(3929925481692122587)
XLA Ops:
  0.0 2.6 %shard_map.235 = bf16[16,2,3200]{2,1,0:T(2,128)(2,1)} custom-call(bf16[32,256]{1,0:T(8,128)(2,1)} %x_ref.1, f32[1,256]{1,0:T(1,128)} %bitcast.39, bf16[256,1024]{1,0:T(8,128)(2,1)} %gate_ref.1, bf16[256,1024]{1,0:T(8,128)(2,1)} %input_ref.1, bf16[256,512]{1,0:T(8,128)(2,1)} %b_ref.1, bf16[256,512]{1,0:T(8,128)(2,1)} %c_ref.1, bf16[16,256]{1,0:T(8,128)(2,1)} %bitcast.38), custom_call_target="tpu_custom_call" | custom-call | tf_op jit(solution)/shard_map/pallas_call | solution.py:87
  2.6 44.4 %all-to-all-start = ((bf16[16,2,3200]{2,1,0:T(2,128)(2,1)}), bf16[16,2,3200]{2,1,0:T(2,128)(2,1)S(1)}, u32[]{:S(2)}, u32[]{:S(2)}) async-start(bf16[16,2,3200]{2,1,0:T(2,128)(2,1)} %shard_map.235), calls=%async_computation | async-start | bytes 409600 | tf_op jit(solution)/shard_map/all_to_all | solution.py:335
  47.0 0.2 multiply_convert_fusion
  47.2 0.0 copy-start.10
  47.2 0.0 copy-start
  47.2 3.2 %collective-permute-start = (bf16[128,1024]{1,0:T(8,128)(2,1)S(1)}, bf16[128,1024]{1,0:T(8,128)(2,1)S(1)}, u32[]{:S(2)}, u32[]{:S(2)}) collective-permute-start(bf16[128,1024]{1,0:T(8,128)(2,1)S(1)} %get-tuple-element.50), channel_id=1, source_target_pairs={{0,1},{1,0},{2,3},{3,2},{4,5},{5,4},{6,7},{7,6},{8,9},{9,8},{10,11... | collective-permute-start | bytes 786440 | tf_op jit(solution)/shard_map/ppermute | solution.py:40
  50.5 0.0 copy-start.16
  50.5 0.0 copy-start.4
  50.6 0.0 copy-start.7
  50.6 0.0 copy-start.8
  50.6 2.0 %collective-permute-start.1 = (bf16[1024,128]{1,0:T(8,128)(2,1)S(1)}, bf16[1024,128]{1,0:T(8,128)(2,1)}, u32[]{:S(2)}, u32[]{:S(2)}) collective-permute-start(bf16[1024,128]{1,0:T(8,128)(2,1)S(1)} %get-tuple-element.48), channel_id=1, source_target_pairs={{0,1},{1,0},{2,3},{3,2},{4,5},{5,4},{6,7},{7,6},{8,9},{9,8},{10,11... | collective-permute-start | bytes 786440 | tf_op jit(solution)/shard_map/ppermute | solution.py:40
  52.6 0.0 copy-start.6
  52.6 0.1 copy.32.refs_6_.bias_ref
  52.7 0.1 copy.33.log_ref
  52.8 0.4 copy-done.6
  53.3 0.0 copy-done.2
  53.3 0.1 copy-done.3
  53.4 1.6 shard_map.236
  55.0 1.0 maximum_select_fusion
  56.0 1.2 maximum_select_fusion.1
  57.2 1.9 %all-to-all-done.arrived_ref = bf16[16,2,3200]{2,1,0:T(2,128)(2,1)S(1)} async-done(((bf16[16,2,3200]{2,1,0:T(2,128)(2,1)}), bf16[16,2,3200]{2,1,0:T(2,128)(2,1)S(1)}, u32[]{:S(2)}, u32[]{:S(2)}) %all-to-all-start) | async-done | bytes 204832 | tf_op jit(solution)/shard_map/all_to_all | solution.py:335
  59.1 1.5 shard_map.237
  60.7 10.6 %all-to-all-start.1 = ((bf16[32,2,1152]{2,1,0:T(2,128)(2,1)}), bf16[32,2,1152]{2,1,0:T(2,128)(2,1)S(1)}, u32[]{:S(2)}, u32[]{:S(2)}) async-start(bf16[32,2,1152]{2,1,0:T(2,128)(2,1)} %shard_map.237), calls=%async_computation.1 | async-start | bytes 294912 | tf_op jit(solution)/shard_map/all_to_all | solution.py:348
  71.3 0.0 copy-start.13
  71.3 2.6 %collective-permute-start.2 = (bf16[1024,128]{1,0:T(8,128)(2,1)S(1)}, bf16[1024,128]{1,0:T(8,128)(2,1)S(1)}, u32[]{:S(2)}, u32[]{:S(2)}) collective-permute-start(bf16[1024,128]{1,0:T(8,128)(2,1)S(1)} %get-tuple-element.45), channel_id=1, source_target_pairs={{0,1},{1,0},{2,3},{3,2},{4,5},{5,4},{6,7},{7,6},{8,9},{9,8},{10,11... | collective-permute-start | bytes 786440 | tf_op jit(solution)/shard_map/ppermute | solution.py:40
  74.0 1.1 collective-permute-done.2.other_ref
  75.1 12.5 %all-to-all-done.1.whole_ref = bf16[32,2,1152]{2,1,0:T(2,128)(2,1)S(1)} async-done(((bf16[32,2,1152]{2,1,0:T(2,128)(2,1)}), bf16[32,2,1152]{2,1,0:T(2,128)(2,1)S(1)}, u32[]{:S(2)}, u32[]{:S(2)}) %all-to-all-start.1) | async-done | bytes 147488 | tf_op jit(solution)/shard_map/all_to_all | solution.py:348
  87.6 1.0 shard_map.238
  88.5 9.3 %all-to-all-start.2 = ((bf16[32,32,128]{2,1,0:T(8,128)(2,1)}), bf16[32,32,128]{2,1,0:T(8,128)(2,1)S(1)}, u32[]{:S(2)}, u32[]{:S(2)}) async-start(bf16[32,32,128]{2,1,0:T(8,128)(2,1)} %get-tuple-element.33), calls=%async_computation.2 | async-start | bytes 524288 | tf_op jit(solution)/shard_map/all_to_all | solution.py:359
  97.9 3.3 %collective-permute-start.3 = (bf16[256,512]{1,0:T(8,128)(2,1)S(1)}, bf16[256,512]{1,0:T(8,128)(2,1)S(1)}, u32[]{:S(2)}, u32[]{:S(2)}) collective-permute-start(bf16[256,512]{1,0:T(8,128)(2,1)S(1)} %get-tuple-element.44), channel_id=1, source_target_pairs={{0,2},{2,0},{1,3},{3,1},{4,6},{6,4},{5,7},{7,5},{8,10},{10,8},{9,1... | collective-permute-start | bytes 786440 | tf_op jit(solution)/shard_map/ppermute | solution.py:40
  101.3 2.1 %collective-permute-start.4 = (bf16[512,256]{1,0:T(8,128)(2,1)S(1)}, bf16[512,256]{1,0:T(8,128)(2,1)S(1)}, u32[]{:S(2)}, u32[]{:S(2)}) collective-permute-start(bf16[512,256]{1,0:T(8,128)(2,1)S(1)} %get-tuple-element.42), channel_id=1, source_target_pairs={{0,2},{2,0},{1,3},{3,1},{4,6},{6,4},{5,7},{7,5},{8,10},{10,8},{9,1... | collective-permute-start | bytes 786440 | tf_op jit(solution)/shard_map/ppermute | solution.py:40
  103.3 4.8 %collective-permute-done.3 = bf16[256,512]{1,0:T(8,128)(2,1)S(1)} collective-permute-done((bf16[256,512]{1,0:T(8,128)(2,1)S(1)}, bf16[256,512]{1,0:T(8,128)(2,1)S(1)}, u32[]{:S(2)}, u32[]{:S(2)}) %collective-permute-start.3) | collective-permute-done | bytes 262176 | tf_op jit(solution)/shard_map/ppermute | solution.py:40
  108.1 0.2 maximum_select_fusion.2
  108.4 0.3 all-to-all-done.2
  108.6 0.1 copy.34
  108.8 1.1 convolution_convert_fusion
  109.8 3.6 %all-to-all-start.3 = ((bf16[8,64,256]{2,1,0:T(8,128)(2,1)}), bf16[8,64,256]{2,1,0:T(8,128)(2,1)S(1)}, u32[]{:S(2)}, u32[]{:S(2)}) async-start(bf16[8,64,256]{2,1,0:T(8,128)(2,1)} %bitcast.13), calls=%async_computation.3 | async-start | bytes 524288 | tf_op jit(solution)/shard_map/all_to_all | solution.py:370
  113.4 0.1 pad.8.clone
  113.5 0.2 collective-permute-done.4
  113.8 0.1 maximum_select_fusion.3.weight_ref
  113.9 0.6 multiply_reduce_fusion
  114.5 0.1 reduce_sum.30
  114.5 0.1 maximum_maximum_fusion
  114.6 15.1 %all-to-all-done.3 = bf16[8,64,256]{2,1,0:T(8,128)(2,1)S(1)} async-done(((bf16[8,64,256]{2,1,0:T(8,128)(2,1)}), bf16[8,64,256]{2,1,0:T(8,128)(2,1)S(1)}, u32[]{:S(2)}, u32[]{:S(2)}) %all-to-all-start.3) | async-done | bytes 262176 | tf_op jit(solution)/shard_map/all_to_all | solution.py:370
  129.9 22.7 %all_to_all.30.units_ref = bf16[8,72,256]{2,1,0:T(8,128)(2,1)S(1)} all-to-all(bf16[8,72,256]{2,1,0:T(8,128)(2,1)S(1)} %broadcast_in_dim.33), channel_id=1, replica_groups=mesh['grp'=2,'dp'=8,'kh'=8,'kl'=2,'tp'=2] {'kh'}, dimensions={0} | all-to-all | bytes 589824 | tf_op jit(solution)/shard_map/all_to_all | solution.py:30
  152.5 1.0 shard_map.239
  153.5 26.0 %all_to_all.31 = bf16[32,32,128]{2,1,0:T(8,128)(2,1)S(1)} all-to-all(bf16[32,32,128]{2,1,0:T(8,128)(2,1)S(1)} %shard_map.239), channel_id=1, replica_groups=mesh['grp'=2,'dp'=8,'kh'=8,'kl'=2,'tp'=2] {'dp','kl','tp'}, dimensions={0} | all-to-all | bytes 524288 | tf_op jit(solution)/shard_map/all_to_all | solution.py:379
  179.6 0.6 add_convert_fusion
  (38 shorter events, 0.4 us)
Async XLA Ops:
  0.0 47.0 %copy-start.12 = (bf16[128,2048]{1,0:T(8,128)(2,1)S(1)}, bf16[128,2048]{1,0:T(8,128)(2,1)}, u32[]{:S(2)}) copy-start(bf16[128,2048]{1,0:T(8,128)(2,1)} %param.48) | copy-start | bytes 1572868
  2.6 44.4 %copy-start.14 = (f32[128]{0:T(128)S(1)}, f32[128]{0:T(128)}, u32[]{:S(2)}) copy-start(f32[128]{0:T(128)} %param.47) | copy-start | bytes 1540
  2.6 56.5 %all-to-all-start = ((bf16[16,2,3200]{2,1,0:T(2,128)(2,1)}), bf16[16,2,3200]{2,1,0:T(2,128)(2,1)S(1)}, u32[]{:S(2)}, u32[]{:S(2)}) async-start(bf16[16,2,3200]{2,1,0:T(2,128)(2,1)} %shard_map.235), calls=%async_computation | async-start | bytes 409600 | tf_op jit(solution)/shard_map/all_to_all | solution.py:335
  47.2 3.3 %copy-start.10 = (bf16[2048,128]{1,0:T(8,128)(2,1)S(1)}, bf16[2048,128]{1,0:T(8,128)(2,1)}, u32[]{:S(2)}) copy-start(bf16[2048,128]{1,0:T(8,128)(2,1)} %param.49) | copy-start | bytes 1572868
  47.2 5.6 %copy-start = (bf16[2,128,1024]{2,1,0:T(8,128)(2,1)S(1)}, bf16[2,128,1024]{2,1,0:T(8,128)(2,1)}, u32[]{:S(2)}) copy-start(bf16[2,128,1024]{2,1,0:T(8,128)(2,1)} %values_ref.1) | copy-start | bytes 1572868
  47.2 5.6 %copy-start.1 = (bf16[2,128,512]{2,1,0:T(8,128)(2,1)S(1)}, bf16[2,128,512]{2,1,0:T(8,128)(2,1)}, u32[]{:S(2)}) copy-start(bf16[2,128,512]{2,1,0:T(8,128)(2,1)} %keys_ref.1) | copy-start | bytes 786436
  47.2 7.8 %collective-permute-start = (bf16[128,1024]{1,0:T(8,128)(2,1)S(1)}, bf16[128,1024]{1,0:T(8,128)(2,1)S(1)}, u32[]{:S(2)}, u32[]{:S(2)}) collective-permute-start(bf16[128,1024]{1,0:T(8,128)(2,1)S(1)} %get-tuple-element.50), channel_id=1, source_target_pairs={{0,1},{1,0},{2,3},{3,2},{4,5},{5,4},{6,7},{7,6},{8,9},{9,8},{10,11... | collective-permute-start | bytes 786440 | tf_op jit(solution)/shard_map/ppermute | solution.py:40
  50.5 2.1 %copy-start.15 = (f32[16]{0:T(128)S(1)}, f32[16]{0:T(128)}, u32[]{:S(2)}) copy-start(f32[16]{0:T(128)} %param.38) | copy-start | bytes 196
  50.5 2.2 %copy-start.16 = (f32[16]{0:T(128)S(1)}, f32[16]{0:T(128)}, u32[]{:S(2)}) copy-start(f32[16]{0:T(128)} %param.39) | copy-start | bytes 196
  50.5 2.3 %copy-start.4 = (f32[4,512]{1,0:T(4,128)S(1)}, f32[4,512]{1,0:T(4,128)}, u32[]{:S(2)}) copy-start(f32[4,512]{1,0:T(4,128)} %conv_b_ref.1) | copy-start | bytes 24580
  50.5 2.3 %copy-start.5 = (f32[4,512]{1,0:T(4,128)S(1)}, f32[4,512]{1,0:T(4,128)}, u32[]{:S(2)}) copy-start(f32[4,512]{1,0:T(4,128)} %conv_c_ref.1) | copy-start | bytes 24580
  50.6 2.3 %copy-start.7 = (bf16[2,3,512]{2,0,1:T(2,128)(2,1)S(1)}, bf16[2,3,512]{2,0,1:T(2,128)(2,1)}, u32[]{:S(2)}) copy-start(bf16[2,3,512]{2,0,1:T(2,128)(2,1)} %param.37) | copy-start | bytes 18436
  50.6 2.3 %copy-start.8 = (f32[1024]{0:T(1024)S(1)}, f32[1024]{0:T(1024)}, u32[]{:S(2)}) copy-start(f32[1024]{0:T(1024)} %param.45) | copy-start | bytes 12292
  50.6 5.4 %collective-permute-start.1 = (bf16[1024,128]{1,0:T(8,128)(2,1)S(1)}, bf16[1024,128]{1,0:T(8,128)(2,1)}, u32[]{:S(2)}, u32[]{:S(2)}) collective-permute-start(bf16[1024,128]{1,0:T(8,128)(2,1)S(1)} %get-tuple-element.48), channel_id=1, source_target_pairs={{0,1},{1,0},{2,3},{3,2},{4,5},{5,4},{6,7},{7,6},{8,9},{9,8},{10,11... | collective-permute-start | bytes 786440 | tf_op jit(solution)/shard_map/ppermute | solution.py:40
  52.6 0.7 copy-start.6
  52.6 0.7 copy-start.2
  52.7 0.7 copy-start.3
  59.1 12.1 %copy-start.11 = (bf16[1024,256]{1,0:T(8,128)(2,1)S(1)}, bf16[1024,256]{1,0:T(8,128)(2,1)}, u32[]{:S(2)}) copy-start(bf16[1024,256]{1,0:T(8,128)(2,1)} %param.46) | copy-start | bytes 1572868
  60.7 26.9 %all-to-all-start.1 = ((bf16[32,2,1152]{2,1,0:T(2,128)(2,1)}), bf16[32,2,1152]{2,1,0:T(2,128)(2,1)S(1)}, u32[]{:S(2)}, u32[]{:S(2)}) async-start(bf16[32,2,1152]{2,1,0:T(2,128)(2,1)} %shard_map.237), calls=%async_computation.1 | async-start | bytes 294912 | tf_op jit(solution)/shard_map/all_to_all | solution.py:348
  71.3 2.7 %copy-start.13 = (bf16[32,256]{1,0:T(8,128)(2,1)S(1)}, bf16[32,256]{1,0:T(8,128)(2,1)}, u32[]{:S(2)}) copy-start(bf16[32,256]{1,0:T(8,128)(2,1)} %x_ref.1) | copy-start | bytes 49156
  71.3 3.8 %collective-permute-start.2 = (bf16[1024,128]{1,0:T(8,128)(2,1)S(1)}, bf16[1024,128]{1,0:T(8,128)(2,1)S(1)}, u32[]{:S(2)}, u32[]{:S(2)}) collective-permute-start(bf16[1024,128]{1,0:T(8,128)(2,1)S(1)} %get-tuple-element.45), channel_id=1, source_target_pairs={{0,1},{1,0},{2,3},{3,2},{4,5},{5,4},{6,7},{7,6},{8,9},{9,8},{10,11... | collective-permute-start | bytes 786440 | tf_op jit(solution)/shard_map/ppermute | solution.py:40
  87.6 10.3 %copy-start.9 = (bf16[256,1024]{1,0:T(8,128)(2,1)S(1)}, bf16[256,1024]{1,0:T(8,128)(2,1)}, u32[]{:S(2)}) copy-start(bf16[256,1024]{1,0:T(8,128)(2,1)} %maximum_select_fusion) | copy-start | bytes 1572868
  88.5 20.1 %all-to-all-start.2 = ((bf16[32,32,128]{2,1,0:T(8,128)(2,1)}), bf16[32,32,128]{2,1,0:T(8,128)(2,1)S(1)}, u32[]{:S(2)}, u32[]{:S(2)}) async-start(bf16[32,32,128]{2,1,0:T(8,128)(2,1)} %get-tuple-element.33), calls=%async_computation.2 | async-start | bytes 524288 | tf_op jit(solution)/shard_map/all_to_all | solution.py:359
  97.9 10.2 %collective-permute-start.3 = (bf16[256,512]{1,0:T(8,128)(2,1)S(1)}, bf16[256,512]{1,0:T(8,128)(2,1)S(1)}, u32[]{:S(2)}, u32[]{:S(2)}) collective-permute-start(bf16[256,512]{1,0:T(8,128)(2,1)S(1)} %get-tuple-element.44), channel_id=1, source_target_pairs={{0,2},{2,0},{1,3},{3,1},{4,6},{6,4},{5,7},{7,5},{8,10},{10,8},{9,1... | collective-permute-start | bytes 786440 | tf_op jit(solution)/shard_map/ppermute | solution.py:40
  101.3 12.5 %collective-permute-start.4 = (bf16[512,256]{1,0:T(8,128)(2,1)S(1)}, bf16[512,256]{1,0:T(8,128)(2,1)S(1)}, u32[]{:S(2)}, u32[]{:S(2)}) collective-permute-start(bf16[512,256]{1,0:T(8,128)(2,1)S(1)} %get-tuple-element.42), channel_id=1, source_target_pairs={{0,2},{2,0},{1,3},{3,1},{4,6},{6,4},{5,7},{7,5},{8,10},{10,8},{9,1... | collective-permute-start | bytes 786440 | tf_op jit(solution)/shard_map/ppermute | solution.py:40
  109.8 19.9 %all-to-all-start.3 = ((bf16[8,64,256]{2,1,0:T(8,128)(2,1)}), bf16[8,64,256]{2,1,0:T(8,128)(2,1)S(1)}, u32[]{:S(2)}, u32[]{:S(2)}) async-start(bf16[8,64,256]{2,1,0:T(8,128)(2,1)} %bitcast.13), calls=%async_computation.3 | async-start | bytes 524288 | tf_op jit(solution)/shard_map/all_to_all | solution.py:370
